TPU v7x, 128 devices: a whole 4x4x4 slice. The times are simulated.
128 devices in a mesh: sp: 32 (over z, y, core), tp: 4 (over x).
Axes of the slice: x: 4, y: 4, z: 4, core: 2. Of those that a mesh axis runs over, the one named last changes fastest.
Arguments:
- tokens: bfloat16 [32768, 2048], P(('sp', 'tp')), may hold values from -6 to 6
- norm_gain: float32 [2048], replicated, may hold values from 0.1 to 1.9
- w_query: bfloat16 [2048, 2048], P(None, 'tp'), may hold values from -0.125 to 0.125
- w_forget: bfloat16 [2048, 2048], P(None, 'tp'), may hold values from -0.125 to 0.125
- w_value: bfloat16 [2048, 2048], P(None, 'tp'), may hold values from -0.125 to 0.125
- w_rgate: bfloat16 [2048, 2048], P(None, 'tp'), may hold values from -0.125 to 0.125
- w_glu_value: bfloat16 [2048, 2048], P(None, 'tp'), may hold values from -0.125 to 0.125
- w_glu_gate: bfloat16 [2048, 2048], P(None, 'tp'), may hold values from -0.125 to 0.125
- forget_gap: float32 [2048], P('tp'), may hold values from 1.5258789e-05 to 0.1
- decay_shift: float32 [32768, 16], P('sp', 'tp'), may hold values from -0.6 to 0, as said below
- head_gain: float32 [128], replicated, may hold values from 0.1 to 1.9
- conv_taps: float32 [31, 2048], P(None, 'tp'), may hold values from -12 to 12
- conv_gain: float32 [2048], P('tp'), may hold values from 0.1 to 1.9
- out_rec: bfloat16 [2048, 2048], P('tp'), may hold values from -0.09375 to 0.09375
- out_conv: bfloat16 [2048, 2048], P('tp'), may hold values from -0.09375 to 0.09375
Outputs:
- mixed: bfloat16 [32768, 2048], P(('sp', 'tp'))
Inputs may be any that keep to these rules, and one draw needn't show every extreme that they name: `decay_shift`: at most zero everywhere.
All inputs are finite; a program needn't handle non-finite values.
Results may differ from a plain program's by a relative error of at most 0.015.
Values may be sent and summed in bfloat16 or wider, within the bound.
No kernel may reach another device: no remote copies, remote signals or barrier semaphores. Data moves between devices by JAX's collectives and lax.ppermute only.
A program may use at most 128 MiB of HBM per device.

v0:
```python
import jax
import jax.numpy as jnp
from jax import lax
from jax.sharding import PartitionSpec as P

HEAD = 128
BLOCK = 64


norm_epsilon = 1e-05
head_epsilon = 1e-06


def from_everyone(array, axis):
    copies = jnp.broadcast_to(array, (lax.axis_size(axis), *array.shape))
    return lax.all_to_all(copies, axis, split_axis=0, concat_axis=0, tiled=True)


def in_order(blocks, dim):
    shape = list(blocks.shape[1:])
    shape[dim] *= blocks.shape[0]
    return jnp.moveaxis(blocks, 0, dim).reshape(shape)


def gathered_copies(array, axis, dim):
    blocks = from_everyone(array, axis)
    return in_order(blocks, dim)


def from_behind(value, axis, steps):
    count = lax.axis_size(axis)
    first, last = (max(0, -steps), min(count, count - steps))
    return lax.ppermute(value, axis, [(source, source + steps) for source in range(first, last)])


def work_in_pieces(array, axis, dim, apply, out_dim):
    size, extent = (lax.axis_size(axis), array.shape[dim])
    count = 2 if extent % 2 == 0 else 1
    finished, length = ([], extent // count)
    for k in range(count):
        share = lax.slice_in_dim(array, k * length, (k + 1) * length, axis=dim)
        starts = jnp.arange(size) * extent + k * length
        finished.append(jax.vmap(apply)(lax.all_gather(share, axis), starts))
    return in_order(jnp.concatenate(finished, axis=out_dim + 1), out_dim)


def layer_norm(values, gain):
    widened = values.astype(jnp.float32)
    row_mean = jnp.mean(widened, axis=-1, keepdims=True)
    centred = widened - row_mean
    row_var = jnp.mean(centred * centred, axis=-1, keepdims=True)
    return centred * lax.rsqrt(row_var + norm_epsilon) * gain


def local_scan(query, key_gate, values, log_forget):
    row_count, head_count, key_width = query.shape
    value_width = values.shape[2]
    block_count = row_count // BLOCK

    def to_blocks(array):
        return array.reshape(block_count, BLOCK, head_count, array.shape[2]).transpose(0, 2, 1, 3)

    def from_blocks(array):
        return array.transpose(0, 2, 1, 3).reshape(row_count, head_count, array.shape[3])

    causal = lax.broadcasted_iota(jnp.int32, (BLOCK, BLOCK), 0) >= lax.broadcasted_iota(
        jnp.int32, (BLOCK, BLOCK), 1
    )

    def advance(carried, inputs):
        current_state, offset = carried
        query_blk, key_block, value_block, log_blk = inputs
        running_total = jnp.cumsum(log_blk, axis=1)
        closing_log = running_total[:, -1:, :]
        query_decayed = query_blk * jnp.exp(running_total)
        scores = jnp.einsum("htk,hsk->hts", query_decayed, key_block * jnp.exp(-running_total))
        scores = jnp.where(causal[None], scores, 0.0)
        output_rows = jnp.einsum("hts,hsv->htv", scores, value_block)
        output_rows = output_rows + jnp.einsum("ori,oiq->orq", query_decayed, current_state)
        query_distant = query_blk * jnp.exp(running_total + offset[:, None, :])
        current_state = jnp.exp(closing_log[:, 0, :])[:, :, None] * current_state + jnp.einsum(
            "itp,ito->ipo", key_block * jnp.exp(closing_log - running_total), value_block
        )
        return ((current_state, offset + closing_log[:, 0, :]), (output_rows, query_distant))

    start_state = jnp.zeros((head_count, key_width, value_width), jnp.float32)
    start_offset = jnp.zeros((head_count, key_width), jnp.float32)
    final, stacked = lax.scan(
        advance,
        (start_state, start_offset),
        (to_blocks(query), to_blocks(key_gate), to_blocks(values), to_blocks(log_forget)),
    )
    return (final[0], final[1], from_blocks(stacked[0]), from_blocks(stacked[1]))


def recur(query_raw, forget_raw, value_raw, rgate_raw, forget_gap, decay_shift, head_gain):
    row_count = query_raw.shape[0]
    head_count = query_raw.shape[1] // HEAD
    query = jax.nn.silu(query_raw.astype(jnp.float32)).reshape(row_count, head_count, HEAD)
    key_gate = forget_gap * jax.nn.sigmoid(-forget_raw.astype(jnp.float32))
    log_forget = jnp.log1p(-key_gate).reshape(row_count, head_count, HEAD) + decay_shift[:, :, None]
    values = value_raw.astype(jnp.float32).reshape(row_count, head_count, HEAD)
    final_state, total_log, nearby_output, query_distant = local_scan(
        query, key_gate.reshape(row_count, head_count, HEAD), values, log_forget
    )
    logs_all = gathered_copies(total_log[None], "sp", 0)
    after_logs = jnp.cumsum(logs_all, axis=0)
    my_index = lax.axis_index("sp")
    own_log = lax.dynamic_index_in_dim(after_logs - logs_all, my_index, 0, keepdims=False)
    segment_piece = lax.all_gather(
        final_state[None].astype(jnp.bfloat16), "sp", axis=0, tiled=True
    ).astype(jnp.float32)
    piece_rows = segment_piece.shape[0]
    indices = jnp.arange(piece_rows, dtype=jnp.int32)
    multiplier = jnp.where(
        (indices < my_index)[:, None, None],
        jnp.exp(jnp.minimum(own_log[None] - after_logs, 0.0)),
        0.0,
    )
    arriving_state = jnp.zeros_like(final_state) + jnp.einsum(
        "dbq,dbqu->bqu", multiplier, segment_piece
    )
    recurrent_branch = nearby_output + jnp.einsum("bji,jiy->bjy", query_distant, arriving_state)
    recurrent_branch = (
        recurrent_branch
        * lax.rsqrt(
            jnp.mean(recurrent_branch * recurrent_branch, axis=-1, keepdims=True) + head_epsilon
        )
        * head_gain
    )
    return (
        recurrent_branch.reshape(row_count, head_count * HEAD)
        * jax.nn.silu(rgate_raw.astype(jnp.float32))
    ).astype(jnp.bfloat16)


def convolve(glu_value, glu_gate, conv_taps, conv_gain):
    row_count = glu_value.shape[0]
    mixed_in = (
        glu_value.astype(jnp.float32) * jax.nn.sigmoid(glu_gate.astype(jnp.float32))
    ).astype(jnp.bfloat16)
    reach = conv_taps.shape[0] - 1
    rim = from_behind(mixed_in[row_count - reach :], "sp", 1)
    padded = lax.optimization_barrier(jnp.concatenate([rim, mixed_in], axis=0)).astype(jnp.float32)
    filtered = jnp.zeros(glu_value.shape, jnp.float32)
    for tap_index in range(reach + 1):
        filtered = filtered + conv_taps[tap_index] * padded[tap_index : tap_index + row_count]
    row_sum, row_square = lax.psum(
        (jnp.sum(filtered, axis=1), jnp.sum(filtered * filtered, axis=1)), "tp"
    )
    channels = filtered.shape[1] * lax.axis_size("tp")
    row_mean = row_sum / channels
    row_var = row_square / channels - row_mean * row_mean
    normed = (filtered - row_mean[:, None]) * lax.rsqrt(row_var[:, None] + norm_epsilon) * conv_gain
    return jax.nn.silu(normed).astype(jnp.bfloat16)


def on_device(
    tokens,
    norm_gain,
    w_query,
    w_forget,
    w_value,
    w_rgate,
    w_glu_value,
    w_glu_gate,
    forget_gap,
    decay_shift,
    head_gain,
    conv_taps,
    conv_gain,
    out_rec,
    out_conv,
):
    weights = (w_query, w_forget, w_value, w_rgate, w_glu_value, w_glu_gate)

    def project(segment_piece, first_row):
        normed = layer_norm(segment_piece, norm_gain).astype(jnp.bfloat16)
        return jnp.concatenate(
            [
                jnp.dot(normed, weight, preferred_element_type=jnp.float32).astype(jnp.bfloat16)
                for weight in weights
            ],
            axis=1,
        )

    projected_in = work_in_pieces(tokens, "tp", 0, project, 0)
    rec_width = w_query.shape[1]
    conv_width = w_glu_value.shape[1]
    query_raw = projected_in[:, 0:rec_width]
    forget_raw = projected_in[:, rec_width : 2 * rec_width]
    value_raw = projected_in[:, 2 * rec_width : 3 * rec_width]
    rgate_raw = projected_in[:, 3 * rec_width : 4 * rec_width]
    glu_value = projected_in[:, 4 * rec_width : 4 * rec_width + conv_width]
    glu_gate = projected_in[:, 4 * rec_width + conv_width : 4 * rec_width + 2 * conv_width]
    conv_out = convolve(glu_value, glu_gate, conv_taps, conv_gain)
    rec_out = recur(query_raw, forget_raw, value_raw, rgate_raw, forget_gap, decay_shift, head_gain)
    return lax.psum_scatter(
        (
            jnp.dot(rec_out, out_rec, preferred_element_type=jnp.float32)
            + jnp.dot(conv_out, out_conv, preferred_element_type=jnp.float32)
        ).astype(jnp.bfloat16),
        "tp",
        scatter_dimension=0,
        tiled=True,
    )


def solution(mesh):
    placed = (
        P(("sp", "tp"), None),
        P(),
        P(None, "tp"),
        P(None, "tp"),
        P(None, "tp"),
        P(None, "tp"),
        P(None, "tp"),
        P(None, "tp"),
        P("tp"),
        P("sp", "tp"),
        P(),
        P(None, "tp"),
        P("tp"),
        P("tp", None),
        P("tp", None),
    )
    return jax.shard_map(
        on_device, mesh=mesh, in_specs=placed, out_specs=P(("sp", "tp"), None), check_vma=False
    )
```

profile of v0, /device:TPU:1, one launch (start us, length us, event | category | flops | bytes accessed | tf_op | source)
XLA Modules:
  0.0 319.8 jit_solution(3020927366686600964)
XLA Ops:
  6.5 2.5 fusion.174
  9.9 1.0 copy.46
  11.0 32.0 %all-gather.7.cloned.1.call-done = bf16[512,2048]{1,0:T(8,128)(2,1)} async-done(((bf16[128,2048]{1,0:T(8,128)(2,1)}), bf16[512,2048]{1,0:T(8,128)(2,1)}) %all-gather.7.cloned.1.call-update) | async-done | bytes 2097168 | tf_op jit(solution)/shard_map/all_gather | solution.py:43
  43.0 2.3 convert_element_type.114
  46.2 29.3 %all-gather.9.cloned.1.call-done = bf16[512,2048]{1,0:T(8,128)(2,1)} async-done(((bf16[128,2048]{1,0:T(8,128)(2,1)}), bf16[512,2048]{1,0:T(8,128)(2,1)}) %all-gather.9.cloned.1.call-update) | async-done | bytes 2097168 | tf_op jit(solution)/shard_map/all_gather | solution.py:43
  75.5 2.1 convert_reduce_fusion
  78.8 1.0 copy-done.4
  79.8 1.4 multiply_convert_fusion.1
  81.3 1.3 fusion.95
  82.6 2.1 fusion.89
  84.7 1.2 fusion.107
  85.9 2.1 fusion.101
  88.0 1.3 fusion.119
  89.3 2.1 fusion.113
  91.5 1.2 fusion.131
  92.7 2.1 fusion.125
  94.9 1.3 fusion.143
  96.1 2.1 fusion.137
  98.3 1.2 fusion.155
  99.5 2.1 fusion.149
  101.6 2.3 pad_maximum_fusion
  104.0 1.2 slice.489
  105.1 3.7 %multiply_convert_fusion.3 = (bf16[1024,512]{1,0:T(8,128)(2,1)S(1)}, f32[1024,512]{1,0:T(8,128)}, f32[1024,512]{1,0:T(8,128)}, f32[1024,512]{1,0:T(8,128)}) fusion(bf16[1024,3072]{1,0:T(8,128)(2,1)S(1)} %bitcast.220, f32[512]{0:T(512)S(1)} %copy-done.11), kind=kLoop, calls=%fused_computation.141 | loop fusion | flops 8912896 | bytes 11536384 | tf_op jit(solution)/shard_map/convert_element_type | solution.py:141
  108.8 1.9 reshape.86
  110.7 3.2 reshape_reshape.10
  113.9 2.1 reshape.91
  116.0 2.9 reshape_reshape.12
  119.0 3.2 add_bitcast_fusion
  122.1 80.5 %while.17 = (s32[]{:T(128)}, f32[4,128,128]{2,1,0:T(8,128)S(1)}, f32[4,128]{1,0:T(4,128)S(1)}, f32[16,4,64,128]{3,2,0,1:T(8,128)}, bf16[16,4,64,128]{3,2,0,1:T(8...) while((s32[]{:T(128)}, f32[4,128,128]{2,1,0:T(8,128)S(1)}, ...), condition=%wide.region_6.0_spmd.clone, body=%wide.region_4.6_spmd.clone.sunk | while | flops 27808772 | bytes 4092065 | solution.py:88
  123.2 1.0 constant_dynamic-slice_fusion.8
  128.3 1.0 constant_dynamic-slice_fusion.8
  133.3 1.0 constant_dynamic-slice_fusion.8
  158.5 1.0 constant_dynamic-slice_fusion.8
  163.5 1.0 constant_dynamic-slice_fusion.8
  183.6 1.0 constant_dynamic-slice_fusion.8
  188.6 1.0 constant_dynamic-slice_fusion.8
  193.7 1.0 constant_dynamic-slice_fusion.8
  203.5 3.8 %collective-permute-start = (bf16[30,512]{1,0:T(8,128)(2,1)S(1)}, bf16[30,512]{1,0:T(8,128)(2,1)S(1)}, u32[]{:S(2)}, u32[]{:S(2)}) collective-permute-start(bf16[30,512]{1,0:T(8,128)(2,1)S(1)} %slice.295), channel_id=1, source_target_pairs={{0,4},{4,8},{8,12},{12,16},{16,20},{20,24},{24,28},{28,32},{32,36}... | collective-permute-start | bytes 92168 | tf_op jit(solution)/shard_map/ppermute | solution.py:33
  207.3 1.9 copy.35
  209.9 6.8 %all-to-all-start = ((f32[32,1,4,128]{3,2,1,0:T(4,128)}), f32[32,1,4,128]{3,2,1,0:T(4,128)S(1)}, u32[]{:S(2)}, u32[]{:S(2)}) async-start(f32[32,1,4,128]{3,2,1,0:T(4,128)} %broadcast_in_dim.35), calls=%async_computation | async-start | bytes 131072 | tf_op jit(solution)/shard_map/all_to_all | solution.py:16
  217.3 9.5 %fusion.171 = (f32[1024]{0:T(1024)S(1)}, f32[1024]{0:T(1024)S(1)}, f32[1024,512]{1,0:T(8,128)}) fusion(f32[1054,512]{1,0:T(8,128)S(1)} %convert_element_type.111, f32[512]{0:T(512)S(1)} %bitcast.246, f32[512]{0:T(512)S(1)} %bitcast.247, f32[512]{0:T(512)S(1)} %bitcast.249, f32[512]{0:T(512)S(1)} %bitcast.250, f32[512]{0:T(512)S(1)} %bitcast.251, ...), kind=kLoop, calls=%fused_computation.198 | loop fusion | flops 33552384 | bytes 67180544 | tf_op jit(solution)/shard_map/reduce_sum | solution.py:149
  226.8 6.7 %all-reduce = (f32[1024]{0:T(1024)S(1)}, f32[1024]{0:T(1024)S(1)}) all-reduce(f32[1024]{0:T(1024)S(1)} %get-tuple-element.115, f32[1024]{0:T(1024)S(1)} %get-tuple-element.114), channel_id=1, replica_groups=mesh['sp'=32,'tp'=4] {'tp'}, use_global_device_ids=true, to_apply=%region_12.13 | all-reduce | flops 2048 | bytes 16384 | tf_op jit(solution)/shard_map/psum | solution.py:148
  233.7 16.6 %all-gather.11.cloned.1.call-done = bf16[128,128,128]{2,1,0:T(8,128)(2,1)} async-done(((bf16[4,128,128]{2,1,0:T(8,128)(2,1)}), bf16[128,128,128]{2,1,0:T(8,128)(2,1)}) %all-gather.11.cloned.1.call-update) | async-done | bytes 4194320 | tf_op jit(solution)/shard_map/all_gather | solution.py:110
  250.3 4.5 %multiply_reduce_fusion = bf16[4,128,128]{2,1,0:T(8,128)(2,1)S(1)} fusion(bf16[4,128,32,128]{3,1,0,2:T(8,128)(2,1)} %bitcast.226, f32[4,128,32]{1,0,2:T(4,128)S(1)} %select_bitcast_fusion), kind=kLoop, calls=%fused_computation.35 | loop fusion | flops 6225920 | bytes 4390912 | tf_op jit(solution)/shard_map/dbq,dbqu->bqu/dot_general | solution.py:120
  255.9 1.9 copy.36
  257.8 5.1 %fusion.158 = f32[1024,2048]{1,0:T(8,128)S(1)} fusion(bf16[512,2048]{1,0:T(8,128)(2,1)} %param.30, f32[1024,512]{1,0:T(8,128)} %copy.36, bf16[1024,3072]{1,0:T(8,128)(2,1)} %bitcast.221), kind=kOutput, calls=%fused_computation.173 | convolution fusion | flops 2151153664 | bytes 13631488 | tf_op jit(solution)/shard_map/dot_general | solution.py:200
  262.9 4.6 %add_convert_fusion = bf16[1024,2048]{1,0:T(8,128)(2,1)} fusion(f32[1024,2048]{1,0:T(8,128)S(1)} %fusion.158, bf16[512,2048]{1,0:T(8,128)(2,1)S(1)} %copy-done.18, f32[1024,512]{1,0:T(8,128)S(1)} %copy-done.6, f32[512]{0:T(512)S(1)} %copy-done.19, f32[1024]{0:T(1024)S(1)} %get-tuple-element.184, f32[1024]{0:T(1024)S(1)} %get-tuple-element.183), kind=kOutput, calls=%fused_computation.36 | convolution fusion | flops 2155872256 | bytes 16787456 | tf_op jit(solution)/shard_map/dot_general | solution.py:201
  267.5 45.8 %reduce-scatter.2.cloned.1.call-done = bf16[256,2048]{1,0:T(8,128)(2,1)} async-done(((bf16[1024,2048]{1,0:T(8,128)(2,1)}), bf16[256,2048]{1,0:T(8,128)(2,1)}) %reduce-scatter.2.cloned.1.call-update) | async-done | bytes 1048592 | tf_op jit(solution)/shard_map/reduce_scatter | solution.py:198
  (260 shorter events, 78.3 us)
Async XLA Ops:
  6.5 74.7 %copy-start = (bf16[2048,512]{1,0:T(8,128)(2,1)S(1)}, bf16[2048,512]{1,0:T(8,128)(2,1)}, u32[]{:S(2)}) copy-start(bf16[2048,512]{1,0:T(8,128)(2,1)} %param.19) | copy-start | bytes 6291460
  6.5 3.4 %copy-start.9 = (f32[1024,4]{0,1:T(4,128)S(1)}, f32[1024,4]{0,1:T(4,128)}, u32[]{:S(2)}) copy-start(f32[1024,4]{0,1:T(4,128)} %param.26) | copy-start | bytes 49156
  6.5 36.5 %all-gather.7.cloned.1.call-start = ((), (), s32[]{:S(2)}) async-start(), calls=%async_computation.3 | async-start | bytes 2621440 | tf_op jit(solution)/shard_map/all_gather | solution.py:43
  9.1 66.4 %all-gather.9.cloned.1.call-start = ((), (), s32[]{:S(2)}) async-start(), calls=%async_computation.4 | async-start | bytes 2621440 | tf_op jit(solution)/shard_map/all_gather | solution.py:43
  9.8 240.5 %all-gather.11.cloned.1.call-start = ((), (), s32[]{:S(2)}) async-start(), calls=%async_computation.5 | async-start | bytes 4325376 | tf_op jit(solution)/shard_map/all_gather | solution.py:110
  43.0 2.3 copy-start.3
  75.5 2.2 copy-start.5
  78.2 1.6 copy-start.4
  78.2 1.6 copy-start.10
  82.5 2.1 copy-start.13
  85.9 2.1 copy-start.14
  89.3 2.2 copy-start.15
  92.7 2.1 copy-start.16
  96.1 2.1 copy-start.17
  104.0 4.8 %copy-start.2 = (bf16[4,256,3072]{2,1,0:T(8,128)(2,1)}, bf16[4,256,3072]{2,1,0:T(8,128)(2,1)S(1)}, u32[]{:S(2)}) copy-start(bf16[4,256,3072]{2,1,0:T(8,128)(2,1)S(1)} %pad_maximum_fusion) | copy-start | bytes 18874372
  104.0 1.2 copy-start.11
  122.1 81.2 %copy-start.8 = (f32[31,512]{1,0:T(8,128)S(1)}, f32[31,512]{1,0:T(8,128)}, u32[]{:S(2)}) copy-start(f32[31,512]{1,0:T(8,128)} %param.28) | copy-start | bytes 190468
  203.5 13.3 %collective-permute-start = (bf16[30,512]{1,0:T(8,128)(2,1)S(1)}, bf16[30,512]{1,0:T(8,128)(2,1)S(1)}, u32[]{:S(2)}, u32[]{:S(2)}) collective-permute-start(bf16[30,512]{1,0:T(8,128)(2,1)S(1)} %slice.295), channel_id=1, source_target_pairs={{0,4},{4,8},{8,12},{12,16},{16,20},{20,24},{24,28},{28,32},{32,36}... | collective-permute-start | bytes 92168 | tf_op jit(solution)/shard_map/ppermute | solution.py:33
  209.9 23.6 %all-to-all-start = ((f32[32,1,4,128]{3,2,1,0:T(4,128)}), f32[32,1,4,128]{3,2,1,0:T(4,128)S(1)}, u32[]{:S(2)}, u32[]{:S(2)}) async-start(f32[32,1,4,128]{3,2,1,0:T(4,128)} %broadcast_in_dim.35), calls=%async_computation | async-start | bytes 131072 | tf_op jit(solution)/shard_map/all_to_all | solution.py:16
  216.7 96.5 %reduce-scatter.2.cloned.1.call-start = ((), (), s32[]{:S(2)}) async-start(), calls=%async_computation.2 | async-start | bytes 5242880 | tf_op jit(solution)/shard_map/reduce_scatter | solution.py:198
  250.3 4.5 %copy-start.7 = (bf16[16,4,64,128]{3,2,0,1:T(8,128)(2,1)S(1)}, bf16[16,4,64,128]{3,2,0,1:T(8,128)(2,1)}, u32[]{:S(2)}) copy-start(bf16[16,4,64,128]{3,2,0,1:T(8,128)(2,1)} %get-tuple-element.63) | copy-start | bytes 3145732
  254.8 0.7 copy-start.12
  257.8 5.1 %copy-start.6 = (f32[1024,512]{1,0:T(8,128)S(1)}, f32[1024,512]{1,0:T(8,128)}, u32[]{:S(2)}) copy-start(f32[1024,512]{1,0:T(8,128)} %get-tuple-element.138) | copy-start | bytes 6291460
  257.8 5.1 %copy-start.18 = (bf16[512,2048]{1,0:T(8,128)(2,1)S(1)}, bf16[512,2048]{1,0:T(8,128)(2,1)}, u32[]{:S(2)}) copy-start(bf16[512,2048]{1,0:T(8,128)(2,1)} %param.31) | copy-start | bytes 6291460
  257.8 5.1 %copy-start.19 = (f32[512]{0:T(512)S(1)}, f32[512]{0:T(512)}, u32[]{:S(2)}) copy-start(f32[512]{0:T(512)} %param.29) | copy-start | bytes 6148
  267.5 45.8 %copy-start.1 = (bf16[2048,512]{1,0:T(8,128)(2,1)S(1)}, bf16[2048,512]{1,0:T(8,128)(2,1)}, u32[]{:S(2)}) copy-start(bf16[2048,512]{1,0:T(8,128)(2,1)} %param.19) | copy-start | bytes 6291460
Sparse Core Ops, SparseCore 0:
  9.2 33.7 all-gather.6
  44.7 30.7 all-gather.8
  203.5 46.7 all-gather.10
  267.6 45.5 reduce-scatter.1
where the time goes:
time: 322 us; the launch traced here: 320 us
  waiting for transfers between devices  124 us (39%)
  local copies, waits for them, and re-layouts  65.3 us (20%)
  matrix products  52.5 us (16%)
  other arithmetic  46 us (14%)
  between operations  13.6 us (4%)
  starting transfers between devices  10.8 us (3%)
  blocking collectives  6.66 us (2%)
    all_gather x2, waiting for transfers between devices, work_in_pieces(): finished.append(jax.vmap(apply)(lax.all_gather(share, axis), starts))  61.3 us
    reduce_scatter x1, waiting for transfers between devices, on_device(): lax.psum_scatter((jnp.dot(rec_out, out_rec, preferred_element_type=jnp.fl...  45.8 us
    dynamic_slice x64, local copies, waits for them, and re-layouts, local_scan(): lax.scan(advance, (start_state, start_offset), (to_blocks(query), to_bloc...  44.5 us
    dot_general x12, matrix products, project(): jnp.dot(normed, weight, preferred_element_type=jnp.float32)  20.2 us
    all_gather x1, waiting for transfers between devices, recur(): lax.all_gather(final_state[None].astype(jnp.bfloat16), 'sp', axis=0, tile...  16.6 us
    dot_general x16, matrix products, advance(): jnp.einsum('ori,oiq->orq', query_decayed, current_state)  13.1 us
    dynamic_update_slice x16, other arithmetic, local_scan(): lax.scan(advance, (start_state, start_offset), (to_blocks(query), to_bloc...  10.6 us
    reduce_sum x1, other arithmetic, convolve(): jnp.sum(filtered, axis=1)  9.47 us
  transfers between devices with their start and end apart: 6, of which 4 were waited for; matrix products, arithmetic and copies ran while one was open for 5% of the time, Pallas kernels for 0%

commit v1 on v0

v1 whole, which is shorter than its diff:
```python
import functools

import jax
import jax.numpy as jnp
import numpy as np
from jax import lax
from jax.experimental import pallas as pl
from jax.experimental.pallas import tpu as pltpu
from jax.sharding import PartitionSpec as P


HEAD = 128
BLK = 128
NORM_EPS = 1e-05
HEAD_EPS = 1e-06
F32 = jnp.float32
BF16 = jnp.bfloat16


SLOT = np.array([[0, 1], [5, 3], [6, 7], [2, 4]])
SLOT_TABLE = np.array(
    [[SLOT[(p // 2 - t) % 4][p % 2] for p in range(8)] for t in range(4)], dtype=np.int32
)
PLACE_TABLE = np.argsort(SLOT_TABLE, axis=1).astype(np.int32)


def params(**kw):
    return pltpu.CompilerParams(vmem_limit_bytes=58 * 1024 * 1024, **kw)


def dot(a, b, dims=((1,), (0,))):
    return lax.dot_general(a, b, (dims, ((), ())), preferred_element_type=F32)


def silu(x):
    return x * jax.nn.sigmoid(x)


WIDE = 4 * HEAD


def gates(forget, gap, shift):
    key = gap * jax.nn.sigmoid(-forget.astype(F32))
    spread = jnp.concatenate(
        [jnp.broadcast_to(shift[:, h : h + 1], (BLK, HEAD)) for h in range(4)], axis=1
    )
    log_forget = jnp.log1p(-key) + spread
    high = log_forget.astype(BF16)
    low = (log_forget - high.astype(F32)).astype(BF16)
    rows = lax.broadcasted_iota(jnp.int32, (BLK, BLK), 0)
    cols = lax.broadcasted_iota(jnp.int32, (BLK, BLK), 1)
    lower = (rows >= cols).astype(F32).astype(BF16)
    return key, dot(lower, high) + dot(lower, low)


def pieces(log_row):
    high = log_row.astype(BF16).astype(F32)
    mid = (log_row - high).astype(BF16).astype(F32)
    low = log_row - high - mid
    row = lax.broadcasted_iota(jnp.int32, (16, HEAD), 0)
    tile = jnp.where(row == 0, high, jnp.where(row == 1, mid, jnp.where(row == 2, low, 0.0)))
    return tile.astype(BF16)


def block_state(key, run, value, store, close_store):
    close = run[BLK - 1 : BLK, :]
    key_far = (key * jnp.exp(close - run)).astype(BF16)
    close_store(jnp.broadcast_to(close, (8, WIDE)))
    for h in range(4):
        lanes = slice(h * HEAD, (h + 1) * HEAD)
        store(h, dot(value[:, lanes], key_far[:, lanes], ((0,), (0,))))


def block_outputs(key, run, value, query, near, query_near, at):
    middle = run[BLK // 2 - 1 : BLK // 2, :]
    query_mid = silu(query.astype(F32)) * jnp.exp(run - middle)
    key_mid = (key * jnp.exp(middle - run)).astype(BF16)
    query_near[at, :] = (query_mid * jnp.exp(middle)).astype(BF16)
    query_mid = query_mid.astype(BF16)
    rows = lax.broadcasted_iota(jnp.int32, (BLK, BLK), 0)
    cols = lax.broadcasted_iota(jnp.int32, (BLK, BLK), 1)
    for h in range(4):
        lanes = slice(h * HEAD, (h + 1) * HEAD)
        scores = dot(query_mid[:, lanes], key_mid[:, lanes], ((1,), (1,)))
        scores = jnp.where(rows >= cols, scores, 0.0).astype(BF16)
        near[at, lanes] = dot(scores, value[:, lanes])


def fetch(tokens, weights, xbuf, wbuf, sems):
    loads = [
        pltpu.make_async_copy(x, xbuf.at[pl.ds(k * BLK, BLK)], sems.at[k]) for k, x in enumerate(tokens)
    ]
    brings = [
        pltpu.make_async_copy(w, wbuf.at[k], sems.at[len(tokens) + k]) for k, w in enumerate(weights)
    ]
    for copy in loads + brings:
        copy.start()
    return loads, brings


def normalise(loads, xbuf, gain, normed):
    g = gain[...]
    for k, load in enumerate(loads):
        load.wait()
        for r in range(k * BLK, (k + 1) * BLK, 32):
            rows = xbuf[r : r + 32, :].astype(F32)
            centred = rows - jnp.mean(rows, axis=-1, keepdims=True)
            var = jnp.mean(centred * centred, axis=-1, keepdims=True)
            normed[r : r + 32, :] = (centred * lax.rsqrt(var + NORM_EPS) * g).astype(BF16)


def glu(value, gate):
    return (value.astype(F32) * jax.nn.sigmoid(gate.astype(F32))).astype(BF16)


def whole_kernel(slots, aliased, place, *refs):
    tokens, refs = refs[:slots], refs[slots:]
    gain, gap, refs = refs[0], refs[1], refs[2:]
    shifts, refs = refs[:slots], refs[slots:]
    weights, refs = refs[:6], refs[6 + aliased :]
    near, query_near, rgate, mixed, added, close, xbuf, normed, wbuf, raw, sems = refs
    loads, brings = fetch(tokens, weights, xbuf, wbuf, sems)
    normalise(loads, xbuf, gain, normed)

    def times(n):
        brings[n].wait()
        return dot(normed[...], wbuf[n]).astype(BF16)

    for n in range(3):
        raw[n] = times(n)
    for k in range(slots):
        at = slice(k * BLK, (k + 1) * BLK)
        key, run = gates(raw[0, at, :], gap[...], shifts[k][...])
        value = raw[1, at, :]

        def store(h, x):
            added[k, h] = x

        def close_store(x):
            close[k] = x

        block_state(key, run, value, store, close_store)
        block_outputs(key, run, value, raw[2, at, :], near, query_near, at)
    rgate[...] = times(3)
    raw[0] = times(4)
    raw[1] = times(5)
    mixed[...] = glu(raw[0], raw[1])


def any_spec():
    return pl.BlockSpec(memory_space=pl.ANY)


def row_spec(shape):
    return pl.BlockSpec(shape, lambda i, p: (0, 0))


BUFFERS = [((WIDE,), F32), ((WIDE,), BF16), ((WIDE,), BF16), ((WIDE,), BF16)]


def project_whole(first, tokens, place, gain, gap, shift, weights, bufs):
    slots = len(tokens)
    group = first // slots
    depth = tokens[0].shape[1]
    aliased = list(bufs) if bufs is not None else []
    rows = slots * BLK
    flat = lambda: pl.BlockSpec((rows, WIDE), lambda i, p: (group, 0))
    head_inputs = 1 + slots + 2 + slots + 6
    return pl.pallas_call(
        functools.partial(whole_kernel, slots, len(aliased)),
        grid_spec=pltpu.PrefetchScalarGridSpec(
            num_scalar_prefetch=1,
            grid=(1,),
            in_specs=[any_spec()] * slots
            + [row_spec((1, depth)), row_spec((1, WIDE))]
            + [pl.BlockSpec((BLK, 4), lambda i, p, k=k: (p[first + k], 0)) for k in range(slots)]
            + [any_spec()] * (6 + len(aliased)),
            out_specs=[flat(), flat(), flat(), flat()]
            + [
                pl.BlockSpec((slots, 4, HEAD, HEAD), lambda i, p: (group, 0, 0, 0)),
                pl.BlockSpec((slots, 8, WIDE), lambda i, p: (group, 0, 0)),
            ],
            scratch_shapes=[
                pltpu.VMEM((rows, depth), BF16),
                pltpu.VMEM((rows, depth), BF16),
                pltpu.VMEM((6, depth, WIDE), BF16),
                pltpu.VMEM((3, rows, WIDE), BF16),
                pltpu.SemaphoreType.DMA((slots + 6,)),
            ],
        ),
        out_shape=[jax.ShapeDtypeStruct((8 * BLK, *tail), kind) for tail, kind in BUFFERS]
        + [
            jax.ShapeDtypeStruct((8, 4, HEAD, HEAD), F32),
            jax.ShapeDtypeStruct((8, 8, WIDE), F32),
        ],
        input_output_aliases={head_inputs + k: k for k in range(len(aliased))},
        compiler_params=params(),
        cost_estimate=pl.CostEstimate(
            flops=2 * rows * depth * WIDE * 9, bytes_accessed=16 * 2**20, transcendentals=0
        ),
    )(place, *tokens, gain, gap, *[shift] * slots, *weights, *aliased)


def last_states_kernel(place, tokens_a, tokens_b, gain, gap, shift_a, shift_b, w_forget, w_value, added, close, fv, pack, starts, offsets, xbuf, normed, wbuf, parts, sems, more):
    loads, brings = fetch((tokens_a, tokens_b), (w_forget, w_value), xbuf, wbuf, sems)
    bring_parts = pltpu.make_async_copy(added.at[pl.ds(0, 6)], parts.at[pl.ds(0, 6)], more.at[0])
    bring_parts.start()
    normalise(loads, xbuf, gain, normed)
    for n in range(2):
        brings[n].wait()
        fv[:, n * WIDE : (n + 1) * WIDE] = dot(normed[...], wbuf[n]).astype(BF16)
    ends = [None] * 2
    for k, shift in enumerate((shift_a, shift_b)):
        at = slice(k * BLK, (k + 1) * BLK)
        key, run = gates(fv[at, 0:WIDE], gap[...], shift[...])

        def store(h, x):
            parts[6 + k, h] = x

        def close_store(x):
            close_now[k] = x

        close_now = {}
        block_state(key, run, fv[at, WIDE : 2 * WIDE], store, close_store)
        ends[k] = close_now[k]
    bring_parts.wait()
    state = [jnp.zeros((HEAD, HEAD), F32) for _ in range(4)]
    total = jnp.zeros((1, WIDE), F32)
    for i in range(8):
        slot = place[8 + i]
        offsets[slot] = jnp.broadcast_to(total, (8, WIDE))
        end = jnp.where(
            slot == 6, ends[0], jnp.where(slot == 7, ends[1], close[jnp.minimum(slot, 5)])
        )[0:1, :]
        keep = jnp.exp(end)
        for h in range(4):
            lanes = slice(h * HEAD, (h + 1) * HEAD)
            starts[slot, h] = state[h].astype(BF16)
            state[h] = state[h] * keep[:, lanes] + parts[slot, h]
        total = total + end
    for h in range(4):
        tile = pieces(total[:, h * HEAD : (h + 1) * HEAD])
        rows = state[h].astype(BF16)
        for j in range(8):
            pack[8 * h + j, 0:16, :] = rows[16 * j : 16 * j + 16, :]
            pack[8 * h + j, 16:32, :] = tile


def last_states(tokens, place, gain, gap, shift, weights, added, close):
    depth = tokens[0].shape[1]
    rows = 2 * BLK
    return pl.pallas_call(
        last_states_kernel,
        grid_spec=pltpu.PrefetchScalarGridSpec(
            num_scalar_prefetch=1,
            grid=(1,),
            in_specs=[any_spec()] * 2
            + [row_spec((1, depth)), row_spec((1, WIDE))]
            + [pl.BlockSpec((BLK, 4), lambda i, p, k=k: (p[6 + k], 0)) for k in range(2)]
            + [any_spec()] * 3
            + [pl.BlockSpec((8, 8, WIDE), lambda i, p: (0, 0, 0))],
            out_specs=[
                pl.BlockSpec((rows, 2 * WIDE), lambda i, p: (0, 0)),
                pl.BlockSpec((32, 32, HEAD), lambda i, p: (0, 0, 0)),
                pl.BlockSpec((8, 4, HEAD, HEAD), lambda i, p: (0, 0, 0, 0)),
                pl.BlockSpec((8, 8, WIDE), lambda i, p: (0, 0, 0)),
            ],
            scratch_shapes=[
                pltpu.VMEM((rows, depth), BF16),
                pltpu.VMEM((rows, depth), BF16),
                pltpu.VMEM((2, depth, WIDE), BF16),
                pltpu.VMEM((8, 4, HEAD, HEAD), F32),
                pltpu.SemaphoreType.DMA((4,)),
                pltpu.SemaphoreType.DMA((1,)),
            ],
        ),
        out_shape=[
            jax.ShapeDtypeStruct((rows, 2 * WIDE), BF16),
            jax.ShapeDtypeStruct((32, 32, HEAD), BF16),
            jax.ShapeDtypeStruct((8, 4, HEAD, HEAD), BF16),
            jax.ShapeDtypeStruct((8, 8, WIDE), F32),
        ],
        compiler_params=params(),
        cost_estimate=pl.CostEstimate(
            flops=2 * rows * depth * WIDE * 6, bytes_accessed=10 * 2**20, transcendentals=0
        ),
        name="last_states",
    )(place, *tokens, gain, gap, shift, shift, *weights, added, close)


def last_rest_kernel(place, tokens_a, tokens_b, gain, gap, shift_a, shift_b, fv, w_query, w_rgate, w_glu_value, w_glu_gate, b0, b1, b2, b3, near, query_near, rgate, mixed, xbuf, normed, wbuf, raw, sems):
    loads, brings = fetch(
        (tokens_a, tokens_b), (w_glu_value, w_glu_gate, w_query, w_rgate), xbuf, wbuf, sems
    )
    normalise(loads, xbuf, gain, normed)

    def times(n):
        brings[n].wait()
        return dot(normed[...], wbuf[n]).astype(BF16)

    for n in range(3):
        raw[n] = times(n)
    mixed[...] = glu(raw[0], raw[1])
    for k, shift in enumerate((shift_a, shift_b)):
        at = slice(k * BLK, (k + 1) * BLK)
        key, run = gates(fv[at, 0:WIDE], gap[...], shift[...])
        block_outputs(key, run, fv[at, WIDE : 2 * WIDE], raw[2, at, :], near, query_near, at)
    rgate[...] = times(3)


def last_rest(tokens, place, gain, gap, shift, fv, weights, bufs):
    depth = tokens[0].shape[1]
    rows = 2 * BLK
    flat = lambda: pl.BlockSpec((rows, WIDE), lambda i, p: (3, 0))
    return pl.pallas_call(
        last_rest_kernel,
        grid_spec=pltpu.PrefetchScalarGridSpec(
            num_scalar_prefetch=1,
            grid=(1,),
            in_specs=[any_spec()] * 2
            + [row_spec((1, depth)), row_spec((1, WIDE))]
            + [pl.BlockSpec((BLK, 4), lambda i, p, k=k: (p[6 + k], 0)) for k in range(2)]
            + [row_spec((rows, 2 * WIDE))]
            + [any_spec()] * 8,
            out_specs=[flat(), flat(), flat(), flat()],
            scratch_shapes=[
                pltpu.VMEM((rows, depth), BF16),
                pltpu.VMEM((rows, depth), BF16),
                pltpu.VMEM((4, depth, WIDE), BF16),
                pltpu.VMEM((3, rows, WIDE), BF16),
                pltpu.SemaphoreType.DMA((6,)),
            ],
        ),
        out_shape=[jax.ShapeDtypeStruct((8 * BLK, *tail), kind) for tail, kind in BUFFERS],
        input_output_aliases={12 + k: k for k in range(4)},
        compiler_params=params(),
        cost_estimate=pl.CostEstimate(
            flops=2 * rows * depth * WIDE * 6, bytes_accessed=12 * 2**20, transcendentals=0
        ),
        name="last_rest",
    )(place, *tokens, gain, gap, shift, shift, fv, *weights, *bufs)


def prefix_kernel(packs, arriving):
    state = jnp.zeros((16, HEAD), F32)
    for i in range(32):
        arriving[i] = state.astype(BF16)
        tile = packs[i, 16:32, :].astype(F32)
        log = tile[0:1] + tile[1:2] + tile[2:3]
        state = jnp.exp(log) * state + packs[i, 0:16, :].astype(F32)


def arriving_states(pack):
    packs = lax.all_to_all(pack, "sp", split_axis=0, concat_axis=0, tiled=True)
    arriving = pl.pallas_call(
        prefix_kernel,
        out_shape=jax.ShapeDtypeStruct((32, 16, HEAD), BF16),
        compiler_params=params(),
        cost_estimate=pl.CostEstimate(flops=10**8, bytes_accessed=2**20, transcendentals=0),
        name="prefix",
    )(packs)
    arrived = lax.all_to_all(arriving, "sp", split_axis=0, concat_axis=0, tiled=True)
    return arrived.reshape(4, HEAD, HEAD)


def filter_kernel(table, mixed, halo, taps, filtered, stats, window):
    i = pl.program_id(0)
    reach = 32

    @pl.when(i == 0)
    def _():
        window[0:reach, :] = halo[...].astype(F32)

    @pl.when(i > 0)
    def _():
        window[0:reach, :] = window[BLK : BLK + reach, :]

    window[reach : reach + BLK, :] = mixed[...].astype(F32)
    row_sum = jnp.zeros((BLK, HEAD), F32)
    row_square = jnp.zeros((BLK, HEAD), F32)
    for c in range(4):
        lanes = slice(c * HEAD, (c + 1) * HEAD)
        acc = jnp.zeros((BLK, HEAD), F32)
        for r in range(8):
            used = [q for q in range(5) if 0 <= 8 * q + r - 2 < 31]
            shifted = window[8 * used[0] + r : 8 * used[-1] + r + BLK, lanes]
            for q in used:
                j, lead = 8 * q + r - 2, 8 * (q - used[0])
                acc = acc + taps[j : j + 1, lanes] * shifted[lead : lead + BLK, :]
        filtered[:, lanes] = acc
        row_sum = row_sum + acc
        row_square = row_square + acc * acc
    lane = lax.broadcasted_iota(jnp.int32, (BLK, HEAD), 1)
    tile = jnp.where(
        lane == 0,
        jnp.sum(row_sum, axis=1, keepdims=True),
        jnp.where(lane == 1, jnp.sum(row_square, axis=1, keepdims=True), 0.0),
    )
    stats[...] = jnp.transpose(tile)[0:8, :]


def filter_rows(place, mixed, halo, taps):
    return pl.pallas_call(
        filter_kernel,
        grid_spec=pltpu.PrefetchScalarGridSpec(
            num_scalar_prefetch=1,
            grid=(8,),
            in_specs=[
                pl.BlockSpec((BLK, WIDE), lambda i, p: (p[8 + i], 0)),
                pl.BlockSpec((32, WIDE), lambda i, p: (0, 0)),
                pl.BlockSpec((31, WIDE), lambda i, p: (0, 0)),
            ],
            out_specs=[
                pl.BlockSpec((BLK, WIDE), lambda i, p: (p[8 + i], 0)),
                pl.BlockSpec((8, BLK), lambda i, p: (0, i)),
            ],
            scratch_shapes=[pltpu.VMEM((32 + BLK, WIDE), F32)],
        ),
        out_shape=[
            jax.ShapeDtypeStruct((8 * BLK, WIDE), F32),
            jax.ShapeDtypeStruct((8, 8 * BLK), F32),
        ],
        compiler_params=params(),
        cost_estimate=pl.CostEstimate(flops=7 * 10**9, bytes_accessed=5 * 2**20, transcendentals=0),
        name="filter_rows",
    )(place, mixed, halo, taps)


def merge_kernel(group, place, near, query_near, rgate, starts, offsets, arrived, head_gain, filtered, s0, s1, s2, s3, conv_gain, w_rec, w_conv, top, bottom, act):
    @pl.when(pl.program_id(0) == 0)
    def _():
        for k in range(2):
            rows = slice(k * BLK, (k + 1) * BLK)
            carry = jnp.exp(offsets[k, 0:1, :])
            for h in range(4):
                lanes = slice(h * HEAD, (h + 1) * HEAD)
                state = starts[k, h].astype(F32) + carry[:, lanes] * arrived[h].astype(F32)
                rec = near[rows, lanes] + dot(query_near[rows, lanes], state.astype(BF16), ((1,), (1,)))
                rec = rec * lax.rsqrt(jnp.mean(rec * rec, axis=-1, keepdims=True) + HEAD_EPS)
                rec = rec * head_gain[...] * silu(rgate[rows, lanes].astype(F32))
                act[rows, lanes] = rec.astype(BF16)
            at = pl.ds(pl.multiple_of(place[2 * group + k] * BLK, BLK), BLK)
            stats = (s0[:, at] + s1[:, at]) + (s2[:, at] + s3[:, at])
            tile = jnp.transpose(jnp.concatenate([stats] * 16, axis=0))
            mean = tile[:, 0:1] / 2048.0
            scale = lax.rsqrt(tile[:, 1:2] / 2048.0 - mean * mean + NORM_EPS)
            normed = (filtered[rows, :] - mean) * scale * conv_gain[...]
            act[rows, WIDE : 2 * WIDE] = silu(normed).astype(BF16)

    part = dot(act[:, 0:WIDE], w_rec[...]) + dot(act[:, WIDE : 2 * WIDE], w_conv[...])
    top[...] = part[0:BLK, :].astype(BF16)
    bottom[...] = part[BLK : 2 * BLK, :].astype(BF16)


def merge(group, place, near, query_near, rgate, starts, offsets, arrived, head_gain, filtered, stats, conv_gain, out_rec, out_conv):
    rows = 2 * BLK
    flat = lambda: pl.BlockSpec((rows, WIDE), lambda n: (group, 0))
    pair = pl.BlockSpec((BLK, WIDE), lambda n: (0, n))
    return pl.pallas_call(
        functools.partial(merge_kernel, group),
        grid=(4,),
        in_specs=[
            pl.BlockSpec(memory_space=pltpu.SMEM),
            flat(),
            flat(),
            flat(),
            pl.BlockSpec((2, 4, HEAD, HEAD), lambda n: (group, 0, 0, 0)),
            pl.BlockSpec((2, 8, WIDE), lambda n: (group, 0, 0)),
            pl.BlockSpec((4, HEAD, HEAD), lambda n: (0, 0, 0)),
            pl.BlockSpec((1, HEAD), lambda n: (0, 0)),
            flat(),
        ]
        + [pl.BlockSpec((8, 8 * BLK), lambda n: (0, 0))] * 4
        + [
            pl.BlockSpec((1, WIDE), lambda n: (0, 0)),
            pl.BlockSpec((WIDE, WIDE), lambda n: (0, n)),
            pl.BlockSpec((WIDE, WIDE), lambda n: (0, n)),
        ],
        out_specs=[pair, pair],
        out_shape=[jax.ShapeDtypeStruct((BLK, 2048), BF16)] * 2,
        scratch_shapes=[pltpu.VMEM((rows, 2 * WIDE), BF16)],
        compiler_params=params(),
        cost_estimate=pl.CostEstimate(
            flops=2 * rows * 1024 * 2048 * 3, bytes_accessed=7 * 2**20, transcendentals=0
        ),
    )(place, near, query_near, rgate, starts, offsets, arrived, head_gain, filtered, *stats, conv_gain, out_rec, out_conv)


def permuted(value, perm):
    return lax.ppermute(value, "tp", perm)


def on_device(
    tokens,
    norm_gain,
    w_query,
    w_forget,
    w_value,
    w_rgate,
    w_glu_value,
    w_glu_gate,
    forget_gap,
    decay_shift,
    head_gain,
    conv_taps,
    conv_gain,
    out_rec,
    out_conv,
):
    ahead = [(i, (i + 1) % 4) for i in range(4)]
    behind = [(i, (i - 1) % 4) for i in range(4)]
    t = lax.axis_index("tp")
    place = lax.dynamic_index_in_dim(
        jnp.asarray(np.concatenate([PLACE_TABLE, SLOT_TABLE], axis=1)), t, 0, keepdims=False
    )

    a, b = tokens[:BLK], tokens[BLK:]
    from_back_a = permuted(a, ahead)
    from_front_b = permuted(b, behind)
    from_back_b = permuted(b, ahead)
    from_front_a = permuted(a, behind)
    far_a = permuted(from_back_a, ahead)
    far_b = permuted(from_front_b, behind)

    gain, gap = norm_gain[None, :], forget_gap[None, :]
    common = (place, gain, gap, decay_shift)
    weights = (w_forget, w_value, w_query, w_rgate, w_glu_value, w_glu_gate)
    bufs = project_whole(0, (a, b), *common, weights, None)
    bufs = project_whole(2, (from_back_a, from_front_b), *common, weights, bufs)
    bufs = project_whole(4, (from_back_b, from_front_a), *common, weights, bufs)
    *bufs, added, close = bufs
    fv, pack, starts, offsets = last_states((far_a, far_b), *common, weights[:2], added, close)
    arrived = arriving_states(pack)
    near, query_near, rgate, mixed = last_rest((far_a, far_b), *common, fv, (w_query, w_rgate, w_glu_value, w_glu_gate), bufs)

    edge = lax.dynamic_slice(mixed, (place[15] * BLK + BLK - 32, 0), (32, WIDE))
    halo = lax.ppermute(edge, "sp", [(i, i + 1) for i in range(31)])
    filtered, stats = filter_rows(place, mixed, halo, conv_taps)
    stats_all = [stats] + [permuted(stats, [(i, (i + d) % 4) for i in range(4)]) for d in (1, 2, 3)]

    part = functools.partial(
        merge, place=place, near=near, query_near=query_near, rgate=rgate, starts=starts, offsets=offsets,
        arrived=arrived, head_gain=head_gain[None, :], filtered=filtered, stats=stats_all,
        conv_gain=conv_gain[None, :], out_rec=out_rec, out_conv=out_conv,
    )
    total = lambda *parts: functools.reduce(jnp.add, [p.astype(F32) for p in parts]).astype(BF16)
    far_top, far_bottom = part(3)
    via_back = permuted(far_top, ahead)
    via_front = permuted(far_bottom, behind)
    back_a, front_b = part(1)
    got_b = permuted(front_b, ahead)
    got_a = permuted(back_a, behind)
    back_b, front_a = part(2)
    sum_a = permuted(total(front_a, via_back), ahead)
    sum_b = permuted(total(back_b, via_front), behind)
    own_a, own_b = part(0)
    return jnp.concatenate([total(own_a, got_a, sum_a), total(own_b, got_b, sum_b)], axis=0)


def solution(mesh):
    placed = (
        P(("sp", "tp"), None),
        P(),
        P(None, "tp"),
        P(None, "tp"),
        P(None, "tp"),
        P(None, "tp"),
        P(None, "tp"),
        P(None, "tp"),
        P("tp"),
        P("sp", "tp"),
        P(),
        P(None, "tp"),
        P("tp"),
        P("tp", None),
        P("tp", None),
    )
    return jax.shard_map(on_device, mesh=mesh, in_specs=placed, out_specs=P(("sp", "tp"), None), check_vma=False)
```

time: 322 us -> 171 us (0.53)
  the two profiles are of different devices: /device:TPU:1 before, /device:TPU:6 now
where the time goes in v1:
time: 171 us; the launch traced here: 169 us
  Pallas kernels  87.5 us (51%)
  starting transfers between devices  38.4 us (22%)
  waiting for transfers between devices  27.8 us (16%)
  local copies, waits for them, and re-layouts  9.85 us (6%)
  other arithmetic  4.99 us (3%)
    pallas_call x3, Pallas kernels, project_whole(): pl.pallas_call(functools.partial(whole_kernel, slots, len(aliased)), grid...  31.8 us
    ppermute x15, waiting for transfers between devices, permuted(): return lax.ppermute(value, 'tp', perm)  27.8 us
    pallas_call x4, Pallas kernels, merge(): pl.pallas_call(functools.partial(merge_kernel, group), grid=(4,), in_spec...  24.5 us
    ppermute x15, starting transfers between devices, permuted(): return lax.ppermute(value, 'tp', perm)  19.9 us
    pallas_call x1, Pallas kernels, filter_rows(): pl.pallas_call(filter_kernel, grid_spec=pltpu.PrefetchScalarGridSpec(num_...  13.7 us
    pallas_call x1, Pallas kernels, last_rest(): pl.pallas_call(last_rest_kernel, grid_spec=pltpu.PrefetchScalarGridSpec(n...  8.84 us
    all_to_all x1, starting transfers between devices, arriving_states(): packs = lax.all_to_all(pack, 'sp', split_axis=0, concat_axis=0, tiled=True)  8.56 us
    all_to_all x1, starting transfers between devices, arriving_states(): lax.all_to_all(arriving, 'sp', split_axis=0, concat_axis=0, tiled=True)  8.02 us
  transfers between devices with their start and end apart: 18, of which 6 were waited for; matrix products, arithmetic and copies ran while one was open for 4% of the time, Pallas kernels for 44%

profile of v1, /device:TPU:6, one launch (start us, length us, event | category | flops | bytes accessed | tf_op | source)
XLA Modules:
  0.0 169.5 jit_solution(13177856654035275740)
XLA Ops:
  0.0 1.3 fusion.1
  1.3 0.9 collective-permute-start.2
  2.2 2.4 %collective-permute-start.4 = (bf16[128,2048]{1,0:T(8,128)(2,1)S(1)}, bf16[128,2048]{1,0:T(8,128)(2,1)S(1)}, u32[]{:S(2)}, u32[]{:S(2)}) collective-permute-start(bf16[128,2048]{1,0:T(8,128)(2,1)S(1)} %get-tuple-element.77.refs_1_), channel_id=1, source_target_pairs={{0,1},{1,2},{2,3},{3,0},{4,5},{5,6},{6,7},{7,4},{8,9},{9,10},{10,1... | collective-permute-start | bytes 1572872 | tf_op jit(solution)/shard_map/ppermute | solution.py:490
  4.6 2.0 %collective-permute-start.5 = (bf16[128,2048]{1,0:T(8,128)(2,1)S(1)}, bf16[128,2048]{1,0:T(8,128)(2,1)S(1)}, u32[]{:S(2)}, u32[]{:S(2)}) collective-permute-start(bf16[128,2048]{1,0:T(8,128)(2,1)S(1)} %get-tuple-element.78.refs_0_), channel_id=1, source_target_pairs={{0,3},{1,0},{2,1},{3,2},{4,7},{5,4},{6,5},{7,6},{8,11},{9,8},{10,9... | collective-permute-start | bytes 1572872 | tf_op jit(solution)/shard_map/ppermute | solution.py:490
  6.6 1.1 copy.41.refs_4_.refs_5_.shift_a.shift_b
  7.7 1.3 constant_dynamic-slice_fusion.1
  9.0 10.6 %shard_map.154 = (f32[1024,512]{1,0:T(8,128)}, bf16[1024,512]{1,0:T(8,128)(2,1)}, bf16[1024,512]{1,0:T(8,128)(2,1)}, bf16[1024,512]{1,0:T(8,128)(2,1)}, f32[8,4,...) custom-call(s32[16]{0:T(128)} %get-tuple-element.80.place.table, bf16[128,2048]{1,0:T(8,128)(2,1)} %copy-done.8, ...), custom_call_target="tpu_custom_call" | custom-call | flops 4831838208 | bytes 16777216 | tf_op jit(solution)/shard_map/pallas_call | solution.py:169
  19.6 0.6 slice.12
  20.9 6.0 %collective-permute-done.refs_0_ = bf16[128,2048]{1,0:T(8,128)(2,1)S(1)} collective-permute-done((bf16[128,2048]{1,0:T(8,128)(2,1)S(1)}, bf16[128,2048]{1,0:T(8,128)(2,1)S(1)}, u32[]{:S(2)}, u32[]{:S(2)}) %collective-permute-start) | collective-permute-done | bytes 524320 | tf_op jit(solution)/shard_map/ppermute | solution.py:490
  26.8 3.6 %collective-permute-start.1 = (bf16[128,2048]{1,0:T(8,128)(2,1)S(1)}, bf16[128,2048]{1,0:T(8,128)(2,1)S(1)}, u32[]{:S(2)}, u32[]{:S(2)}) collective-permute-start(bf16[128,2048]{1,0:T(8,128)(2,1)S(1)} %collective-permute-done.refs_0_), channel_id=1, source_target_pairs={{0,1},{1,2},{2,3},{3,0},{4,5},{5,6},{6,7},{7,4},{8,9},{9,10},{10,1... | collective-permute-start | bytes 1572872 | tf_op jit(solution)/shard_map/ppermute | solution.py:490
  30.5 0.8 copy-done.2
  31.3 10.6 %shard_map.155 = (f32[1024,512]{1,0:T(8,128)}, bf16[1024,512]{1,0:T(8,128)(2,1)}, bf16[1024,512]{1,0:T(8,128)(2,1)}, bf16[1024,512]{1,0:T(8,128)(2,1)}, f32[8,4,...) custom-call(s32[16]{0:T(128)} %get-tuple-element.80.place.table, ...), custom_call_target="tpu_custom_call", output_to_operand_aliasing={{0}: (13, {}), {1}: (14, {}), {2}: (15, {}), {3}: (16, {}),... | custom-call | flops 4831838208 | bytes 16777216 | tf_op jit(solution)/shard_map/pallas_call | solution.py:169
  41.9 0.8 copy-done.4
  42.7 0.2 copy-done.5
  42.9 10.6 %shard_map.156 = (f32[1024,512]{1,0:T(8,128)}, bf16[1024,512]{1,0:T(8,128)(2,1)}, bf16[1024,512]{1,0:T(8,128)(2,1)}, bf16[1024,512]{1,0:T(8,128)(2,1)}, f32[8,4,...) custom-call(s32[16]{0:T(128)} %get-tuple-element.80.place.table, ...), custom_call_target="tpu_custom_call", output_to_operand_aliasing={{0}: (13, {}), {1}: (14, {}), {2}: (15, {}), {3}: (16, {}),... | custom-call | flops 4831838208 | bytes 16777216 | tf_op jit(solution)/shard_map/pallas_call | solution.py:169
  53.5 0.8 copy-done.6
  54.3 0.2 copy-done.7
  54.6 7.1 %last_states.1 = (bf16[256,1024]{1,0:T(8,128)(2,1)}, bf16[32,32,128]{2,1,0:T(8,128)(2,1)}, bf16[8,4,128,128]{3,2,1,0:T(8,128)(2,1)}, f32[8,8,512]{2,1,0:T(8,128)}) custom-call(s32[16]{0:T(128)} %get-tuple-element.80.place.table, bf16[128,2048]{1,0:T(8,128)(2,1)} %copy-done.6, bf16[128,2048]{1,0:T(8,128)(2,1)} %copy-done.7, f32[1,2048]{1,0:T(1,128)} %bitcast.16, ...), custom_call_target="tpu_custom_call" | custom-call | flops 3221225472 | bytes 10485760 | tf_op jit(solution)/shard_map/last_states/pallas_call | solution.py:252
  61.6 8.6 %all-to-all-start = ((bf16[32,32,128]{2,1,0:T(8,128)(2,1)}), bf16[32,32,128]{2,1,0:T(8,128)(2,1)S(1)}, u32[]{:S(2)}, u32[]{:S(2)}) async-start(bf16[32,32,128]{2,1,0:T(8,128)(2,1)} %get-tuple-element.65), calls=%async_computation | async-start | bytes 524288 | tf_op jit(solution)/shard_map/all_to_all | solution.py:354
  70.2 8.8 %last_rest.1 = (f32[1024,512]{1,0:T(8,128)}, bf16[1024,512]{1,0:T(8,128)(2,1)}, bf16[1024,512]{1,0:T(8,128)(2,1)}, bf16[1024,512]{1,0:T(8,128)(2,1)}) custom-call(s32[16]{0:T(128)} %get-tuple-element.80.place.table, bf16[128,2048]{1,0:T(8,128)(2,1)} %copy-done.6, ...), custom_call_target="tpu_custom_call", output_to_operand_aliasing={{0}: (12, {}), {1}: (13, {}), {2}: (14, {}), {3}: (15, {})} | custom-call | flops 3221225472 | bytes 12582912 | tf_op jit(solution)/shard_map/last_rest/pallas_call | solution.py:315
  79.0 0.8 constant_dynamic-slice_fusion
  79.8 1.9 %collective-permute-start.6 = (bf16[32,512]{1,0:T(8,128)(2,1)S(1)}, bf16[32,512]{1,0:T(8,128)(2,1)S(1)}, u32[]{:S(2)}, u32[]{:S(2)}) collective-permute-start(bf16[32,512]{1,0:T(8,128)(2,1)S(1)} %constant_dynamic-slice_fusion), channel_id=1, source_target_pairs={{0,4},{4,8},{8,12},{12,16},{16,20},{20,24},{24,28},{28,32},{32,36}... | collective-permute-start | bytes 98312 | tf_op jit(solution)/shard_map/ppermute | solution.py:537
  81.8 0.7 copy-done.1
  82.5 1.7 prefix.1
  84.2 8.0 %all-to-all-start.1 = ((bf16[32,16,128]{2,1,0:T(8,128)(2,1)}), bf16[32,16,128]{2,1,0:T(8,128)(2,1)S(1)}, u32[]{:S(2)}, u32[]{:S(2)}) async-start(bf16[32,16,128]{2,1,0:T(8,128)(2,1)} %prefix.1), calls=%async_computation.1 | async-start | bytes 262144 | tf_op jit(solution)/shard_map/all_to_all | solution.py:362
  92.2 0.6 copy-done.16
  92.8 13.7 %filter_rows.1 = (f32[1024,512]{1,0:T(8,128)}, f32[8,1024]{1,0:T(8,128)}) custom-call(s32[16]{0:T(128)} %get-tuple-element.80.place.table, bf16[1024,512]{1,0:T(8,128)(2,1)} %get-tuple-element.66.mixed, bf16[32,512]{1,0:T(8,128)(2,1)} %copy-done.16, f32[31,512]{1,0:T(8,128)} %taps.1), custom_call_target="tpu_custom_call" | custom-call | flops 7000000000 | bytes 5242880 | tf_op jit(solution)/shard_map/filter_rows/pallas_call | solution.py:403
  106.5 2.4 %collective-permute-start.7 = (f32[8,1024]{1,0:T(8,128)}, f32[8,1024]{1,0:T(8,128)S(1)}, u32[]{:S(2)}, u32[]{:S(2)}) collective-permute-start(f32[8,1024]{1,0:T(8,128)} %get-tuple-element.68.s0), channel_id=1, source_target_pairs={{0,1},{1,2},{2,3},{3,0},{4,5},{5,6},{6,7},{7,4},{8,9},{9,10},{10,1... | collective-permute-start | bytes 98312 | tf_op jit(solution)/shard_map/ppermute | solution.py:490
  108.9 0.9 collective-permute-start.9
  109.8 1.0 collective-permute-done.7.s1
  110.8 3.7 %collective-permute-done.8.s2 = f32[8,1024]{1,0:T(8,128)S(1)} collective-permute-done((f32[8,1024]{1,0:T(8,128)}, f32[8,1024]{1,0:T(8,128)S(1)}, u32[]{:S(2)}, u32[]{:S(2)}) %collective-permute-start.8) | collective-permute-done | bytes 32800 | tf_op jit(solution)/shard_map/ppermute | solution.py:490
  114.6 0.5 copy-done.12
  115.3 6.1 %shard_map.160 = (bf16[128,2048]{1,0:T(8,128)(2,1)}, bf16[128,2048]{1,0:T(8,128)(2,1)}) custom-call(s32[16]{0:T(128)} %get-tuple-element.80.place.table, f32[1024,512]{1,0:T(8,128)} %get-tuple-element.60.near, bf16[1024,512]{1,0:T(8,128)(2,1)} %get-tuple-element.61.query_near, bf16[1024,512]{1,0:T(8,128)(2,1)} %get-tuple-element.62.rgate, ...), custom_call_target="tpu_custom_call" | custom-call | flops 3221225472 | bytes 7340032 | tf_op jit(solution)/shard_map/pallas_call | solution.py:459
  121.4 0.9 collective-permute-start.11
  122.3 6.1 %shard_map.158 = (bf16[128,2048]{1,0:T(8,128)(2,1)}, bf16[128,2048]{1,0:T(8,128)(2,1)}) custom-call(s32[16]{0:T(128)} %get-tuple-element.80.place.table, f32[1024,512]{1,0:T(8,128)} %get-tuple-element.60.near, bf16[1024,512]{1,0:T(8,128)(2,1)} %get-tuple-element.61.query_near, bf16[1024,512]{1,0:T(8,128)(2,1)} %get-tuple-element.62.rgate, ...), custom_call_target="tpu_custom_call" | custom-call | flops 3221225472 | bytes 7340032 | tf_op jit(solution)/shard_map/pallas_call | solution.py:459
  128.4 1.2 collective-permute-start.10
  129.7 2.1 %collective-permute-start.13 = (bf16[128,2048]{1,0:T(8,128)(2,1)}, bf16[128,2048]{1,0:T(8,128)(2,1)S(1)}, u32[]{:S(2)}, u32[]{:S(2)}) collective-permute-start(bf16[128,2048]{1,0:T(8,128)(2,1)} %get-tuple-element.74), channel_id=1, source_target_pairs={{0,1},{1,2},{2,3},{3,0},{4,5},{5,6},{6,7},{7,4},{8,9},{9,10},{10,1... | collective-permute-start | bytes 1572872 | tf_op jit(solution)/shard_map/ppermute | solution.py:490
  131.8 6.1 %shard_map.159 = (bf16[128,2048]{1,0:T(8,128)(2,1)}, bf16[128,2048]{1,0:T(8,128)(2,1)}) custom-call(s32[16]{0:T(128)} %get-tuple-element.80.place.table, f32[1024,512]{1,0:T(8,128)} %get-tuple-element.60.near, bf16[1024,512]{1,0:T(8,128)(2,1)} %get-tuple-element.61.query_near, bf16[1024,512]{1,0:T(8,128)(2,1)} %get-tuple-element.62.rgate, ...), custom_call_target="tpu_custom_call" | custom-call | flops 3221225472 | bytes 7340032 | tf_op jit(solution)/shard_map/pallas_call | solution.py:459
  137.9 1.2 add_convert_fusion.3
  139.0 3.3 %collective-permute-start.12 = (bf16[128,2048]{1,0:T(8,128)(2,1)S(1)}, bf16[128,2048]{1,0:T(8,128)(2,1)S(1)}, u32[]{:S(2)}, u32[]{:S(2)}) collective-permute-start(bf16[128,2048]{1,0:T(8,128)(2,1)S(1)} %add_convert_fusion.3), channel_id=1, source_target_pairs={{0,1},{1,2},{2,3},{3,0},{4,5},{5,6},{6,7},{7,4},{8,9},{9,10},{10,1... | collective-permute-start | bytes 1572872 | tf_op jit(solution)/shard_map/ppermute | solution.py:490
  142.3 11.5 %collective-permute-done.14 = bf16[128,2048]{1,0:T(8,128)(2,1)S(1)} collective-permute-done((bf16[128,2048]{1,0:T(8,128)(2,1)S(1)}, bf16[128,2048]{1,0:T(8,128)(2,1)S(1)}, u32[]{:S(2)}, u32[]{:S(2)}) %collective-permute-start.14) | collective-permute-done | bytes 524320 | tf_op jit(solution)/shard_map/ppermute | solution.py:490
  153.9 1.2 add_convert_fusion.1
  155.0 0.1 collective-permute-start.15
  155.1 6.2 %shard_map.157 = (bf16[128,2048]{1,0:T(8,128)(2,1)}, bf16[128,2048]{1,0:T(8,128)(2,1)}) custom-call(s32[16]{0:T(128)} %get-tuple-element.80.place.table, f32[1024,512]{1,0:T(8,128)} %get-tuple-element.60.near, bf16[1024,512]{1,0:T(8,128)(2,1)} %get-tuple-element.61.query_near, bf16[1024,512]{1,0:T(8,128)(2,1)} %get-tuple-element.62.rgate, ...), custom_call_target="tpu_custom_call" | custom-call | flops 3221225472 | bytes 7340032 | tf_op jit(solution)/shard_map/pallas_call | solution.py:459
  161.3 1.3 add_convert_fusion.2
  162.7 5.5 %collective-permute-done.15 = bf16[128,2048]{1,0:T(8,128)(2,1)S(1)} collective-permute-done((bf16[128,2048]{1,0:T(8,128)(2,1)S(1)}, bf16[128,2048]{1,0:T(8,128)(2,1)S(1)}, u32[]{:S(2)}, u32[]{:S(2)}) %collective-permute-start.15) | collective-permute-done | bytes 524320 | tf_op jit(solution)/shard_map/ppermute | solution.py:490
  168.1 0.2 add_convert_fusion
  168.4 1.1 pad_maximum_fusion
  (43 shorter events, 0.3 us)
Async XLA Ops:
  0.0 6.6 %copy-start.14 = (f32[1024,4]{0,1:T(4,128)S(1)}, f32[1024,4]{0,1:T(4,128)}, u32[]{:S(2)}) copy-start(f32[1024,4]{0,1:T(4,128)} %param.25) | copy-start | bytes 49156
  1.3 7.7 %copy-start.8 = (bf16[128,2048]{1,0:T(8,128)(2,1)}, bf16[128,2048]{1,0:T(8,128)(2,1)S(1)}, u32[]{:S(2)}) copy-start(bf16[128,2048]{1,0:T(8,128)(2,1)S(1)} %get-tuple-element.78.refs_0_) | copy-start | bytes 1572868
  1.3 7.7 %copy-start.9 = (bf16[128,2048]{1,0:T(8,128)(2,1)}, bf16[128,2048]{1,0:T(8,128)(2,1)S(1)}, u32[]{:S(2)}) copy-start(bf16[128,2048]{1,0:T(8,128)(2,1)S(1)} %get-tuple-element.77.refs_1_) | copy-start | bytes 1572868
  1.3 29.1 %collective-permute-start.2 = (bf16[128,2048]{1,0:T(8,128)(2,1)S(1)}, bf16[128,2048]{1,0:T(8,128)(2,1)S(1)}, u32[]{:S(2)}, u32[]{:S(2)}) collective-permute-start(bf16[128,2048]{1,0:T(8,128)(2,1)S(1)} %get-tuple-element.77.refs_1_), channel_id=1, source_target_pairs={{0,3},{1,0},{2,1},{3,2},{4,7},{5,4},{6,5},{7,6},{8,11},{9,8},{10,9... | collective-permute-start | bytes 1572872 | tf_op jit(solution)/shard_map/ppermute | solution.py:490
  2.2 39.7 %collective-permute-start.4 = (bf16[128,2048]{1,0:T(8,128)(2,1)S(1)}, bf16[128,2048]{1,0:T(8,128)(2,1)S(1)}, u32[]{:S(2)}, u32[]{:S(2)}) collective-permute-start(bf16[128,2048]{1,0:T(8,128)(2,1)S(1)} %get-tuple-element.77.refs_1_), channel_id=1, source_target_pairs={{0,1},{1,2},{2,3},{3,0},{4,5},{5,6},{6,7},{7,4},{8,9},{9,10},{10,1... | collective-permute-start | bytes 1572872 | tf_op jit(solution)/shard_map/ppermute | solution.py:490
  4.6 22.2 %collective-permute-start = (bf16[128,2048]{1,0:T(8,128)(2,1)S(1)}, bf16[128,2048]{1,0:T(8,128)(2,1)S(1)}, u32[]{:S(2)}, u32[]{:S(2)}) collective-permute-start(bf16[128,2048]{1,0:T(8,128)(2,1)S(1)} %get-tuple-element.78.refs_0_), channel_id=1, source_target_pairs={{0,1},{1,2},{2,3},{3,0},{4,5},{5,6},{6,7},{7,4},{8,9},{9,10},{10,1... | collective-permute-start | bytes 1572872 | tf_op jit(solution)/shard_map/ppermute | solution.py:490
  4.6 37.3 %collective-permute-start.5 = (bf16[128,2048]{1,0:T(8,128)(2,1)S(1)}, bf16[128,2048]{1,0:T(8,128)(2,1)S(1)}, u32[]{:S(2)}, u32[]{:S(2)}) collective-permute-start(bf16[128,2048]{1,0:T(8,128)(2,1)S(1)} %get-tuple-element.78.refs_0_), channel_id=1, source_target_pairs={{0,3},{1,0},{2,1},{3,2},{4,7},{5,4},{6,5},{7,6},{8,11},{9,8},{10,9... | collective-permute-start | bytes 1572872 | tf_op jit(solution)/shard_map/ppermute | solution.py:490
  26.8 3.6 %copy-start.3 = (bf16[128,2048]{1,0:T(8,128)(2,1)}, bf16[128,2048]{1,0:T(8,128)(2,1)S(1)}, u32[]{:S(2)}) copy-start(bf16[128,2048]{1,0:T(8,128)(2,1)S(1)} %collective-permute-done.refs_0_) | copy-start | bytes 1572868
  26.8 26.7 %collective-permute-start.1 = (bf16[128,2048]{1,0:T(8,128)(2,1)S(1)}, bf16[128,2048]{1,0:T(8,128)(2,1)S(1)}, u32[]{:S(2)}, u32[]{:S(2)}) collective-permute-start(bf16[128,2048]{1,0:T(8,128)(2,1)S(1)} %collective-permute-done.refs_0_), channel_id=1, source_target_pairs={{0,1},{1,2},{2,3},{3,0},{4,5},{5,6},{6,7},{7,4},{8,9},{9,10},{10,1... | collective-permute-start | bytes 1572872 | tf_op jit(solution)/shard_map/ppermute | solution.py:490
  30.4 0.8 copy-start.2
  30.4 23.1 %collective-permute-start.3 = (bf16[128,2048]{1,0:T(8,128)(2,1)S(1)}, bf16[128,2048]{1,0:T(8,128)(2,1)S(1)}, u32[]{:S(2)}, u32[]{:S(2)}) collective-permute-start(bf16[128,2048]{1,0:T(8,128)(2,1)S(1)} %collective-permute-done.2.refs_1_), channel_id=1, source_target_pairs={{0,3},{1,0},{2,1},{3,2},{4,7},{5,4},{6,5},{7,6},{8,11},{9,8},{10,9... | collective-permute-start | bytes 1572872 | tf_op jit(solution)/shard_map/ppermute | solution.py:490
  41.9 0.8 copy-start.4
  41.9 1.0 copy-start.5
  53.5 0.8 copy-start.6
  53.5 1.0 copy-start.7
  61.6 20.1 %all-to-all-start = ((bf16[32,32,128]{2,1,0:T(8,128)(2,1)}), bf16[32,32,128]{2,1,0:T(8,128)(2,1)S(1)}, u32[]{:S(2)}, u32[]{:S(2)}) async-start(bf16[32,32,128]{2,1,0:T(8,128)(2,1)} %get-tuple-element.65), calls=%async_computation | async-start | bytes 524288 | tf_op jit(solution)/shard_map/all_to_all | solution.py:354
  79.8 12.4 %collective-permute-start.6 = (bf16[32,512]{1,0:T(8,128)(2,1)S(1)}, bf16[32,512]{1,0:T(8,128)(2,1)S(1)}, u32[]{:S(2)}, u32[]{:S(2)}) collective-permute-start(bf16[32,512]{1,0:T(8,128)(2,1)S(1)} %constant_dynamic-slice_fusion), channel_id=1, source_target_pairs={{0,4},{4,8},{8,12},{12,16},{16,20},{20,24},{24,28},{28,32},{32,36}... | collective-permute-start | bytes 98312 | tf_op jit(solution)/shard_map/ppermute | solution.py:537
  81.8 0.7 copy-start.1
  84.2 30.4 %all-to-all-start.1 = ((bf16[32,16,128]{2,1,0:T(8,128)(2,1)}), bf16[32,16,128]{2,1,0:T(8,128)(2,1)S(1)}, u32[]{:S(2)}, u32[]{:S(2)}) async-start(bf16[32,16,128]{2,1,0:T(8,128)(2,1)} %prefix.1), calls=%async_computation.1 | async-start | bytes 262144 | tf_op jit(solution)/shard_map/all_to_all | solution.py:362
  92.2 0.6 copy-start.16
  106.5 4.3 %collective-permute-start.7 = (f32[8,1024]{1,0:T(8,128)}, f32[8,1024]{1,0:T(8,128)S(1)}, u32[]{:S(2)}, u32[]{:S(2)}) collective-permute-start(f32[8,1024]{1,0:T(8,128)} %get-tuple-element.68.s0), channel_id=1, source_target_pairs={{0,1},{1,2},{2,3},{3,0},{4,5},{5,6},{6,7},{7,4},{8,9},{9,10},{10,1... | collective-permute-start | bytes 98312 | tf_op jit(solution)/shard_map/ppermute | solution.py:490
  108.9 5.6 %collective-permute-start.8 = (f32[8,1024]{1,0:T(8,128)}, f32[8,1024]{1,0:T(8,128)S(1)}, u32[]{:S(2)}, u32[]{:S(2)}) collective-permute-start(f32[8,1024]{1,0:T(8,128)} %get-tuple-element.68.s0), channel_id=1, source_target_pairs={{0,2},{1,3},{2,0},{3,1},{4,6},{5,7},{6,4},{7,5},{8,10},{9,11},{10,... | collective-permute-start | bytes 98312 | tf_op jit(solution)/shard_map/ppermute | solution.py:490
  108.9 5.7 %collective-permute-start.9 = (f32[8,1024]{1,0:T(8,128)}, f32[8,1024]{1,0:T(8,128)S(1)}, u32[]{:S(2)}, u32[]{:S(2)}) collective-permute-start(f32[8,1024]{1,0:T(8,128)} %get-tuple-element.68.s0), channel_id=1, source_target_pairs={{0,3},{1,0},{2,1},{3,2},{4,7},{5,4},{6,5},{7,6},{8,11},{9,8},{10,9... | collective-permute-start | bytes 98312 | tf_op jit(solution)/shard_map/ppermute | solution.py:490
  110.8 3.8 %copy-start.11 = (f32[8,1024]{1,0:T(8,128)}, f32[8,1024]{1,0:T(8,128)S(1)}, u32[]{:S(2)}) copy-start(f32[8,1024]{1,0:T(8,128)S(1)} %collective-permute-done.7.s1) | copy-start | bytes 98308
  114.5 0.6 copy-start.12
  114.6 0.6 copy-start.13
  114.6 0.7 copy-start
  121.4 10.4 %copy-start.15 = (bf16[128,2048]{1,0:T(8,128)(2,1)S(1)}, bf16[128,2048]{1,0:T(8,128)(2,1)}, u32[]{:S(2)}) copy-start(bf16[128,2048]{1,0:T(8,128)(2,1)} %get-tuple-element.76) | copy-start | bytes 1572868
  121.4 16.5 %collective-permute-start.11 = (bf16[128,2048]{1,0:T(8,128)(2,1)}, bf16[128,2048]{1,0:T(8,128)(2,1)S(1)}, u32[]{:S(2)}, u32[]{:S(2)}) collective-permute-start(bf16[128,2048]{1,0:T(8,128)(2,1)} %get-tuple-element.72), channel_id=1, source_target_pairs={{0,1},{1,2},{2,3},{3,0},{4,5},{5,6},{6,7},{7,4},{8,9},{9,10},{10,1... | collective-permute-start | bytes 1572872 | tf_op jit(solution)/shard_map/ppermute | solution.py:490
  128.4 32.8 %collective-permute-start.10 = (bf16[128,2048]{1,0:T(8,128)(2,1)}, bf16[128,2048]{1,0:T(8,128)(2,1)S(1)}, u32[]{:S(2)}, u32[]{:S(2)}) collective-permute-start(bf16[128,2048]{1,0:T(8,128)(2,1)} %get-tuple-element.70), channel_id=1, source_target_pairs={{0,3},{1,0},{2,1},{3,2},{4,7},{5,4},{6,5},{7,6},{8,11},{9,8},{10,9... | collective-permute-start | bytes 1572872 | tf_op jit(solution)/shard_map/ppermute | solution.py:490
  129.7 33.0 %collective-permute-start.13 = (bf16[128,2048]{1,0:T(8,128)(2,1)}, bf16[128,2048]{1,0:T(8,128)(2,1)S(1)}, u32[]{:S(2)}, u32[]{:S(2)}) collective-permute-start(bf16[128,2048]{1,0:T(8,128)(2,1)} %get-tuple-element.74), channel_id=1, source_target_pairs={{0,1},{1,2},{2,3},{3,0},{4,5},{5,6},{6,7},{7,4},{8,9},{9,10},{10,1... | collective-permute-start | bytes 1572872 | tf_op jit(solution)/shard_map/ppermute | solution.py:490
  131.8 22.1 %collective-permute-start.14 = (bf16[128,2048]{1,0:T(8,128)(2,1)S(1)}, bf16[128,2048]{1,0:T(8,128)(2,1)S(1)}, u32[]{:S(2)}, u32[]{:S(2)}) collective-permute-start(bf16[128,2048]{1,0:T(8,128)(2,1)S(1)} %copy-done.15), channel_id=1, source_target_pairs={{0,3},{1,0},{2,1},{3,2},{4,7},{5,4},{6,5},{7,6},{8,11},{9,8},{10,9... | collective-permute-start | bytes 1572872 | tf_op jit(solution)/shard_map/ppermute | solution.py:490
  139.0 22.3 %collective-permute-start.12 = (bf16[128,2048]{1,0:T(8,128)(2,1)S(1)}, bf16[128,2048]{1,0:T(8,128)(2,1)S(1)}, u32[]{:S(2)}, u32[]{:S(2)}) collective-permute-start(bf16[128,2048]{1,0:T(8,128)(2,1)S(1)} %add_convert_fusion.3), channel_id=1, source_target_pairs={{0,1},{1,2},{2,3},{3,0},{4,5},{5,6},{6,7},{7,4},{8,9},{9,10},{10,1... | collective-permute-start | bytes 1572872 | tf_op jit(solution)/shard_map/ppermute | solution.py:490
  155.0 13.1 %collective-permute-start.15 = (bf16[128,2048]{1,0:T(8,128)(2,1)S(1)}, bf16[128,2048]{1,0:T(8,128)(2,1)S(1)}, u32[]{:S(2)}, u32[]{:S(2)}) collective-permute-start(bf16[128,2048]{1,0:T(8,128)(2,1)S(1)} %add_convert_fusion.1), channel_id=1, source_target_pairs={{0,3},{1,0},{2,1},{3,2},{4,7},{5,4},{6,5},{7,6},{8,11},{9,8},{10,9... | collective-permute-start | bytes 1572872 | tf_op jit(solution)/shard_map/ppermute | solution.py:490
  161.3 6.9 %copy-start.10 = (bf16[128,2048]{1,0:T(8,128)(2,1)S(1)}, bf16[128,2048]{1,0:T(8,128)(2,1)}, u32[]{:S(2)}) copy-start(bf16[128,2048]{1,0:T(8,128)(2,1)} %get-tuple-element.73) | copy-start | bytes 1572868

commit v2 on v1

v2 whole, which is shorter than its diff:
```python
import functools

import jax
import jax.numpy as jnp
import numpy as np
from jax import lax
from jax.experimental import pallas as pl
from jax.experimental.pallas import tpu as pltpu
from jax.sharding import PartitionSpec as P


HEAD = 128
BLK = 128
NORM_EPS = 1e-05
HEAD_EPS = 1e-06
F32 = jnp.float32
BF16 = jnp.bfloat16


SLOT = np.array([[0, 1], [5, 3], [6, 7], [2, 4]])
SLOT_TABLE = np.array(
    [[SLOT[(p // 2 - t) % 4][p % 2] for p in range(8)] for t in range(4)], dtype=np.int32
)
PLACE_TABLE = np.argsort(SLOT_TABLE, axis=1).astype(np.int32)


def params(**kw):
    return pltpu.CompilerParams(vmem_limit_bytes=58 * 1024 * 1024, **kw)


def dot(a, b, dims=((1,), (0,))):
    return lax.dot_general(a, b, (dims, ((), ())), preferred_element_type=F32)


def silu(x):
    return x * jax.nn.sigmoid(x)


WIDE = 4 * HEAD


def gates(forget, gap, shift):
    key = gap * jax.nn.sigmoid(-forget.astype(F32))
    spread = jnp.concatenate(
        [jnp.broadcast_to(shift[:, h : h + 1], (BLK, HEAD)) for h in range(4)], axis=1
    )
    log_forget = jnp.log1p(-key) + spread
    high = log_forget.astype(BF16)
    low = (log_forget - high.astype(F32)).astype(BF16)
    rows = lax.broadcasted_iota(jnp.int32, (BLK, BLK), 0)
    cols = lax.broadcasted_iota(jnp.int32, (BLK, BLK), 1)
    lower = (rows >= cols).astype(F32).astype(BF16)
    return key, dot(lower, high) + dot(lower, low)


def pieces(log_row):
    high = log_row.astype(BF16).astype(F32)
    mid = (log_row - high).astype(BF16).astype(F32)
    low = log_row - high - mid
    row = lax.broadcasted_iota(jnp.int32, (16, HEAD), 0)
    tile = jnp.where(row == 0, high, jnp.where(row == 1, mid, jnp.where(row == 2, low, 0.0)))
    return tile.astype(BF16)


def block_outputs(key, run, value, query, near, query_near, at):
    middle = run[BLK // 2 - 1 : BLK // 2, :]
    query_mid = silu(query.astype(F32)) * jnp.exp(run - middle)
    key_mid = (key * jnp.exp(middle - run)).astype(BF16)
    query_near[at, :] = (query_mid * jnp.exp(middle)).astype(BF16)
    query_mid = query_mid.astype(BF16)
    rows = lax.broadcasted_iota(jnp.int32, (BLK, BLK), 0)
    cols = lax.broadcasted_iota(jnp.int32, (BLK, BLK), 1)
    for h in range(4):
        lanes = slice(h * HEAD, (h + 1) * HEAD)
        scores = dot(query_mid[:, lanes], key_mid[:, lanes], ((1,), (1,)))
        scores = jnp.where(rows >= cols, scores, 0.0).astype(BF16)
        near[at, lanes] = dot(scores, value[:, lanes])


def fetch(pairs, sems):
    copies = [pltpu.make_async_copy(source, target, sems.at[k]) for k, (source, target) in enumerate(pairs)]
    for copy in copies:
        copy.start()
    return copies


def norm_kernel(tokens, gain, top, bottom):
    g = gain[...]
    for k, out in enumerate((top, bottom)):
        for r in range(0, BLK, 32):
            rows = tokens[k * BLK + r : k * BLK + r + 32, :].astype(F32)
            centred = rows - jnp.mean(rows, axis=-1, keepdims=True)
            var = jnp.mean(centred * centred, axis=-1, keepdims=True)
            out[r : r + 32, :] = (centred * lax.rsqrt(var + NORM_EPS) * g).astype(BF16)


def norm_rows(tokens, gain):
    half = jax.ShapeDtypeStruct((BLK, tokens.shape[1]), BF16)
    return pl.pallas_call(
        norm_kernel, out_shape=[half, half], compiler_params=params(), name="norm_rows"
    )(tokens, gain)


def glu(value, gate):
    return (value.astype(F32) * jax.nn.sigmoid(gate.astype(F32))).astype(BF16)


def keys_kernel(reuse, last, place, *refs):
    x_top, x_bottom, gap, shift_top, shift_bottom = refs[:5]
    weights, refs = refs[5:9], refs[9:]
    if last:
        added, close_all, fv, mixed, pack, starts, offsets, xbuf, wbuf, parts, sems, more = refs[2:]
    else:
        fv, mixed, added, close, xbuf, wbuf, sems = refs[4 if reuse else 0 :]
    copies = fetch(
        [(x_top, xbuf.at[pl.ds(0, BLK)]), (x_bottom, xbuf.at[pl.ds(BLK, BLK)])]
        + [(w, wbuf.at[k]) for k, w in enumerate(weights)],
        sems,
    )
    if last:
        bring_parts = pltpu.make_async_copy(added.at[pl.ds(0, 6)], parts.at[pl.ds(0, 6)], more.at[0])
        bring_parts.start()
    copies[0].wait()
    copies[1].wait()

    def times(n):
        copies[2 + n].wait()
        return dot(xbuf[...], wbuf[n]).astype(BF16)

    fv[:, 0:WIDE] = times(0)
    fv[:, WIDE : 2 * WIDE] = times(1)
    ends = []
    for k, shift in enumerate((shift_top, shift_bottom)):
        at = slice(k * BLK, (k + 1) * BLK)
        key, run = gates(fv[at, 0:WIDE], gap[...], shift[...])
        value = fv[at, WIDE : 2 * WIDE]
        end = run[BLK - 1 : BLK, :]
        key_far = (key * jnp.exp(end - run)).astype(BF16)
        ends.append(end)
        if not last:
            close[k] = jnp.broadcast_to(end, (8, WIDE))
        for h in range(4):
            lanes = slice(h * HEAD, (h + 1) * HEAD)
            sum_h = dot(value[:, lanes], key_far[:, lanes], ((0,), (0,)))
            if last:
                parts[6 + k, h] = sum_h
            else:
                added[k, h] = sum_h
    mixed[...] = glu(times(2), times(3))
    if last:
        bring_parts.wait()
        scan_blocks(place, ends, close_all, parts, pack, starts, offsets)


def scan_blocks(place, ends, close_all, parts, pack, starts, offsets):
    state = [jnp.zeros((HEAD, HEAD), F32) for _ in range(4)]
    total = jnp.zeros((1, WIDE), F32)
    for i in range(8):
        slot = place[8 + i]
        offsets[slot] = jnp.broadcast_to(total, (8, WIDE))
        end = jnp.where(
            slot == 6, ends[0], jnp.where(slot == 7, ends[1], close_all[jnp.minimum(slot, 5)][0:1, :])
        )
        keep = jnp.exp(end)
        for h in range(4):
            lanes = slice(h * HEAD, (h + 1) * HEAD)
            starts[slot, h] = state[h].astype(BF16)
            state[h] = state[h] * keep[:, lanes] + parts[slot, h]
        total = total + end
    for h in range(4):
        tile = pieces(total[:, h * HEAD : (h + 1) * HEAD])
        rows = state[h].astype(BF16)
        for j in range(8):
            pack[8 * h + j, 0:16, :] = rows[16 * j : 16 * j + 16, :]
            pack[8 * h + j, 16:32, :] = tile


def any_spec():
    return pl.BlockSpec(memory_space=pl.ANY)


def keys(group, x, place, gap, shift, weights, bufs):
    depth = x[0].shape[1]
    rows = 2 * BLK
    last = group == 3
    block = lambda *shape: pl.BlockSpec(shape, lambda i, p: (group,) + (0,) * (len(shape) - 1))
    whole = lambda *shape: pl.BlockSpec(shape, lambda i, p: (0,) * len(shape))
    array = jax.ShapeDtypeStruct
    out_specs = [block(rows, 2 * WIDE), block(rows, WIDE)]
    out_shape = [array((8 * BLK, 2 * WIDE), BF16), array((8 * BLK, WIDE), BF16)]
    scratch = [pltpu.VMEM((rows, depth), BF16), pltpu.VMEM((4, depth, WIDE), BF16)]
    if last:
        buf_specs = [any_spec()] * 3 + [whole(8, 8, WIDE)]
        out_specs += [whole(32, 32, HEAD), whole(8, 4, HEAD, HEAD), whole(8, 8, WIDE)]
        out_shape += [array((32, 32, HEAD), BF16), array((8, 4, HEAD, HEAD), BF16), array((8, 8, WIDE), F32)]
        scratch += [
            pltpu.VMEM((8, 4, HEAD, HEAD), F32),
            pltpu.SemaphoreType.DMA((6,)),
            pltpu.SemaphoreType.DMA((1,)),
        ]
    else:
        buf_specs = [any_spec()] * len(bufs)
        out_specs += [block(2, 4, HEAD, HEAD), block(2, 8, WIDE)]
        out_shape += [array((8, 4, HEAD, HEAD), F32), array((8, 8, WIDE), F32)]
        scratch += [pltpu.SemaphoreType.DMA((6,))]
    aliased = min(len(bufs), 2 if last else 4)
    return pl.pallas_call(
        functools.partial(keys_kernel, bool(bufs), last),
        grid_spec=pltpu.PrefetchScalarGridSpec(
            num_scalar_prefetch=1,
            grid=(1,),
            in_specs=[any_spec()] * 2
            + [whole(1, WIDE)]
            + [pl.BlockSpec((BLK, 4), lambda i, p, k=k: (p[2 * group + k], 0)) for k in range(2)]
            + [any_spec()] * 4
            + buf_specs,
            out_specs=out_specs,
            scratch_shapes=scratch,
        ),
        out_shape=out_shape,
        input_output_aliases={10 + k: k for k in range(aliased)},
        compiler_params=params(),
        cost_estimate=pl.CostEstimate(
            flops=2 * rows * depth * WIDE * 6, bytes_accessed=12 * 2**20, transcendentals=0
        ),
    )(place, *x, gap, shift, shift, *weights, *bufs)


def prefix_kernel(packs, arriving):
    state = jnp.zeros((16, HEAD), F32)
    for i in range(32):
        arriving[i] = state.astype(BF16)
        tile = packs[i, 16:32, :].astype(F32)
        log = tile[0:1] + tile[1:2] + tile[2:3]
        state = jnp.exp(log) * state + packs[i, 0:16, :].astype(F32)


def arriving_states(pack):
    packs = lax.all_to_all(pack, "sp", split_axis=0, concat_axis=0, tiled=True)
    arriving = pl.pallas_call(
        prefix_kernel,
        out_shape=jax.ShapeDtypeStruct((32, 16, HEAD), BF16),
        compiler_params=params(),
        cost_estimate=pl.CostEstimate(flops=10**8, bytes_accessed=2**20, transcendentals=0),
        name="prefix",
    )(packs)
    arrived = lax.all_to_all(arriving, "sp", split_axis=0, concat_axis=0, tiled=True)
    return arrived.reshape(4, HEAD, HEAD)


def filter_kernel(table, mixed, halo, taps, filtered, stats, window):
    i = pl.program_id(0)
    reach = 32

    @pl.when(i == 0)
    def _():
        window[0:reach, :] = halo[...].astype(F32)

    @pl.when(i > 0)
    def _():
        window[0:reach, :] = window[BLK : BLK + reach, :]

    window[reach : reach + BLK, :] = mixed[...].astype(F32)
    row_sum = jnp.zeros((BLK, HEAD), F32)
    row_square = jnp.zeros((BLK, HEAD), F32)
    for c in range(4):
        lanes = slice(c * HEAD, (c + 1) * HEAD)
        acc = jnp.zeros((BLK, HEAD), F32)
        for r in range(8):
            used = [q for q in range(5) if 0 <= 8 * q + r - 2 < 31]
            shifted = window[8 * used[0] + r : 8 * used[-1] + r + BLK, lanes]
            part = None
            for q in used:
                j, lead = 8 * q + r - 2, 8 * (q - used[0])
                term = taps[j : j + 1, lanes] * shifted[lead : lead + BLK, :]
                part = term if part is None else part + term
            acc = acc + part
        filtered[:, lanes] = acc
        row_sum = row_sum + acc
        row_square = row_square + acc * acc
    lane = lax.broadcasted_iota(jnp.int32, (BLK, HEAD), 1)
    tile = jnp.where(
        lane == 0,
        jnp.sum(row_sum, axis=1, keepdims=True),
        jnp.where(lane == 1, jnp.sum(row_square, axis=1, keepdims=True), 0.0),
    )
    stats[...] = jnp.transpose(tile)[0:8, :]


def filter_rows(place, mixed, halo, taps):
    return pl.pallas_call(
        filter_kernel,
        grid_spec=pltpu.PrefetchScalarGridSpec(
            num_scalar_prefetch=1,
            grid=(8,),
            in_specs=[
                pl.BlockSpec((BLK, WIDE), lambda i, p: (p[8 + i], 0)),
                pl.BlockSpec((32, WIDE), lambda i, p: (0, 0)),
                pl.BlockSpec((31, WIDE), lambda i, p: (0, 0)),
            ],
            out_specs=[
                pl.BlockSpec((BLK, WIDE), lambda i, p: (p[8 + i], 0)),
                pl.BlockSpec((8, BLK), lambda i, p: (0, i)),
            ],
            scratch_shapes=[pltpu.VMEM((32 + BLK, WIDE), F32)],
        ),
        out_shape=[
            jax.ShapeDtypeStruct((8 * BLK, WIDE), F32),
            jax.ShapeDtypeStruct((8, 8 * BLK), F32),
        ],
        compiler_params=params(),
        cost_estimate=pl.CostEstimate(flops=7 * 10**9, bytes_accessed=5 * 2**20, transcendentals=0),
        name="filter_rows",
    )(place, mixed, halo, taps)


def merge_kernel(group, place, x_top, x_bottom, fv, gap, shift_top, shift_bottom, starts, offsets, arrived, head_gain, filtered, s0, s1, s2, s3, conv_gain, w_query, w_rgate, w_rec, w_conv, top, bottom, xbuf, wbuf, obuf, query, rgate, near, query_near, act, sems):
    copies = fetch(
        [
            (x_top, xbuf.at[pl.ds(0, BLK)]),
            (x_bottom, xbuf.at[pl.ds(BLK, BLK)]),
            (w_query, wbuf.at[0]),
            (w_rgate, wbuf.at[1]),
            (w_rec, obuf.at[0]),
            (w_conv, obuf.at[1]),
        ],
        sems,
    )
    for k in range(3):
        copies[k].wait()
    query[...] = dot(xbuf[...], wbuf[0]).astype(BF16)
    copies[3].wait()
    rgate[...] = dot(xbuf[...], wbuf[1]).astype(BF16)
    for k, shift in enumerate((shift_top, shift_bottom)):
        rows = slice(k * BLK, (k + 1) * BLK)
        key, run = gates(fv[rows, 0:WIDE], gap[...], shift[...])
        block_outputs(key, run, fv[rows, WIDE : 2 * WIDE], query[rows, :], near, query_near, rows)
        carry = jnp.exp(offsets[k, 0:1, :])
        for h in range(4):
            lanes = slice(h * HEAD, (h + 1) * HEAD)
            state = starts[k, h].astype(F32) + carry[:, lanes] * arrived[h].astype(F32)
            rec = near[rows, lanes] + dot(query_near[rows, lanes], state.astype(BF16), ((1,), (1,)))
            rec = rec * lax.rsqrt(jnp.mean(rec * rec, axis=-1, keepdims=True) + HEAD_EPS)
            rec = rec * head_gain[...] * silu(rgate[rows, lanes].astype(F32))
            act[rows, lanes] = rec.astype(BF16)
        at = pl.ds(pl.multiple_of(place[2 * group + k] * BLK, BLK), BLK)
        stats = (s0[:, at] + s1[:, at]) + (s2[:, at] + s3[:, at])
        tile = jnp.transpose(jnp.concatenate([stats] * 16, axis=0))
        mean = tile[:, 0:1] / 2048.0
        scale = lax.rsqrt(tile[:, 1:2] / 2048.0 - mean * mean + NORM_EPS)
        normed = (filtered[rows, :] - mean) * scale * conv_gain[...]
        act[rows, WIDE : 2 * WIDE] = silu(normed).astype(BF16)
    copies[4].wait()
    copies[5].wait()
    for n in range(4):
        cols = slice(n * 512, (n + 1) * 512)
        part = dot(act[:, 0:WIDE], obuf[0, :, cols]) + dot(act[:, WIDE : 2 * WIDE], obuf[1, :, cols])
        top[:, cols] = part[0:BLK, :].astype(BF16)
        bottom[:, cols] = part[BLK : 2 * BLK, :].astype(BF16)


def merge(group, x, place, fv, gap, shift, starts, offsets, arrived, head_gain, filtered, stats, conv_gain, w_query, w_rgate, out_rec, out_conv):
    rows = 2 * BLK
    depth, width = w_query.shape[0], out_rec.shape[1]
    block = lambda *shape: pl.BlockSpec(shape, lambda i, p: (group,) + (0,) * (len(shape) - 1))
    whole = lambda *shape: pl.BlockSpec(shape, lambda i, p: (0,) * len(shape))
    return pl.pallas_call(
        functools.partial(merge_kernel, group),
        grid_spec=pltpu.PrefetchScalarGridSpec(
            num_scalar_prefetch=1,
            grid=(1,),
            in_specs=[any_spec()] * 2
            + [block(rows, 2 * WIDE), whole(1, WIDE)]
            + [pl.BlockSpec((BLK, 4), lambda i, p, k=k: (p[2 * group + k], 0)) for k in range(2)]
            + [block(2, 4, HEAD, HEAD), block(2, 8, WIDE), whole(4, HEAD, HEAD), whole(1, HEAD)]
            + [block(rows, WIDE)]
            + [whole(8, 8 * BLK)] * 4
            + [whole(1, WIDE)]
            + [any_spec()] * 4,
            out_specs=[whole(BLK, width), whole(BLK, width)],
            scratch_shapes=[
                pltpu.VMEM((rows, depth), BF16),
                pltpu.VMEM((2, depth, WIDE), BF16),
                pltpu.VMEM((2, WIDE, width), BF16),
                pltpu.VMEM((rows, WIDE), BF16),
                pltpu.VMEM((rows, WIDE), BF16),
                pltpu.VMEM((rows, WIDE), F32),
                pltpu.VMEM((rows, WIDE), BF16),
                pltpu.VMEM((rows, 2 * WIDE), BF16),
                pltpu.SemaphoreType.DMA((6,)),
            ],
        ),
        out_shape=[jax.ShapeDtypeStruct((BLK, width), BF16)] * 2,
        compiler_params=params(),
        cost_estimate=pl.CostEstimate(
            flops=2 * rows * 1024 * 2048 * 6, bytes_accessed=10 * 2**20, transcendentals=0
        ),
    )(place, *x, fv, gap, shift, shift, starts, offsets, arrived, head_gain, filtered, *stats, conv_gain, w_query, w_rgate, out_rec, out_conv)


def finish_kernel(own_a, got_a, sum_a, own_b, got_b, sum_b, out):
    for k, parts in enumerate(((own_a, got_a, sum_a), (own_b, got_b, sum_b))):
        total = sum(p[...].astype(F32) for p in parts[1:]) + parts[0][...].astype(F32)
        out[k * BLK : (k + 1) * BLK, :] = total.astype(BF16)


def finish(*parts):
    width = parts[0].shape[1]
    return pl.pallas_call(
        finish_kernel,
        grid=(4,),
        in_specs=[pl.BlockSpec((BLK, width // 4), lambda n: (0, n))] * 6,
        out_specs=pl.BlockSpec((2 * BLK, width // 4), lambda n: (0, n)),
        out_shape=jax.ShapeDtypeStruct((2 * BLK, width), BF16),
        compiler_params=params(),
        name="finish",
    )(*parts)


def permuted(value, perm):
    return lax.ppermute(value, "tp", perm)


def on_device(
    tokens,
    norm_gain,
    w_query,
    w_forget,
    w_value,
    w_rgate,
    w_glu_value,
    w_glu_gate,
    forget_gap,
    decay_shift,
    head_gain,
    conv_taps,
    conv_gain,
    out_rec,
    out_conv,
):
    ahead = [(i, (i + 1) % 4) for i in range(4)]
    behind = [(i, (i - 1) % 4) for i in range(4)]
    t = lax.axis_index("tp")
    place = lax.dynamic_index_in_dim(
        jnp.asarray(np.concatenate([PLACE_TABLE, SLOT_TABLE], axis=1)), t, 0, keepdims=False
    )

    gap = forget_gap[None, :]
    a, b = norm_rows(tokens, norm_gain[None, :])
    from_back_a = permuted(a, ahead)
    from_front_b = permuted(b, behind)
    from_back_b = permuted(b, ahead)
    from_front_a = permuted(a, behind)
    far_a = permuted(from_back_a, ahead)
    far_b = permuted(from_front_b, behind)
    slots = ((a, b), (from_back_a, from_front_b), (from_back_b, from_front_a), (far_a, far_b))

    bufs = ()
    for group in range(3):
        bufs = keys(group, slots[group], place, gap, decay_shift, (w_forget, w_value, w_glu_value, w_glu_gate), bufs)
    fv, mixed, pack, starts, offsets = keys(
        3, slots[3], place, gap, decay_shift, (w_forget, w_value, w_glu_value, w_glu_gate), bufs
    )

    edge = lax.dynamic_slice(mixed, (place[15] * BLK + BLK - 32, 0), (32, WIDE))
    halo = lax.ppermute(edge, "sp", [(i, i + 1) for i in range(31)])
    arrived = arriving_states(pack)
    filtered, stats = filter_rows(place, mixed, halo, conv_taps)
    stats_all = [stats] + [permuted(stats, [(i, (i + d) % 4) for i in range(4)]) for d in (1, 2, 3)]

    part = functools.partial(
        merge, place=place, fv=fv, gap=gap, shift=decay_shift, starts=starts, offsets=offsets, arrived=arrived,
        head_gain=head_gain[None, :], filtered=filtered, stats=stats_all, conv_gain=conv_gain[None, :],
        w_query=w_query, w_rgate=w_rgate, out_rec=out_rec, out_conv=out_conv,
    )
    add = lambda x, y: (x.astype(F32) + y.astype(F32)).astype(BF16)
    far_top, far_bottom = part(3, slots[3])
    via_back = permuted(far_top, ahead)
    via_front = permuted(far_bottom, behind)
    back_a, front_b = part(1, slots[1])
    got_b = permuted(front_b, ahead)
    got_a = permuted(back_a, behind)
    back_b, front_a = part(2, slots[2])
    sum_a = permuted(add(front_a, via_back), ahead)
    sum_b = permuted(add(back_b, via_front), behind)
    own_a, own_b = part(0, slots[0])
    return finish(own_a, got_a, sum_a, own_b, got_b, sum_b)


def solution(mesh):
    placed = (
        P(("sp", "tp"), None),
        P(),
        P(None, "tp"),
        P(None, "tp"),
        P(None, "tp"),
        P(None, "tp"),
        P(None, "tp"),
        P(None, "tp"),
        P("tp"),
        P("sp", "tp"),
        P(),
        P(None, "tp"),
        P("tp"),
        P("tp", None),
        P("tp", None),
    )
    return jax.shard_map(on_device, mesh=mesh, in_specs=placed, out_specs=P(("sp", "tp"), None), check_vma=False)
```

time: 171 us -> 150 us (0.88)
  the two profiles are of different devices: /device:TPU:6 before, /device:TPU:8 now
where the time goes in v2:
time: 150 us; the launch traced here: 149 us
  Pallas kernels  87.3 us (58%)
  starting transfers between devices  39.7 us (26%)
  waiting for transfers between devices  9.68 us (6%)
  local copies, waits for them, and re-layouts  9.15 us (6%)
  other arithmetic  2.33 us (2%)
    pallas_call x4, Pallas kernels, merge(): pl.pallas_call(functools.partial(merge_kernel, group), grid_spec=pltpu.Pr...  37.2 us
    pallas_call x4, Pallas kernels, keys(): pl.pallas_call(functools.partial(keys_kernel, bool(bufs), last), grid_spe...  32.1 us
    ppermute x15, starting transfers between devices, permuted(): return lax.ppermute(value, 'tp', perm)  24.1 us
    pallas_call x1, Pallas kernels, filter_rows(): pl.pallas_call(filter_kernel, grid_spec=pltpu.PrefetchScalarGridSpec(num_...  9.57 us
    all_to_all x1, starting transfers between devices, arriving_states(): packs = lax.all_to_all(pack, 'sp', split_axis=0, concat_axis=0, tiled=True)  8.56 us
    unnamed x33, local copies, waits for them, and re-layouts  6.55 us
    ppermute x15, waiting for transfers between devices, permuted(): return lax.ppermute(value, 'tp', perm)  6.04 us
    all_to_all x1, starting transfers between devices, arriving_states(): lax.all_to_all(arriving, 'sp', split_axis=0, concat_axis=0, tiled=True)  5.06 us
  transfers between devices with their start and end apart: 18, of which 6 were waited for; matrix products, arithmetic and copies ran while one was open for 4% of the time, Pallas kernels for 42%

profile of v2, /device:TPU:8, one launch (start us, length us, event | category | flops | bytes accessed | tf_op | source)
XLA Modules:
  0.0 149.1 jit_solution(10062206223258519003)
XLA Ops:
  0.0 2.8 %norm_rows.1 = (bf16[128,2048]{1,0:T(8,128)(2,1)}, bf16[128,2048]{1,0:T(8,128)(2,1)}) custom-call(bf16[256,2048]{1,0:T(8,128)(2,1)} %tokens.1, f32[1,2048]{1,0:T(1,128)} %bitcast.21), custom_call_target="tpu_custom_call" | custom-call | tf_op jit(solution)/shard_map/norm_rows/pallas_call | solution.py:99
  2.8 1.5 %collective-permute-start = (bf16[128,2048]{1,0:T(8,128)(2,1)}, bf16[128,2048]{1,0:T(8,128)(2,1)S(1)}, u32[]{:S(2)}, u32[]{:S(2)}) collective-permute-start(bf16[128,2048]{1,0:T(8,128)(2,1)} %get-tuple-element.34.refs_0_.x_top), channel_id=1, source_target_pairs={{0,1},{1,2},{2,3},{3,0},{4,5},{5,6},{6,7},{7,4},{8,9},{9,10},{10,1... | collective-permute-start | bytes 1572872 | tf_op jit(solution)/shard_map/ppermute | solution.py:421
  4.3 1.7 %collective-permute-start.2 = (bf16[128,2048]{1,0:T(8,128)(2,1)}, bf16[128,2048]{1,0:T(8,128)(2,1)S(1)}, u32[]{:S(2)}, u32[]{:S(2)}) collective-permute-start(bf16[128,2048]{1,0:T(8,128)(2,1)} %get-tuple-element.35.refs_1_.x_bottom), channel_id=1, source_target_pairs={{0,3},{1,0},{2,1},{3,2},{4,7},{5,4},{6,5},{7,6},{8,11},{9,8},{10,9... | collective-permute-start | bytes 1572872 | tf_op jit(solution)/shard_map/ppermute | solution.py:421
  6.0 0.3 collective-permute-start.4
  6.3 3.0 %collective-permute-start.5 = (bf16[128,2048]{1,0:T(8,128)(2,1)}, bf16[128,2048]{1,0:T(8,128)(2,1)S(1)}, u32[]{:S(2)}, u32[]{:S(2)}) collective-permute-start(bf16[128,2048]{1,0:T(8,128)(2,1)} %get-tuple-element.34.refs_0_.x_top), channel_id=1, source_target_pairs={{0,3},{1,0},{2,1},{3,2},{4,7},{5,4},{6,5},{7,6},{8,11},{9,8},{10,9... | collective-permute-start | bytes 1572872 | tf_op jit(solution)/shard_map/ppermute | solution.py:421
  9.3 1.7 %copy.33.refs_3_.refs_4_.shift_top.shift_bottom = f32[1024,4]{1,0:T(8,128)} copy(f32[1024,4]{0,1:T(4,128)} %param.25) | data formatting | bytes 32768 | tf_op args[9]
  11.0 1.3 constant_dynamic-slice_fusion.1
  12.3 7.8 %shard_map.154 = (bf16[1024,1024]{1,0:T(8,128)(2,1)}, bf16[1024,512]{1,0:T(8,128)(2,1)}, f32[8,4,128,128]{3,2,1,0:T(8,128)}, f32[8,8,512]{2,1,0:T(8,128)}) custom-call(s32[16]{0:T(128)} %get-tuple-element.64.place.table, bf16[128,2048]{1,0:T(8,128)(2,1)} %get-tuple-element.34.refs_0_.x_top, bf16[128,2048]{1,0:T(8,128)(2,1)} %get-tuple-element.35.refs_1_.x_bottom, ...), custom_call_target="tpu_custom_call" | custom-call | flops 3221225472 | bytes 12582912 | tf_op jit(solution)/shard_map/pallas_call | solution.py:207
  20.1 0.1 collective-permute-start.1
  20.2 3.2 %collective-permute-start.3 = (bf16[128,2048]{1,0:T(8,128)(2,1)S(1)}, bf16[128,2048]{1,0:T(8,128)(2,1)S(1)}, u32[]{:S(2)}, u32[]{:S(2)}) collective-permute-start(bf16[128,2048]{1,0:T(8,128)(2,1)S(1)} %collective-permute-done.2.refs_1_.x_bottom), channel_id=1, source_target_pairs={{0,3},{1,0},{2,1},{3,2},{4,7},{5,4},{6,5},{7,6},{8,11},{9,8},{10,9... | collective-permute-start | bytes 1572872 | tf_op jit(solution)/shard_map/ppermute | solution.py:421
  23.5 7.9 %shard_map.155 = (bf16[1024,1024]{1,0:T(8,128)(2,1)}, bf16[1024,512]{1,0:T(8,128)(2,1)}, f32[8,4,128,128]{3,2,1,0:T(8,128)}, f32[8,8,512]{2,1,0:T(8,128)}) custom-call(s32[16]{0:T(128)} %get-tuple-element.64.place.table, bf16[128,2048]{1,0:T(8,128)(2,1)} %copy-done.3, ...), custom_call_target="tpu_custom_call", output_to_operand_aliasing={{0}: (10, {}), {1}: (11, {}), {2}: (12, {}), {3}: (13, {})} | custom-call | flops 3221225472 | bytes 12582912 | tf_op jit(solution)/shard_map/pallas_call | solution.py:207
  31.4 0.8 copy-done.1
  32.2 0.2 copy-done.2
  32.4 7.8 %shard_map.156 = (bf16[1024,1024]{1,0:T(8,128)(2,1)}, bf16[1024,512]{1,0:T(8,128)(2,1)}, f32[8,4,128,128]{3,2,1,0:T(8,128)}, f32[8,8,512]{2,1,0:T(8,128)}) custom-call(s32[16]{0:T(128)} %get-tuple-element.64.place.table, bf16[128,2048]{1,0:T(8,128)(2,1)} %copy-done.1, ...), custom_call_target="tpu_custom_call", output_to_operand_aliasing={{0}: (10, {}), {1}: (11, {}), {2}: (12, {}), {3}: (13, {})} | custom-call | flops 3221225472 | bytes 12582912 | tf_op jit(solution)/shard_map/pallas_call | solution.py:207
  40.3 0.1 collective-permute-done.1.refs_0_.x_top
  40.4 0.8 copy-done.5
  41.2 0.2 copy-done.6
  41.3 8.5 %shard_map.157 = (bf16[1024,1024]{1,0:T(8,128)(2,1)}, bf16[1024,512]{1,0:T(8,128)(2,1)}, bf16[32,32,128]{2,1,0:T(8,128)(2,1)}, bf16[8,4,128,128]{3,2,1,0:T(8,128)(2,1)}, f32[8,8,512]{2,1,0:T(8,128)}) custom-call(s32[16]{0:T(128)} %get-tuple-element.64.place.table, bf16[128,2048]{1,0:T(8,128)(2,1)} %copy-done.5, ...), custom_call_target="tpu_custom_call", output_to_operand_aliasing={{0}: (10, {}), {1}: (11, {})} | custom-call | flops 3221225472 | bytes 12582912 | tf_op jit(solution)/shard_map/pallas_call | solution.py:207
  49.9 8.6 %all-to-all-start = ((bf16[32,32,128]{2,1,0:T(8,128)(2,1)}), bf16[32,32,128]{2,1,0:T(8,128)(2,1)S(1)}, u32[]{:S(2)}, u32[]{:S(2)}) async-start(bf16[32,32,128]{2,1,0:T(8,128)(2,1)} %get-tuple-element.51), calls=%async_computation | async-start | bytes 524288 | tf_op jit(solution)/shard_map/all_to_all | solution.py:239
  58.4 0.6 slice.4
  59.6 0.8 constant_dynamic-slice_fusion
  60.3 2.0 %collective-permute-start.6 = (bf16[32,512]{1,0:T(8,128)(2,1)S(1)}, bf16[32,512]{1,0:T(8,128)(2,1)S(1)}, u32[]{:S(2)}, u32[]{:S(2)}) collective-permute-start(bf16[32,512]{1,0:T(8,128)(2,1)S(1)} %constant_dynamic-slice_fusion), channel_id=1, source_target_pairs={{0,4},{4,8},{8,12},{12,16},{16,20},{20,24},{24,28},{28,32},{32,36}... | collective-permute-start | bytes 98312 | tf_op jit(solution)/shard_map/ppermute | solution.py:466
  62.4 3.6 %all-to-all-done.packs = bf16[32,32,128]{2,1,0:T(8,128)(2,1)S(1)} async-done(((bf16[32,32,128]{2,1,0:T(8,128)(2,1)}), bf16[32,32,128]{2,1,0:T(8,128)(2,1)S(1)}, u32[]{:S(2)}, u32[]{:S(2)}) %all-to-all-start) | async-done | bytes 262176 | tf_op jit(solution)/shard_map/all_to_all | solution.py:239
  66.0 0.7 copy-done
  66.7 1.7 %prefix.1 = bf16[32,16,128]{2,1,0:T(8,128)(2,1)} custom-call(bf16[32,32,128]{2,1,0:T(8,128)(2,1)} %copy-done), custom_call_target="tpu_custom_call" | custom-call | flops 100000000 | bytes 1048576 | tf_op jit(solution)/shard_map/prefix/pallas_call | solution.py:240
  68.4 5.1 %all-to-all-start.1 = ((bf16[32,16,128]{2,1,0:T(8,128)(2,1)}), bf16[32,16,128]{2,1,0:T(8,128)(2,1)S(1)}, u32[]{:S(2)}, u32[]{:S(2)}) async-start(bf16[32,16,128]{2,1,0:T(8,128)(2,1)} %prefix.1), calls=%async_computation.1 | async-start | bytes 262144 | tf_op jit(solution)/shard_map/all_to_all | solution.py:247
  73.5 0.6 copy-done.15
  74.1 9.6 %filter_rows.1 = (f32[1024,512]{1,0:T(8,128)}, f32[8,1024]{1,0:T(8,128)}) custom-call(s32[16]{0:T(128)} %get-tuple-element.64.place.table, bf16[1024,512]{1,0:T(8,128)(2,1)} %get-tuple-element.52.mixed, bf16[32,512]{1,0:T(8,128)(2,1)} %copy-done.15, f32[31,512]{1,0:T(8,128)} %taps.1), custom_call_target="tpu_custom_call" | custom-call | flops 7000000000 | bytes 5242880 | tf_op jit(solution)/shard_map/filter_rows/pallas_call | solution.py:291
  83.7 1.3 collective-permute-start.7
  85.0 2.9 %collective-permute-start.8 = (f32[8,1024]{1,0:T(8,128)}, f32[8,1024]{1,0:T(8,128)S(1)}, u32[]{:S(2)}, u32[]{:S(2)}) collective-permute-start(f32[8,1024]{1,0:T(8,128)} %get-tuple-element.54.s0), channel_id=1, source_target_pairs={{0,2},{1,3},{2,0},{3,1},{4,6},{5,7},{6,4},{7,5},{8,10},{9,11},{10,... | collective-permute-start | bytes 98312 | tf_op jit(solution)/shard_map/ppermute | solution.py:421
  87.9 0.9 collective-permute-start.9
  88.9 0.1 collective-permute-done.7.s1
  89.0 1.6 %collective-permute-done.8.s2 = f32[8,1024]{1,0:T(8,128)S(1)} collective-permute-done((f32[8,1024]{1,0:T(8,128)}, f32[8,1024]{1,0:T(8,128)S(1)}, u32[]{:S(2)}, u32[]{:S(2)}) %collective-permute-start.8) | collective-permute-done | bytes 32800 | tf_op jit(solution)/shard_map/ppermute | solution.py:421
  90.6 1.4 collective-permute-done.9.s3
  92.1 0.6 copy-done.14
  92.7 9.3 %shard_map.161 = (bf16[128,2048]{1,0:T(8,128)(2,1)}, bf16[128,2048]{1,0:T(8,128)(2,1)}) custom-call(s32[16]{0:T(128)} %get-tuple-element.64.place.table, bf16[128,2048]{1,0:T(8,128)(2,1)} %copy-done.5, bf16[128,2048]{1,0:T(8,128)(2,1)} %copy-done.6, bf16[1024,1024]{1,0:T(8,128)(2,1)} %get-tuple-element.48.fv, f32[1,512]{1,0:T(1,128)} %bitcast.17, ...), custom_call_target="tpu_custom_call" | custom-call | flops 6442450944 | bytes 10485760 | tf_op jit(solution)/shard_map/pallas_call | solution.py:367
  102.1 2.2 %collective-permute-start.14 = (bf16[128,2048]{1,0:T(8,128)(2,1)}, bf16[128,2048]{1,0:T(8,128)(2,1)S(1)}, u32[]{:S(2)}, u32[]{:S(2)}) collective-permute-start(bf16[128,2048]{1,0:T(8,128)(2,1)} %get-tuple-element.62), channel_id=1, source_target_pairs={{0,3},{1,0},{2,1},{3,2},{4,7},{5,4},{6,5},{7,6},{8,11},{9,8},{10,9... | collective-permute-start | bytes 1572872 | tf_op jit(solution)/shard_map/ppermute | solution.py:421
  104.3 9.3 %shard_map.159 = (bf16[128,2048]{1,0:T(8,128)(2,1)}, bf16[128,2048]{1,0:T(8,128)(2,1)}) custom-call(s32[16]{0:T(128)} %get-tuple-element.64.place.table, bf16[128,2048]{1,0:T(8,128)(2,1)} %copy-done.3, bf16[128,2048]{1,0:T(8,128)(2,1)} %copy-done.4, bf16[1024,1024]{1,0:T(8,128)(2,1)} %get-tuple-element.48.fv, f32[1,512]{1,0:T(1,128)} %bitcast.18, ...), custom_call_target="tpu_custom_call" | custom-call | flops 6442450944 | bytes 10485760 | tf_op jit(solution)/shard_map/pallas_call | solution.py:367
  113.6 3.3 %collective-permute-start.10 = (bf16[128,2048]{1,0:T(8,128)(2,1)}, bf16[128,2048]{1,0:T(8,128)(2,1)S(1)}, u32[]{:S(2)}, u32[]{:S(2)}) collective-permute-start(bf16[128,2048]{1,0:T(8,128)(2,1)} %get-tuple-element.56), channel_id=1, source_target_pairs={{0,3},{1,0},{2,1},{3,2},{4,7},{5,4},{6,5},{7,6},{8,11},{9,8},{10,9... | collective-permute-start | bytes 1572872 | tf_op jit(solution)/shard_map/ppermute | solution.py:421
  116.9 9.3 %shard_map.160 = (bf16[128,2048]{1,0:T(8,128)(2,1)}, bf16[128,2048]{1,0:T(8,128)(2,1)}) custom-call(s32[16]{0:T(128)} %get-tuple-element.64.place.table, bf16[128,2048]{1,0:T(8,128)(2,1)} %copy-done.1, bf16[128,2048]{1,0:T(8,128)(2,1)} %copy-done.2, bf16[1024,1024]{1,0:T(8,128)(2,1)} %get-tuple-element.48.fv, f32[1,512]{1,0:T(1,128)} %bitcast.19, ...), custom_call_target="tpu_custom_call" | custom-call | flops 6442450944 | bytes 10485760 | tf_op jit(solution)/shard_map/pallas_call | solution.py:367
  126.2 1.2 add_convert_fusion
  127.3 3.6 %collective-permute-start.15 = (bf16[128,2048]{1,0:T(8,128)(2,1)S(1)}, bf16[128,2048]{1,0:T(8,128)(2,1)S(1)}, u32[]{:S(2)}, u32[]{:S(2)}) collective-permute-start(bf16[128,2048]{1,0:T(8,128)(2,1)S(1)} %add_convert_fusion), channel_id=1, source_target_pairs={{0,3},{1,0},{2,1},{3,2},{4,7},{5,4},{6,5},{7,6},{8,11},{9,8},{10,9... | collective-permute-start | bytes 1572872 | tf_op jit(solution)/shard_map/ppermute | solution.py:421
  130.9 1.2 add_convert_fusion.1
  132.1 0.1 collective-permute-start.12
  132.2 9.3 %shard_map.158 = (bf16[128,2048]{1,0:T(8,128)(2,1)}, bf16[128,2048]{1,0:T(8,128)(2,1)}) custom-call(s32[16]{0:T(128)} %get-tuple-element.64.place.table, bf16[128,2048]{1,0:T(8,128)(2,1)} %get-tuple-element.34.refs_0_.x_top, bf16[128,2048]{1,0:T(8,128)(2,1)} %get-tuple-element.35.refs_1_.x_bottom, bf16[1024,1024]{1,0:T(8,128)(2,1)} %get-tuple-element.48.fv, ...), custom_call_target="tpu_custom_call" | custom-call | flops 6442450944 | bytes 10485760 | tf_op jit(solution)/shard_map/pallas_call | solution.py:367
  141.6 2.7 %collective-permute-done.12.sum_a = bf16[128,2048]{1,0:T(8,128)(2,1)S(1)} collective-permute-done((bf16[128,2048]{1,0:T(8,128)(2,1)S(1)}, bf16[128,2048]{1,0:T(8,128)(2,1)S(1)}, u32[]{:S(2)}, u32[]{:S(2)}) %collective-permute-start.12) | collective-permute-done | bytes 524320 | tf_op jit(solution)/shard_map/ppermute | solution.py:421
  144.3 0.8 copy-done.10
  145.1 4.0 %finish.1 = bf16[256,2048]{1,0:T(8,128)(2,1)} custom-call(bf16[128,2048]{1,0:T(8,128)(2,1)} %get-tuple-element.55.own_a, bf16[128,2048]{1,0:T(8,128)(2,1)} %copy-done.7, bf16[128,2048]{1,0:T(8,128)(2,1)} %copy-done.10, bf16[128,2048]{1,0:T(8,128)(2,1)} %get-tuple-element.59.own_b, bf16[128,2048]{1,0:T(8,128)(2,1)} %copy-done.8, bf16[128,2048]{1,0:T(8,128)(2,1)} %copy-done.9), custom_call_target="tpu_custom_call" | custom-call | tf_op jit(solution)/shard_map/finish/pallas_call | solution.py:409
  (38 shorter events, 0.2 us)
Async XLA Ops:
  2.8 17.3 %collective-permute-start = (bf16[128,2048]{1,0:T(8,128)(2,1)}, bf16[128,2048]{1,0:T(8,128)(2,1)S(1)}, u32[]{:S(2)}, u32[]{:S(2)}) collective-permute-start(bf16[128,2048]{1,0:T(8,128)(2,1)} %get-tuple-element.34.refs_0_.x_top), channel_id=1, source_target_pairs={{0,1},{1,2},{2,3},{3,0},{4,5},{5,6},{6,7},{7,4},{8,9},{9,10},{10,1... | collective-permute-start | bytes 1572872 | tf_op jit(solution)/shard_map/ppermute | solution.py:421
  4.3 15.9 %collective-permute-start.2 = (bf16[128,2048]{1,0:T(8,128)(2,1)}, bf16[128,2048]{1,0:T(8,128)(2,1)S(1)}, u32[]{:S(2)}, u32[]{:S(2)}) collective-permute-start(bf16[128,2048]{1,0:T(8,128)(2,1)} %get-tuple-element.35.refs_1_.x_bottom), channel_id=1, source_target_pairs={{0,3},{1,0},{2,1},{3,2},{4,7},{5,4},{6,5},{7,6},{8,11},{9,8},{10,9... | collective-permute-start | bytes 1572872 | tf_op jit(solution)/shard_map/ppermute | solution.py:421
  6.0 25.3 %collective-permute-start.4 = (bf16[128,2048]{1,0:T(8,128)(2,1)}, bf16[128,2048]{1,0:T(8,128)(2,1)S(1)}, u32[]{:S(2)}, u32[]{:S(2)}) collective-permute-start(bf16[128,2048]{1,0:T(8,128)(2,1)} %get-tuple-element.35.refs_1_.x_bottom), channel_id=1, source_target_pairs={{0,1},{1,2},{2,3},{3,0},{4,5},{5,6},{6,7},{7,4},{8,9},{9,10},{10,1... | collective-permute-start | bytes 1572872 | tf_op jit(solution)/shard_map/ppermute | solution.py:421
  6.3 25.0 %collective-permute-start.5 = (bf16[128,2048]{1,0:T(8,128)(2,1)}, bf16[128,2048]{1,0:T(8,128)(2,1)S(1)}, u32[]{:S(2)}, u32[]{:S(2)}) collective-permute-start(bf16[128,2048]{1,0:T(8,128)(2,1)} %get-tuple-element.34.refs_0_.x_top), channel_id=1, source_target_pairs={{0,3},{1,0},{2,1},{3,2},{4,7},{5,4},{6,5},{7,6},{8,11},{9,8},{10,9... | collective-permute-start | bytes 1572872 | tf_op jit(solution)/shard_map/ppermute | solution.py:421
  20.1 3.3 %copy-start.3 = (bf16[128,2048]{1,0:T(8,128)(2,1)}, bf16[128,2048]{1,0:T(8,128)(2,1)S(1)}, u32[]{:S(2)}) copy-start(bf16[128,2048]{1,0:T(8,128)(2,1)S(1)} %collective-permute-done.refs_0_.x_top) | copy-start | bytes 1572868
  20.1 20.2 %collective-permute-start.1 = (bf16[128,2048]{1,0:T(8,128)(2,1)S(1)}, bf16[128,2048]{1,0:T(8,128)(2,1)S(1)}, u32[]{:S(2)}, u32[]{:S(2)}) collective-permute-start(bf16[128,2048]{1,0:T(8,128)(2,1)S(1)} %collective-permute-done.refs_0_.x_top), channel_id=1, source_target_pairs={{0,1},{1,2},{2,3},{3,0},{4,5},{5,6},{6,7},{7,4},{8,9},{9,10},{10,1... | collective-permute-start | bytes 1572872 | tf_op jit(solution)/shard_map/ppermute | solution.py:421
  20.2 3.2 %copy-start.4 = (bf16[128,2048]{1,0:T(8,128)(2,1)}, bf16[128,2048]{1,0:T(8,128)(2,1)S(1)}, u32[]{:S(2)}) copy-start(bf16[128,2048]{1,0:T(8,128)(2,1)S(1)} %collective-permute-done.2.refs_1_.x_bottom) | copy-start | bytes 1572868
  20.2 20.1 %collective-permute-start.3 = (bf16[128,2048]{1,0:T(8,128)(2,1)S(1)}, bf16[128,2048]{1,0:T(8,128)(2,1)S(1)}, u32[]{:S(2)}, u32[]{:S(2)}) collective-permute-start(bf16[128,2048]{1,0:T(8,128)(2,1)S(1)} %collective-permute-done.2.refs_1_.x_bottom), channel_id=1, source_target_pairs={{0,3},{1,0},{2,1},{3,2},{4,7},{5,4},{6,5},{7,6},{8,11},{9,8},{10,9... | collective-permute-start | bytes 1572872 | tf_op jit(solution)/shard_map/ppermute | solution.py:421
  31.4 0.8 copy-start.1
  31.4 1.0 copy-start.2
  40.4 0.8 copy-start.5
  40.4 1.0 copy-start.6
  49.9 16.1 %all-to-all-start = ((bf16[32,32,128]{2,1,0:T(8,128)(2,1)}), bf16[32,32,128]{2,1,0:T(8,128)(2,1)S(1)}, u32[]{:S(2)}, u32[]{:S(2)}) async-start(bf16[32,32,128]{2,1,0:T(8,128)(2,1)} %get-tuple-element.51), calls=%async_computation | async-start | bytes 524288 | tf_op jit(solution)/shard_map/all_to_all | solution.py:239
  60.3 13.1 %collective-permute-start.6 = (bf16[32,512]{1,0:T(8,128)(2,1)S(1)}, bf16[32,512]{1,0:T(8,128)(2,1)S(1)}, u32[]{:S(2)}, u32[]{:S(2)}) collective-permute-start(bf16[32,512]{1,0:T(8,128)(2,1)S(1)} %constant_dynamic-slice_fusion), channel_id=1, source_target_pairs={{0,4},{4,8},{8,12},{12,16},{16,20},{20,24},{24,28},{28,32},{32,36}... | collective-permute-start | bytes 98312 | tf_op jit(solution)/shard_map/ppermute | solution.py:466
  66.0 0.7 copy-start
  68.4 23.7 %all-to-all-start.1 = ((bf16[32,16,128]{2,1,0:T(8,128)(2,1)}), bf16[32,16,128]{2,1,0:T(8,128)(2,1)S(1)}, u32[]{:S(2)}, u32[]{:S(2)}) async-start(bf16[32,16,128]{2,1,0:T(8,128)(2,1)} %prefix.1), calls=%async_computation.1 | async-start | bytes 262144 | tf_op jit(solution)/shard_map/all_to_all | solution.py:247
  73.5 0.6 copy-start.15
  83.7 5.3 %collective-permute-start.7 = (f32[8,1024]{1,0:T(8,128)}, f32[8,1024]{1,0:T(8,128)S(1)}, u32[]{:S(2)}, u32[]{:S(2)}) collective-permute-start(f32[8,1024]{1,0:T(8,128)} %get-tuple-element.54.s0), channel_id=1, source_target_pairs={{0,1},{1,2},{2,3},{3,0},{4,5},{5,6},{6,7},{7,4},{8,9},{9,10},{10,1... | collective-permute-start | bytes 98312 | tf_op jit(solution)/shard_map/ppermute | solution.py:421
  85.0 5.6 %collective-permute-start.8 = (f32[8,1024]{1,0:T(8,128)}, f32[8,1024]{1,0:T(8,128)S(1)}, u32[]{:S(2)}, u32[]{:S(2)}) collective-permute-start(f32[8,1024]{1,0:T(8,128)} %get-tuple-element.54.s0), channel_id=1, source_target_pairs={{0,2},{1,3},{2,0},{3,1},{4,6},{5,7},{6,4},{7,5},{8,10},{9,11},{10,... | collective-permute-start | bytes 98312 | tf_op jit(solution)/shard_map/ppermute | solution.py:421
  87.9 4.1 %collective-permute-start.9 = (f32[8,1024]{1,0:T(8,128)}, f32[8,1024]{1,0:T(8,128)S(1)}, u32[]{:S(2)}, u32[]{:S(2)}) collective-permute-start(f32[8,1024]{1,0:T(8,128)} %get-tuple-element.54.s0), channel_id=1, source_target_pairs={{0,3},{1,0},{2,1},{3,2},{4,7},{5,4},{6,5},{7,6},{8,11},{9,8},{10,9... | collective-permute-start | bytes 98312 | tf_op jit(solution)/shard_map/ppermute | solution.py:421
  89.0 3.1 %copy-start.12 = (f32[8,1024]{1,0:T(8,128)}, f32[8,1024]{1,0:T(8,128)S(1)}, u32[]{:S(2)}) copy-start(f32[8,1024]{1,0:T(8,128)S(1)} %collective-permute-done.7.s1) | copy-start | bytes 98308
  90.6 1.4 copy-start.13
  92.0 0.6 copy-start.14
  92.1 0.7 copy-start.11
  102.1 24.1 %collective-permute-start.14 = (bf16[128,2048]{1,0:T(8,128)(2,1)}, bf16[128,2048]{1,0:T(8,128)(2,1)S(1)}, u32[]{:S(2)}, u32[]{:S(2)}) collective-permute-start(bf16[128,2048]{1,0:T(8,128)(2,1)} %get-tuple-element.62), channel_id=1, source_target_pairs={{0,3},{1,0},{2,1},{3,2},{4,7},{5,4},{6,5},{7,6},{8,11},{9,8},{10,9... | collective-permute-start | bytes 1572872 | tf_op jit(solution)/shard_map/ppermute | solution.py:421
  104.3 26.6 %collective-permute-start.11 = (bf16[128,2048]{1,0:T(8,128)(2,1)}, bf16[128,2048]{1,0:T(8,128)(2,1)S(1)}, u32[]{:S(2)}, u32[]{:S(2)}) collective-permute-start(bf16[128,2048]{1,0:T(8,128)(2,1)} %get-tuple-element.58), channel_id=1, source_target_pairs={{0,1},{1,2},{2,3},{3,0},{4,5},{5,6},{6,7},{7,4},{8,9},{9,10},{10,1... | collective-permute-start | bytes 1572872 | tf_op jit(solution)/shard_map/ppermute | solution.py:421
  113.6 28.0 %collective-permute-start.10 = (bf16[128,2048]{1,0:T(8,128)(2,1)}, bf16[128,2048]{1,0:T(8,128)(2,1)S(1)}, u32[]{:S(2)}, u32[]{:S(2)}) collective-permute-start(bf16[128,2048]{1,0:T(8,128)(2,1)} %get-tuple-element.56), channel_id=1, source_target_pairs={{0,3},{1,0},{2,1},{3,2},{4,7},{5,4},{6,5},{7,6},{8,11},{9,8},{10,9... | collective-permute-start | bytes 1572872 | tf_op jit(solution)/shard_map/ppermute | solution.py:421
  116.9 24.7 %collective-permute-start.13 = (bf16[128,2048]{1,0:T(8,128)(2,1)}, bf16[128,2048]{1,0:T(8,128)(2,1)S(1)}, u32[]{:S(2)}, u32[]{:S(2)}) collective-permute-start(bf16[128,2048]{1,0:T(8,128)(2,1)} %get-tuple-element.60), channel_id=1, source_target_pairs={{0,1},{1,2},{2,3},{3,0},{4,5},{5,6},{6,7},{7,4},{8,9},{9,10},{10,1... | collective-permute-start | bytes 1572872 | tf_op jit(solution)/shard_map/ppermute | solution.py:421
  127.3 14.2 %collective-permute-start.15 = (bf16[128,2048]{1,0:T(8,128)(2,1)S(1)}, bf16[128,2048]{1,0:T(8,128)(2,1)S(1)}, u32[]{:S(2)}, u32[]{:S(2)}) collective-permute-start(bf16[128,2048]{1,0:T(8,128)(2,1)S(1)} %add_convert_fusion), channel_id=1, source_target_pairs={{0,3},{1,0},{2,1},{3,2},{4,7},{5,4},{6,5},{7,6},{8,11},{9,8},{10,9... | collective-permute-start | bytes 1572872 | tf_op jit(solution)/shard_map/ppermute | solution.py:421
  132.1 12.2 %collective-permute-start.12 = (bf16[128,2048]{1,0:T(8,128)(2,1)S(1)}, bf16[128,2048]{1,0:T(8,128)(2,1)S(1)}, u32[]{:S(2)}, u32[]{:S(2)}) collective-permute-start(bf16[128,2048]{1,0:T(8,128)(2,1)S(1)} %add_convert_fusion.1), channel_id=1, source_target_pairs={{0,1},{1,2},{2,3},{3,0},{4,5},{5,6},{6,7},{7,4},{8,9},{9,10},{10,1... | collective-permute-start | bytes 1572872 | tf_op jit(solution)/shard_map/ppermute | solution.py:421
  141.5 2.8 %copy-start.7 = (bf16[128,2048]{1,0:T(8,128)(2,1)}, bf16[128,2048]{1,0:T(8,128)(2,1)S(1)}, u32[]{:S(2)}) copy-start(bf16[128,2048]{1,0:T(8,128)(2,1)S(1)} %collective-permute-done.10.got_a) | copy-start | bytes 1572868
  141.5 2.8 %copy-start.8 = (bf16[128,2048]{1,0:T(8,128)(2,1)}, bf16[128,2048]{1,0:T(8,128)(2,1)S(1)}, u32[]{:S(2)}) copy-start(bf16[128,2048]{1,0:T(8,128)(2,1)S(1)} %collective-permute-done.13.got_b) | copy-start | bytes 1572868
  141.6 2.7 %copy-start.9 = (bf16[128,2048]{1,0:T(8,128)(2,1)}, bf16[128,2048]{1,0:T(8,128)(2,1)S(1)}, u32[]{:S(2)}) copy-start(bf16[128,2048]{1,0:T(8,128)(2,1)S(1)} %collective-permute-done.15.sum_b) | copy-start | bytes 1572868
  144.3 0.8 copy-start.10

commit v3 on v2

v3 whole, which is shorter than its diff:
```python
import functools

import jax
import jax.numpy as jnp
import numpy as np
from jax import lax
from jax.experimental import pallas as pl
from jax.experimental.pallas import tpu as pltpu
from jax.sharding import PartitionSpec as P


HEAD = 128
BLK = 128
NORM_EPS = 1e-05
HEAD_EPS = 1e-06
F32 = jnp.float32
BF16 = jnp.bfloat16


SLOT = np.array([[0, 1], [5, 3], [6, 7], [2, 4]])
SLOT_TABLE = np.array(
    [[SLOT[(p // 2 - t) % 4][p % 2] for p in range(8)] for t in range(4)], dtype=np.int32
)
PLACE_TABLE = np.argsort(SLOT_TABLE, axis=1).astype(np.int32)
PLACES = np.concatenate([PLACE_TABLE, SLOT_TABLE], axis=1).reshape(-1)


def block_of(t, places, slot):
    return places[16 * t[0] + slot]


def slot_of(t, places, block):
    return places[16 * t[0] + 8 + block]


def params(mib=8, **kw):
    return pltpu.CompilerParams(vmem_limit_bytes=mib * 1024 * 1024, **kw)


def dot(a, b, dims=((1,), (0,))):
    return lax.dot_general(a, b, (dims, ((), ())), preferred_element_type=F32)


def silu(x):
    return x * jax.nn.sigmoid(x)


WIDE = 4 * HEAD


def gates(forget, gap, shift):
    key = gap * jax.nn.sigmoid(-forget.astype(F32))
    columns = jnp.transpose(jnp.concatenate([shift] * (BLK // 4), axis=0))
    spread = jnp.concatenate(
        [jnp.broadcast_to(columns[:, h : h + 1], (BLK, HEAD)) for h in range(4)], axis=1
    )
    log_forget = jnp.log1p(-key) + spread
    high = log_forget.astype(BF16)
    low = (log_forget - high.astype(F32)).astype(BF16)
    rows = lax.broadcasted_iota(jnp.int32, (BLK, BLK), 0)
    cols = lax.broadcasted_iota(jnp.int32, (BLK, BLK), 1)
    lower = (rows >= cols).astype(F32).astype(BF16)
    return key, dot(lower, high) + dot(lower, low)


def pieces(log_row):
    high = log_row.astype(BF16).astype(F32)
    mid = (log_row - high).astype(BF16).astype(F32)
    low = log_row - high - mid
    row = lax.broadcasted_iota(jnp.int32, (16, HEAD), 0)
    tile = jnp.where(row == 0, high, jnp.where(row == 1, mid, jnp.where(row == 2, low, 0.0)))
    return tile.astype(BF16)


def block_outputs(key, run, value, query, near, query_near, at):
    middle = run[BLK // 2 - 1 : BLK // 2, :]
    query_mid = silu(query.astype(F32)) * jnp.exp(run - middle)
    key_mid = (key * jnp.exp(middle - run)).astype(BF16)
    query_near[at, :] = (query_mid * jnp.exp(middle)).astype(BF16)
    query_mid = query_mid.astype(BF16)
    rows = lax.broadcasted_iota(jnp.int32, (BLK, BLK), 0)
    cols = lax.broadcasted_iota(jnp.int32, (BLK, BLK), 1)
    for h in range(4):
        lanes = slice(h * HEAD, (h + 1) * HEAD)
        scores = dot(query_mid[:, lanes], key_mid[:, lanes], ((1,), (1,)))
        scores = jnp.where(rows >= cols, scores, 0.0).astype(BF16)
        near[at, lanes] = dot(scores, value[:, lanes])


def fetch(pairs, sems):
    copies = [pltpu.make_async_copy(source, target, sems.at[k]) for k, (source, target) in enumerate(pairs)]
    for copy in copies:
        copy.start()
    return copies


def norm_kernel(tokens, gain, top, bottom, rows_in, sems):
    halves = [pl.ds(0, BLK), pl.ds(BLK, BLK)]
    copies = fetch([(tokens.at[h], rows_in.at[h]) for h in halves], sems)
    g = gain[...]
    for k, out in enumerate((top, bottom)):
        copies[k].wait()
        for r in range(0, BLK, 16):
            rows = rows_in[k * BLK + r : k * BLK + r + 16, :].astype(F32)
            centred = rows - jnp.mean(rows, axis=-1, keepdims=True)
            var = jnp.mean(centred * centred, axis=-1, keepdims=True)
            out[r : r + 16, :] = (centred * lax.rsqrt(var + NORM_EPS) * g).astype(BF16)


def norm_rows(tokens, gain):
    half = jax.ShapeDtypeStruct((BLK, tokens.shape[1]), BF16)
    return pl.pallas_call(
        norm_kernel,
        in_specs=[hbm_spec(), pl.BlockSpec(gain.shape, lambda: (0, 0))],
        out_shape=[half, half],
        scratch_shapes=[pltpu.VMEM(tokens.shape, BF16), pltpu.SemaphoreType.DMA((2,))],
        compiler_params=params(58),
        name="norm_rows",
    )(tokens, gain)


def glu(value, gate):
    return (value.astype(F32) * jax.nn.sigmoid(gate.astype(F32))).astype(BF16)


def keys_kernel(first, last, t, places, *refs):
    x_top, x_bottom, gap, shift_top, shift_bottom = refs[:5]
    weights, refs = refs[5:9], refs[9:]
    if first:
        fv, mixed, added, close, xbuf, sems = refs
    elif last:
        mixed_in, added, close_all, fv, mixed, pack, starts, offsets, edge, xbuf, parts, tail, sems = refs[1:]
    else:
        fv, mixed, added, close, xbuf, sems = refs[4:]
    pairs = [(x_top, xbuf.at[pl.ds(0, BLK)]), (x_bottom, xbuf.at[pl.ds(BLK, BLK)])]
    if last:
        tail_slot = slot_of(t, places, 7)
        start = pl.multiple_of(jnp.minimum(tail_slot, 5) * BLK + BLK - 32, 32)
        pairs += [(added.at[pl.ds(0, 6)], parts.at[pl.ds(0, 6)]), (mixed_in.at[pl.ds(start, 32)], tail)]
    copies = fetch(pairs, sems)
    copies[0].wait()
    copies[1].wait()

    def times(n):
        return dot(xbuf[...], weights[n][...]).astype(BF16)

    fv[:, 0:WIDE] = times(0)
    fv[:, WIDE : 2 * WIDE] = times(1)
    ends = []
    for k, shift in enumerate((shift_top, shift_bottom)):
        at = slice(k * BLK, (k + 1) * BLK)
        key, run = gates(fv[at, 0:WIDE], gap[...], shift[...])
        value = fv[at, WIDE : 2 * WIDE]
        end = run[BLK - 1 : BLK, :]
        key_far = (key * jnp.exp(end - run)).astype(BF16)
        ends.append(end)
        if not last:
            close[k] = jnp.broadcast_to(end, (8, WIDE))
        for h in range(4):
            lanes = slice(h * HEAD, (h + 1) * HEAD)
            sum_h = dot(value[:, lanes], key_far[:, lanes], ((0,), (0,)))
            if last:
                parts[6 + k, h] = sum_h
            else:
                added[k, h] = sum_h
    mixed_now = glu(times(2), times(3))
    mixed[...] = mixed_now
    if last:
        copies[2].wait()
        copies[3].wait()
        edge[...] = jnp.where(
            tail_slot == 7, mixed_now[2 * BLK - 32 :, :].astype(F32), tail[...].astype(F32)
        ).astype(BF16)
        scan_blocks(t, places, ends, close_all, parts, pack, starts, offsets)


def scan_blocks(t, places, ends, close_all, parts, pack, starts, offsets):
    state = [jnp.zeros((HEAD, HEAD), F32) for _ in range(4)]
    total = jnp.zeros((1, WIDE), F32)
    for i in range(8):
        slot = slot_of(t, places, i)
        offsets[slot] = jnp.broadcast_to(total, (8, WIDE))
        end = jnp.where(
            slot == 6, ends[0], jnp.where(slot == 7, ends[1], close_all[jnp.minimum(slot, 5)][0:1, :])
        )
        keep = jnp.exp(end)
        for h in range(4):
            lanes = slice(h * HEAD, (h + 1) * HEAD)
            starts[slot, h] = state[h].astype(BF16)
            state[h] = state[h] * keep[:, lanes] + parts[slot, h]
        total = total + end
    for h in range(4):
        tile = pieces(total[:, h * HEAD : (h + 1) * HEAD])
        rows = state[h].astype(BF16)
        for j in range(8):
            pack[8 * h + j, 0:16, :] = rows[16 * j : 16 * j + 16, :]
            pack[8 * h + j, 16:24, :] = tile[0:8, :]


def any_spec():
    return pl.BlockSpec(memory_space=pl.ANY)


def hbm_spec():
    return pl.BlockSpec(memory_space=pltpu.HBM)


def keys(group, x, t, gap, shift, weights, bufs):
    depth = x[0].shape[1]
    rows = 2 * BLK
    first, last = group == 0, group == 3
    block = lambda *shape: pl.BlockSpec(shape, lambda i, t, p: (group,) + (0,) * (len(shape) - 1))
    whole = lambda *shape: pl.BlockSpec(shape, lambda i, t, p: (0,) * len(shape))
    array = jax.ShapeDtypeStruct
    out_specs = [block(rows, 2 * WIDE), block(rows, WIDE)]
    out_shape = [array((8 * BLK, 2 * WIDE), BF16), array((8 * BLK, WIDE), BF16)]
    scratch = [pltpu.VMEM((rows, depth), BF16)]
    weight_specs = [pl.BlockSpec(memory_space=pltpu.VMEM)] * 4
    if last:
        buf_specs = [any_spec(), any_spec(), any_spec(), whole(8, 8, WIDE)]
        out_specs += [whole(32, 24, HEAD), whole(8, 4, HEAD, HEAD), whole(8, 8, WIDE), whole(32, WIDE)]
        out_shape += [
            array((32, 24, HEAD), BF16),
            array((8, 4, HEAD, HEAD), BF16),
            array((8, 8, WIDE), F32),
            array((32, WIDE), BF16),
        ]
        scratch += [pltpu.VMEM((8, 4, HEAD, HEAD), F32), pltpu.VMEM((32, WIDE), BF16)]
    else:
        buf_specs = [any_spec()] * len(bufs)
        out_specs += [block(2, 4, HEAD, HEAD), block(2, 8, WIDE)]
        out_shape += [array((8, 4, HEAD, HEAD), F32), array((8, 8, WIDE), F32)]
    copies = 4 if last else 2
    aliased = min(len(bufs), 2 if last else 4)
    return pl.pallas_call(
        functools.partial(keys_kernel, first, last),
        grid_spec=pltpu.PrefetchScalarGridSpec(
            num_scalar_prefetch=2,
            grid=(1,),
            in_specs=[any_spec()] * 2
            + [whole(1, WIDE)]
            + [pl.BlockSpec((4, BLK), lambda i, t, p, k=k: (0, block_of(t, p, 2 * group + k))) for k in range(2)]
            + weight_specs
            + buf_specs,
            out_specs=out_specs,
            scratch_shapes=scratch + [pltpu.SemaphoreType.DMA((copies,))],
        ),
        out_shape=out_shape,
        input_output_aliases={11 + k: k for k in range(aliased)},
        compiler_params=params(28),
        cost_estimate=pl.CostEstimate(
            flops=2 * rows * depth * WIDE * 6, bytes_accessed=12 * 2**20, transcendentals=0
        ),
    )(t, jnp.asarray(PLACES), *x, gap, shift, shift, *weights, *bufs)


def prefix_kernel(packs, arriving):
    state = jnp.zeros((16, HEAD), F32)
    for i in range(32):
        arriving[i] = state.astype(BF16)
        tile = packs[i, 16:24, :].astype(F32)
        log = tile[0:1] + tile[1:2] + tile[2:3]
        state = jnp.exp(log) * state + packs[i, 0:16, :].astype(F32)


def arriving_states(pack):
    packs = lax.all_to_all(pack, "sp", split_axis=0, concat_axis=0, tiled=True)
    arriving = pl.pallas_call(
        prefix_kernel,
        out_shape=jax.ShapeDtypeStruct((32, 16, HEAD), BF16),
        compiler_params=params(),
        cost_estimate=pl.CostEstimate(flops=10**8, bytes_accessed=2**20, transcendentals=0),
        name="prefix",
    )(packs)
    arrived = lax.all_to_all(arriving, "sp", split_axis=0, concat_axis=0, tiled=True)
    return arrived.reshape(4, HEAD, HEAD)


def filter_kernel(t, places, mixed, halo, taps, filtered, stats, window, sums):
    i = pl.program_id(0)
    reach = 32

    @pl.when(i == 0)
    def _():
        window[0:reach, :] = halo[...].astype(F32)

    @pl.when(i > 0)
    def _():
        window[0:reach, :] = window[BLK : BLK + reach, :]

    window[reach : reach + BLK, :] = mixed[...].astype(F32)
    sums[...] = jnp.zeros_like(sums)

    def one(c, carry):
        lanes = pl.ds(pl.multiple_of(c * HEAD, HEAD), HEAD)
        acc = jnp.zeros((BLK, HEAD), F32)
        for r in range(8):
            used = [q for q in range(5) if 0 <= 8 * q + r - 2 < 31]
            shifted = window[8 * used[0] + r : 8 * used[-1] + r + BLK, lanes]
            part = None
            for q in used:
                j, lead = 8 * q + r - 2, 8 * (q - used[0])
                term = taps[j : j + 1, lanes] * shifted[lead : lead + BLK, :]
                part = term if part is None else part + term
            acc = acc + part
        filtered[:, lanes] = acc
        sums[0] = sums[0] + acc
        sums[1] = sums[1] + acc * acc
        return carry

    lax.fori_loop(0, 4, one, 0)
    lane = lax.broadcasted_iota(jnp.int32, (BLK, HEAD), 1)
    tile = jnp.where(
        lane == 0,
        jnp.sum(sums[0], axis=1, keepdims=True),
        jnp.where(lane == 1, jnp.sum(sums[1], axis=1, keepdims=True), 0.0),
    )
    stats[...] = jnp.transpose(tile)[0:8, :]


def filter_rows(t, mixed, halo, taps):
    return pl.pallas_call(
        filter_kernel,
        grid_spec=pltpu.PrefetchScalarGridSpec(
            num_scalar_prefetch=2,
            grid=(8,),
            in_specs=[
                pl.BlockSpec((BLK, WIDE), lambda i, t, p: (slot_of(t, p, i), 0)),
                pl.BlockSpec((32, WIDE), lambda i, t, p: (0, 0)),
                pl.BlockSpec((31, WIDE), lambda i, t, p: (0, 0)),
            ],
            out_specs=[
                pl.BlockSpec((BLK, WIDE), lambda i, t, p: (slot_of(t, p, i), 0)),
                pl.BlockSpec((8, BLK), lambda i, t, p: (0, i)),
            ],
            scratch_shapes=[pltpu.VMEM((32 + BLK, WIDE), F32), pltpu.VMEM((2, BLK, HEAD), F32)],
        ),
        out_shape=[
            jax.ShapeDtypeStruct((8 * BLK, WIDE), F32),
            jax.ShapeDtypeStruct((8, 8 * BLK), F32),
        ],
        compiler_params=params(58),
        cost_estimate=pl.CostEstimate(flops=7 * 10**9, bytes_accessed=5 * 2**20, transcendentals=0),
        name="filter_rows",
    )(t, jnp.asarray(PLACES), mixed, halo, taps)


QUERY_SCRATCH = [((2 * BLK, 2048), BF16), ((2, 2048, WIDE), BF16), ((2 * BLK, 2 * WIDE), BF16), ((2 * BLK, WIDE), BF16)]
NEAR_SCRATCH = [((2 * BLK, WIDE), F32), ((2 * BLK, WIDE), BF16), ((2 * BLK, WIDE), BF16)]


def rows_of(ref, group, size):
    return ref.at[pl.ds(group * size, size)]


def query_side(group, later, ins, scratch, outs, sems):
    x_top, x_bottom, fv_all, w_query, w_rgate, gap, *shifts = ins
    xbuf, wbuf, fv, query = scratch
    near, query_near, rgate = outs
    copies = fetch(
        [
            (x_top, xbuf.at[pl.ds(0, BLK)]),
            (x_bottom, xbuf.at[pl.ds(BLK, BLK)]),
            (w_query, wbuf.at[0]),
            (rows_of(fv_all, group, 2 * BLK), fv),
            (w_rgate, wbuf.at[1]),
        ],
        sems,
    )
    for k in range(3):
        copies[k].wait()
    more = later()
    query[...] = dot(xbuf[...], wbuf[0]).astype(BF16)
    copies[3].wait()
    for k, shift in enumerate(shifts):
        rows = slice(k * BLK, (k + 1) * BLK)
        key, run = gates(fv[rows, 0:WIDE], gap[...], shift[...])
        block_outputs(key, run, fv[rows, WIDE : 2 * WIDE], query[rows, :], near, query_near, rows)
    copies[4].wait()
    rgate[...] = dot(xbuf[...], wbuf[1]).astype(BF16)
    return more


def query_kernel(group, t, places, *refs):
    outs, scratch, sems = refs[8:11], refs[11:15], refs[15]
    query_side(group, lambda: None, refs[:8], scratch, outs, sems)


def query_specs(group):
    return (
        [hbm_spec()] * 5
        + [pl.BlockSpec((1, WIDE), lambda i, t, p: (0, 0))]
        + [pl.BlockSpec((4, BLK), lambda i, t, p, k=k: (0, block_of(t, p, 2 * group + k))) for k in range(2)]
    )


def query_rows(group, x, t, fv, gap, shift, w_query, w_rgate):
    return pl.pallas_call(
        functools.partial(query_kernel, group),
        grid_spec=pltpu.PrefetchScalarGridSpec(
            num_scalar_prefetch=2,
            grid=(1,),
            in_specs=query_specs(group),
            out_specs=[pl.BlockSpec((2 * BLK, WIDE), lambda i, t, p: (0, 0))] * 3,
            scratch_shapes=[pltpu.VMEM(*v) for v in QUERY_SCRATCH] + [pltpu.SemaphoreType.DMA((5,))],
        ),
        out_shape=[jax.ShapeDtypeStruct((2 * BLK, WIDE), kind) for kind in (F32, BF16, BF16)],
        compiler_params=params(58),
        cost_estimate=pl.CostEstimate(
            flops=2 * 2 * BLK * 2048 * WIDE * 4, bytes_accessed=6 * 2**20, transcendentals=0
        ),
    )(t, jnp.asarray(PLACES), *x, fv, w_query, w_rgate, gap, shift, shift)


MERGE_SCRATCH = [
    ((2, WIDE, 2048), BF16),
    ((2, 4, HEAD, HEAD), BF16),
    ((2, 8, WIDE), F32),
    ((4, HEAD, HEAD), BF16),
    ((2 * BLK, WIDE), F32),
    ((4, 8, 8 * BLK), F32),
    ((2 * BLK, 2 * WIDE), BF16),
]


def merge_kernel(group, split, t, places, *refs):
    lead, refs = (refs[:3], refs[3:]) if split else (refs[:8], refs[8:])
    starts_all, offsets_all, arrived_all, filtered_all, *stats_all = refs[:8]
    w_rec, w_conv, head_gain, conv_gain, top, bottom = refs[8:14]
    obuf, starts, offsets, arrived, filtered, stats_buf, act = refs[14:21]
    near, query_near, rgate = refs[21:24]
    sems, refs = refs[24], refs[25:]

    def later():
        return fetch(
            [
                (rows_of(starts_all, group, 2), starts),
                (rows_of(offsets_all, group, 2), offsets),
                (arrived_all, arrived),
                (rows_of(filtered_all, group, 2 * BLK), filtered),
            ]
            + [(s, stats_buf.at[k]) for k, s in enumerate(stats_all)]
            + [(w_rec, obuf.at[0]), (w_conv, obuf.at[1])],
            sems,
        )

    if split:
        first = fetch(list(zip(lead, (near, query_near, rgate))), refs[0])
        more = later()
        for copy in first:
            copy.wait()
    else:
        more = query_side(group, later, lead, refs[:4], (near, query_near, rgate), refs[4])
    for copy in more[:8]:
        copy.wait()
    for k in range(2):
        rows = slice(k * BLK, (k + 1) * BLK)
        carry = jnp.exp(offsets[k, 0:1, :])
        for h in range(4):
            lanes = slice(h * HEAD, (h + 1) * HEAD)
            state = starts[k, h].astype(F32) + carry[:, lanes] * arrived[h].astype(F32)
            rec = near[rows, lanes] + dot(query_near[rows, lanes], state.astype(BF16), ((1,), (1,)))
            rec = rec * lax.rsqrt(jnp.mean(rec * rec, axis=-1, keepdims=True) + HEAD_EPS)
            rec = rec * head_gain[...] * silu(rgate[rows, lanes].astype(F32))
            act[rows, lanes] = rec.astype(BF16)
        at = pl.ds(pl.multiple_of(block_of(t, places, 2 * group + k) * BLK, BLK), BLK)
        stats = (stats_buf[0, :, at] + stats_buf[1, :, at]) + (stats_buf[2, :, at] + stats_buf[3, :, at])
        tile = jnp.transpose(jnp.concatenate([stats] * 16, axis=0))
        mean = tile[:, 0:1] / 2048.0
        scale = lax.rsqrt(tile[:, 1:2] / 2048.0 - mean * mean + NORM_EPS)
        normed = (filtered[rows, :] - mean) * scale * conv_gain[...]
        act[rows, WIDE : 2 * WIDE] = silu(normed).astype(BF16)
    more[8].wait()
    more[9].wait()
    for n in range(4):
        cols = slice(n * 512, (n + 1) * 512)
        part = dot(act[:, 0:WIDE], obuf[0, :, cols]) + dot(act[:, WIDE : 2 * WIDE], obuf[1, :, cols])
        top[:, cols] = part[0:BLK, :].astype(BF16)
        bottom[:, cols] = part[BLK : 2 * BLK, :].astype(BF16)


def merge(group, x, t, fv, gap, shift, starts, offsets, arrived, head_gain, filtered, stats, conv_gain, w_query, w_rgate, out_rec, out_conv, ready=None):
    width = out_rec.shape[1]
    split = ready is not None
    whole = lambda *shape: pl.BlockSpec(shape, lambda i, t, p: (0,) * len(shape))
    scratch = [pltpu.VMEM(*v) for v in MERGE_SCRATCH + NEAR_SCRATCH] + [pltpu.SemaphoreType.DMA((10,))]
    if split:
        lead, lead_specs = ready, [hbm_spec()] * 3
        scratch += [pltpu.SemaphoreType.DMA((3,))]
    else:
        lead, lead_specs = (*x, fv, w_query, w_rgate, gap, shift, shift), query_specs(group)
        scratch += [pltpu.VMEM(*v) for v in QUERY_SCRATCH] + [pltpu.SemaphoreType.DMA((5,))]
    return pl.pallas_call(
        functools.partial(merge_kernel, group, split),
        grid_spec=pltpu.PrefetchScalarGridSpec(
            num_scalar_prefetch=2,
            grid=(1,),
            in_specs=lead_specs + [hbm_spec()] * 10 + [whole(1, HEAD), whole(1, WIDE)],
            out_specs=[whole(BLK, width), whole(BLK, width)],
            scratch_shapes=scratch,
        ),
        out_shape=[jax.ShapeDtypeStruct((BLK, width), BF16)] * 2,
        compiler_params=params(58),
        cost_estimate=pl.CostEstimate(
            flops=2 * 2 * BLK * 1024 * 2048 * 6, bytes_accessed=10 * 2**20, transcendentals=0
        ),
    )(t, jnp.asarray(PLACES), *lead, starts, offsets, arrived, filtered, *stats, out_rec, out_conv, head_gain, conv_gain)


def finish_kernel(own_a, got_a, sum_a, own_b, got_b, sum_b, out):
    for k, parts in enumerate(((own_a, got_a, sum_a), (own_b, got_b, sum_b))):
        total = sum(p[...].astype(F32) for p in parts[1:]) + parts[0][...].astype(F32)
        out[k * BLK : (k + 1) * BLK, :] = total.astype(BF16)


def finish(*parts):
    width = parts[0].shape[1]
    return pl.pallas_call(
        finish_kernel,
        grid=(4,),
        in_specs=[pl.BlockSpec((BLK, width // 4), lambda n: (0, n))] * 6,
        out_specs=pl.BlockSpec((2 * BLK, width // 4), lambda n: (0, n)),
        out_shape=jax.ShapeDtypeStruct((2 * BLK, width), BF16),
        compiler_params=params(),
        name="finish",
    )(*parts)


def permuted(value, perm):
    return lax.ppermute(value, "tp", perm)


def on_device(
    tokens,
    norm_gain,
    w_query,
    w_forget,
    w_value,
    w_rgate,
    w_glu_value,
    w_glu_gate,
    forget_gap,
    decay_shift,
    head_gain,
    conv_taps,
    conv_gain,
    out_rec,
    out_conv,
):
    ahead = [(i, (i + 1) % 4) for i in range(4)]
    behind = [(i, (i - 1) % 4) for i in range(4)]
    t = lax.axis_index("tp").astype(jnp.int32).reshape(1)
    gap, shift = forget_gap[None, :], decay_shift.T
    a, b = norm_rows(tokens, norm_gain[None, :])
    from_back_a = permuted(a, ahead)
    from_front_b = permuted(b, behind)
    from_back_b = permuted(b, ahead)
    from_front_a = permuted(a, behind)
    far_a = permuted(from_back_a, ahead)
    far_b = permuted(from_front_b, behind)
    slots = ((a, b), (from_back_a, from_front_b), (from_back_b, from_front_a), (far_a, far_b))

    weights = (w_forget, w_value, w_glu_value, w_glu_gate)
    bufs = ()
    for group in range(3):
        bufs = keys(group, slots[group], t, gap, shift, weights, bufs)
    fv, mixed, pack, starts, offsets, edge = keys(3, slots[3], t, gap, shift, weights, bufs)

    halo = lax.ppermute(edge, "sp", [(i, i + 1) for i in range(31)])
    arrived = arriving_states(pack)
    filtered, stats = filter_rows(t, mixed, halo, conv_taps)
    stats_all = [stats] + [permuted(stats, [(i, (i + d) % 4) for i in range(4)]) for d in (1, 2, 3)]
    ready = query_rows(3, slots[3], t, fv, gap, shift, w_query, w_rgate)

    part = functools.partial(
        merge, t=t, fv=fv, gap=gap, shift=shift, starts=starts, offsets=offsets, arrived=arrived,
        head_gain=head_gain[None, :], filtered=filtered, stats=stats_all, conv_gain=conv_gain[None, :],
        w_query=w_query, w_rgate=w_rgate, out_rec=out_rec, out_conv=out_conv,
    )
    add = lambda x, y: (x.astype(F32) + y.astype(F32)).astype(BF16)
    far_top, far_bottom = part(3, slots[3], ready=ready)
    via_back = permuted(far_top, ahead)
    via_front = permuted(far_bottom, behind)
    back_a, front_b = part(1, slots[1])
    got_b = permuted(front_b, ahead)
    got_a = permuted(back_a, behind)
    back_b, front_a = part(2, slots[2])
    sum_a = permuted(add(front_a, via_back), ahead)
    sum_b = permuted(add(back_b, via_front), behind)
    own_a, own_b = part(0, slots[0])
    return finish(own_a, got_a, sum_a, own_b, got_b, sum_b)


def solution(mesh):
    placed = (
        P(("sp", "tp"), None),
        P(),
        P(None, "tp"),
        P(None, "tp"),
        P(None, "tp"),
        P(None, "tp"),
        P(None, "tp"),
        P(None, "tp"),
        P("tp"),
        P("sp", "tp"),
        P(),
        P(None, "tp"),
        P("tp"),
        P("tp", None),
        P("tp", None),
    )
    return jax.shard_map(on_device, mesh=mesh, in_specs=placed, out_specs=P(("sp", "tp"), None), check_vma=False)
```

time: 150 us -> 147 us (0.980)
  the two profiles are of different devices: /device:TPU:8 before, /device:TPU:1 now
where the time goes in v3:
time: 147 us; the launch traced here: 144 us
  Pallas kernels  76.4 us (52%)
  starting transfers between devices  40.4 us (27%)
  local copies, waits for them, and re-layouts  16.5 us (11%)
  waiting for transfers between devices  8.37 us (6%)
  other arithmetic  2.33 us (2%)
    pallas_call x4, Pallas kernels, merge(): pl.pallas_call(functools.partial(merge_kernel, group, split), grid_spec=p...  35.4 us
    ppermute x15, starting transfers between devices, permuted(): return lax.ppermute(value, 'tp', perm)  19.3 us
    pallas_call x4, Pallas kernels, keys(): pl.pallas_call(functools.partial(keys_kernel, first, last), grid_spec=plt...  18.2 us
    unnamed x56, local copies, waits for them, and re-layouts  16.5 us
    pallas_call x1, Pallas kernels, filter_rows(): pl.pallas_call(filter_kernel, grid_spec=pltpu.PrefetchScalarGridSpec(num_...  9.78 us
    all_to_all x1, starting transfers between devices, arriving_states(): lax.all_to_all(arriving, 'sp', split_axis=0, concat_axis=0, tiled=True)  8.23 us
    ppermute x15, waiting for transfers between devices, permuted(): return lax.ppermute(value, 'tp', perm)  8.06 us
    all_to_all x1, starting transfers between devices, arriving_states(): packs = lax.all_to_all(pack, 'sp', split_axis=0, concat_axis=0, tiled=True)  7.93 us
  transfers between devices with their start and end apart: 18, of which 3 were waited for; matrix products, arithmetic and copies ran while one was open for 2% of the time, Pallas kernels for 41%

profile of v3, /device:TPU:1, one launch (start us, length us, event | category | flops | bytes accessed | tf_op | source)
XLA Modules:
  0.0 144.3 jit_solution(5548716977869379076)
XLA Ops:
  0.0 3.2 %norm_rows.1 = (bf16[128,2048]{1,0:T(8,128)(2,1)}, bf16[128,2048]{1,0:T(8,128)(2,1)}) custom-call(bf16[256,2048]{1,0:T(8,128)(2,1)} %tokens.1, f32[1,2048]{1,0:T(1,128)} %bitcast.35), custom_call_target="tpu_custom_call" | custom-call | tf_op jit(solution)/shard_map/norm_rows/pallas_call | solution.py:112
  3.2 2.1 %collective-permute-start = (bf16[128,2048]{1,0:T(8,128)(2,1)}, bf16[128,2048]{1,0:T(8,128)(2,1)}, u32[]{:S(2)}, u32[]{:S(2)}) collective-permute-start(bf16[128,2048]{1,0:T(8,128)(2,1)} %get-tuple-element.38.refs_0_), channel_id=1, source_target_pairs={{0,1},{1,2},{2,3},{3,0},{4,5},{5,6},{6,7},{7,4},{8,9},{9,10},{10,1... | collective-permute-start | bytes 1572872 | tf_op jit(solution)/shard_map/ppermute | solution.py:530
  5.3 1.4 collective-permute-start.2
  6.8 2.6 %collective-permute-start.5 = (bf16[128,2048]{1,0:T(8,128)(2,1)}, bf16[128,2048]{1,0:T(8,128)(2,1)}, u32[]{:S(2)}, u32[]{:S(2)}) collective-permute-start(bf16[128,2048]{1,0:T(8,128)(2,1)} %get-tuple-element.38.refs_0_), channel_id=1, source_target_pairs={{0,3},{1,0},{2,1},{3,2},{4,7},{5,4},{6,5},{7,6},{8,11},{9,8},{10,9... | collective-permute-start | bytes 1572872 | tf_op jit(solution)/shard_map/ppermute | solution.py:530
  9.4 1.6 %copy-done = bf16[2048,512]{1,0:T(8,128)(2,1)S(1)} copy-done((bf16[2048,512]{1,0:T(8,128)(2,1)S(1)}, bf16[2048,512]{1,0:T(8,128)(2,1)}, u32[]{:S(2)}) %copy-start) | copy-done | bytes 2097176
  11.0 1.6 %copy-done.2 = bf16[2048,512]{1,0:T(8,128)(2,1)S(1)} copy-done((bf16[2048,512]{1,0:T(8,128)(2,1)S(1)}, bf16[2048,512]{1,0:T(8,128)(2,1)}, u32[]{:S(2)}) %copy-start.2) | copy-done | bytes 2097176
  12.6 1.6 %copy-done.4 = bf16[2048,512]{1,0:T(8,128)(2,1)S(1)} copy-done((bf16[2048,512]{1,0:T(8,128)(2,1)S(1)}, bf16[2048,512]{1,0:T(8,128)(2,1)}, u32[]{:S(2)}) %copy-start.4) | copy-done | bytes 2097176
  14.2 1.6 %copy-done.6 = bf16[2048,512]{1,0:T(8,128)(2,1)S(1)} copy-done((bf16[2048,512]{1,0:T(8,128)(2,1)S(1)}, bf16[2048,512]{1,0:T(8,128)(2,1)}, u32[]{:S(2)}) %copy-start.6) | copy-done | bytes 2097176
  15.7 0.7 copy-done.10
  16.5 0.7 copy-done.15
  17.1 0.7 copy-done.17
  17.8 1.0 copy-done.20
  18.8 1.0 copy-done.21
  19.9 3.7 %shard_map.154 = (bf16[1024,1024]{1,0:T(8,128)(2,1)S(1)}, bf16[1024,512]{1,0:T(8,128)(2,1)S(1)}, f32[8,4,128,128]{3,2,1,0:T(8,128)S(1)}, f32[8,8,512]{2,1,0:T(8,128)S(1)}) custom-call(s32[1]{0:T(128)} %bitcast.t, s32[64]{0:T(128)S(1)} %copy-done.17, bf16[128,2048]{1,0:T(8,128)(2,1)S(1)} %copy-done.20, bf16[128,2048]{1,0:T(8,128)(2,1)S(1)} %copy-done.21, ...), custom_call_target="tpu_custom_call" | custom-call | flops 3221225472 | bytes 12582912 | tf_op jit(solution)/shard_map/pallas_call | solution.py:235
  23.7 2.7 %collective-permute-start.3 = (bf16[128,2048]{1,0:T(8,128)(2,1)}, bf16[128,2048]{1,0:T(8,128)(2,1)S(1)}, u32[]{:S(2)}, u32[]{:S(2)}) collective-permute-start(bf16[128,2048]{1,0:T(8,128)(2,1)} %collective-permute-done.2.refs_1_), channel_id=1, source_target_pairs={{0,3},{1,0},{2,1},{3,2},{4,7},{5,4},{6,5},{7,6},{8,11},{9,8},{10,9... | collective-permute-start | bytes 1572872 | tf_op jit(solution)/shard_map/ppermute | solution.py:530
  26.4 4.8 %shard_map.155 = (bf16[1024,1024]{1,0:T(8,128)(2,1)S(1)}, bf16[1024,512]{1,0:T(8,128)(2,1)S(1)}, f32[8,4,128,128]{3,2,1,0:T(8,128)S(1)}, f32[8,8,512]{2,1,0:T(8,128)S(1)}) custom-call(s32[1]{0:T(128)} %bitcast.t, s32[64]{0:T(128)S(1)} %copy-done.18, ...), custom_call_target="tpu_custom_call", output_to_operand_aliasing={{0}: (11, {}), {1}: (12, {}), {2}: (13, {}), {3}: (14, {})} | custom-call | flops 3221225472 | bytes 12582912 | tf_op jit(solution)/shard_map/pallas_call | solution.py:235
  31.3 4.8 %shard_map.156 = (bf16[1024,1024]{1,0:T(8,128)(2,1)S(1)}, bf16[1024,512]{1,0:T(8,128)(2,1)S(1)}, f32[8,4,128,128]{3,2,1,0:T(8,128)S(1)}, f32[8,8,512]{2,1,0:T(8,128)S(1)}) custom-call(s32[1]{0:T(128)} %bitcast.t, s32[64]{0:T(128)S(1)} %copy-done.18, ...), custom_call_target="tpu_custom_call", output_to_operand_aliasing={{0}: (11, {}), {1}: (12, {}), {2}: (13, {}), {3}: (14, {})} | custom-call | flops 3221225472 | bytes 12582912 | tf_op jit(solution)/shard_map/pallas_call | solution.py:235
  36.1 4.5 %collective-permute-done.1.refs_0_ = bf16[128,2048]{1,0:T(8,128)(2,1)S(1)} collective-permute-done((bf16[128,2048]{1,0:T(8,128)(2,1)}, bf16[128,2048]{1,0:T(8,128)(2,1)S(1)}, u32[]{:S(2)}, u32[]{:S(2)}) %collective-permute-start.1) | collective-permute-done | bytes 524320 | tf_op jit(solution)/shard_map/ppermute | solution.py:530
  40.6 4.8 %shard_map.157 = (bf16[1024,1024]{1,0:T(8,128)(2,1)S(1)}, bf16[1024,512]{1,0:T(8,128)(2,1)S(1)}, bf16[32,24,128]{2,1,0:T(8,128)(2,1)}, bf16[8,4,128,128]{3,2,1,0...) custom-call(s32[1]{0:T(128)} %bitcast.t, ...), custom_call_target="tpu_custom_call", output_to_operand_aliasing={{0}: (11, {}), {1}: (12, {})} | custom-call | flops 3221225472 | bytes 12582912 | tf_op jit(solution)/shard_map/pallas_call | solution.py:235
  45.4 1.0 copy-done.9
  46.4 1.0 copy-done.19
  47.4 0.7 copy-done.22
  48.0 4.9 %collective-permute-start.6 = (bf16[32,512]{1,0:T(8,128)(2,1)S(1)}, bf16[32,512]{1,0:T(8,128)(2,1)S(1)}, u32[]{:S(2)}, u32[]{:S(2)}) collective-permute-start(bf16[32,512]{1,0:T(8,128)(2,1)S(1)} %get-tuple-element.57), channel_id=1, source_target_pairs={{0,4},{4,8},{8,12},{12,16},{16,20},{20,24},{24,28},{28,32},{32,36}... | collective-permute-start | bytes 98312 | tf_op jit(solution)/shard_map/ppermute | solution.py:569
  52.9 7.9 %all-to-all-start = ((bf16[32,24,128]{2,1,0:T(8,128)(2,1)}), bf16[32,24,128]{2,1,0:T(8,128)(2,1)S(1)}, u32[]{:S(2)}, u32[]{:S(2)}) async-start(bf16[32,24,128]{2,1,0:T(8,128)(2,1)} %get-tuple-element.55), calls=%async_computation | async-start | bytes 393216 | tf_op jit(solution)/shard_map/all_to_all | solution.py:267
  60.9 0.6 copy-done.27
  61.5 9.8 %filter_rows.1 = (f32[1024,512]{1,0:T(8,128)}, f32[8,1024]{1,0:T(8,128)}) custom-call(s32[1]{0:T(128)} %bitcast.t, s32[64]{0:T(128)} %constant.6.clone.places, bf16[1024,512]{1,0:T(8,128)(2,1)} %copy-done.9, bf16[32,512]{1,0:T(8,128)(2,1)} %copy-done.27, f32[31,512]{1,0:T(8,128)} %taps.1), custom_call_target="tpu_custom_call" | custom-call | flops 7000000000 | bytes 5242880 | tf_op jit(solution)/shard_map/filter_rows/pallas_call | solution.py:322
  71.3 1.2 collective-permute-start.7
  72.5 2.6 %collective-permute-start.8 = (f32[8,1024]{1,0:T(8,128)}, f32[8,1024]{1,0:T(8,128)S(1)}, u32[]{:S(2)}, u32[]{:S(2)}) collective-permute-start(f32[8,1024]{1,0:T(8,128)} %get-tuple-element.59.refs_12_.refs_7_), channel_id=1, source_target_pairs={{0,2},{1,3},{2,0},{3,1},{4,6},{5,7},{6,4},{7,5},{8,10},{9,11},{10,... | collective-permute-start | bytes 98312 | tf_op jit(solution)/shard_map/ppermute | solution.py:530
  75.1 0.7 collective-permute-start.9
  75.8 0.7 prefix.1
  76.5 8.2 %all-to-all-start.1 = ((bf16[32,16,128]{2,1,0:T(8,128)(2,1)}), bf16[32,16,128]{2,1,0:T(8,128)(2,1)S(1)}, u32[]{:S(2)}, u32[]{:S(2)}) async-start(bf16[32,16,128]{2,1,0:T(8,128)(2,1)} %prefix.1), calls=%async_computation.1 | async-start | bytes 262144 | tf_op jit(solution)/shard_map/all_to_all | solution.py:275
  84.8 7.2 %shard_map.161 = (f32[256,512]{1,0:T(8,128)}, bf16[256,512]{1,0:T(8,128)(2,1)}, bf16[256,512]{1,0:T(8,128)(2,1)}) custom-call(s32[1]{0:T(128)} %bitcast.t, s32[64]{0:T(128)} %constant.6.clone.places, bf16[128,2048]{1,0:T(8,128)(2,1)} %copy-done.11, bf16[128,2048]{1,0:T(8,128)(2,1)} %copy-done.12, bf16[1024,1024]{1,0:T(8,128)(2,1)} %copy-done.8, ...), custom_call_target="tpu_custom_call" | custom-call | flops 2147483648 | bytes 6291456 | tf_op jit(solution)/shard_map/pallas_call | solution.py:398
  92.0 0.3 all-to-all-done.1
  92.3 0.3 copy-done.24
  92.6 0.3 copy-done.23
  93.0 7.1 %shard_map.162 = (bf16[128,2048]{1,0:T(8,128)(2,1)}, bf16[128,2048]{1,0:T(8,128)(2,1)}) custom-call(s32[1]{0:T(128)} %bitcast.t, s32[64]{0:T(128)} %constant.6.clone.places, f32[256,512]{1,0:T(8,128)} %get-tuple-element.63.refs_0_, bf16[256,512]{1,0:T(8,128)(2,1)} %get-tuple-element.64.refs_1_, bf16[256,512]{1,0:T(8,128)(2,1)} %get-tuple-element.65.refs_2_, ...), custom_call_target="tpu_custom_call" | custom-call | flops 6442450944 | bytes 10485760 | tf_op jit(solution)/shard_map/pallas_call | solution.py:493
  100.2 1.5 %collective-permute-start.11 = (bf16[128,2048]{1,0:T(8,128)(2,1)}, bf16[128,2048]{1,0:T(8,128)(2,1)S(1)}, u32[]{:S(2)}, u32[]{:S(2)}) collective-permute-start(bf16[128,2048]{1,0:T(8,128)(2,1)} %get-tuple-element.66), channel_id=1, source_target_pairs={{0,1},{1,2},{2,3},{3,0},{4,5},{5,6},{6,7},{7,4},{8,9},{9,10},{10,1... | collective-permute-start | bytes 1572872 | tf_op jit(solution)/shard_map/ppermute | solution.py:530
  101.7 9.4 %shard_map.159 = (bf16[128,2048]{1,0:T(8,128)(2,1)}, bf16[128,2048]{1,0:T(8,128)(2,1)}) custom-call(s32[1]{0:T(128)} %bitcast.t, s32[64]{0:T(128)} %constant.6.clone.places, bf16[128,2048]{1,0:T(8,128)(2,1)} %collective-permute-done.refs_0_, bf16[128,2048]{1,0:T(8,128)(2,1)} %collective-permute-done.2.refs_1_, bf16[1024,1024]{1,0:T(8,128)(2,1)} %copy-done.8, ...), custom_call_target="tpu_custom_call" | custom-call | flops 6442450944 | bytes 10485760 | tf_op jit(solution)/shard_map/pallas_call | solution.py:493
  111.1 1.4 collective-permute-start.10
  112.6 9.4 %shard_map.160 = (bf16[128,2048]{1,0:T(8,128)(2,1)}, bf16[128,2048]{1,0:T(8,128)(2,1)}) custom-call(s32[1]{0:T(128)} %bitcast.t, s32[64]{0:T(128)} %constant.6.clone.places, bf16[128,2048]{1,0:T(8,128)(2,1)} %collective-permute-done.4.refs_0_, bf16[128,2048]{1,0:T(8,128)(2,1)} %collective-permute-done.5.refs_1_, bf16[1024,1024]{1,0:T(8,128)(2,1)} %copy-done.8, ...), custom_call_target="tpu_custom_call" | custom-call | flops 6442450944 | bytes 10485760 | tf_op jit(solution)/shard_map/pallas_call | solution.py:493
  122.1 1.2 add_convert_fusion
  123.2 2.8 %collective-permute-start.15 = (bf16[128,2048]{1,0:T(8,128)(2,1)S(1)}, bf16[128,2048]{1,0:T(8,128)(2,1)S(1)}, u32[]{:S(2)}, u32[]{:S(2)}) collective-permute-start(bf16[128,2048]{1,0:T(8,128)(2,1)S(1)} %add_convert_fusion), channel_id=1, source_target_pairs={{0,3},{1,0},{2,1},{3,2},{4,7},{5,4},{6,5},{7,6},{8,11},{9,8},{10,9... | collective-permute-start | bytes 1572872 | tf_op jit(solution)/shard_map/ppermute | solution.py:530
  126.1 1.2 add_convert_fusion.1
  127.3 9.4 %shard_map.158 = (bf16[128,2048]{1,0:T(8,128)(2,1)}, bf16[128,2048]{1,0:T(8,128)(2,1)}) custom-call(s32[1]{0:T(128)} %bitcast.t, s32[64]{0:T(128)} %constant.6.clone.places, bf16[128,2048]{1,0:T(8,128)(2,1)} %get-tuple-element.38.refs_0_, bf16[128,2048]{1,0:T(8,128)(2,1)} %get-tuple-element.39.refs_1_, bf16[1024,1024]{1,0:T(8,128)(2,1)} %copy-done.8, ...), custom_call_target="tpu_custom_call" | custom-call | flops 6442450944 | bytes 10485760 | tf_op jit(solution)/shard_map/pallas_call | solution.py:493
  136.8 3.6 %collective-permute-done.12.sum_a = bf16[128,2048]{1,0:T(8,128)(2,1)S(1)} collective-permute-done((bf16[128,2048]{1,0:T(8,128)(2,1)S(1)}, bf16[128,2048]{1,0:T(8,128)(2,1)S(1)}, u32[]{:S(2)}, u32[]{:S(2)}) %collective-permute-start.12) | collective-permute-done | bytes 524320 | tf_op jit(solution)/shard_map/ppermute | solution.py:530
  140.3 1.0 copy-done.13
  141.4 1.0 copy-done.14
  142.4 1.9 %finish.1 = bf16[256,2048]{1,0:T(8,128)(2,1)} custom-call(bf16[128,2048]{1,0:T(8,128)(2,1)S(1)} %copy-done.13, bf16[128,2048]{1,0:T(8,128)(2,1)S(1)} %collective-permute-done.10.got_a, bf16[128,2048]{1,0:T(8,128)(2,1)S(1)} %collective-permute-done.12.sum_a, bf16[128,2048]{1,0:T(8,128)(2,1)S(1)} %copy-done.14, ...), custom_call_target="tpu_custom_call" | custom-call | tf_op jit(solution)/shard_map/finish/pallas_call | solution.py:518
  (59 shorter events, 0.7 us)
Async XLA Ops:
  3.2 20.4 %collective-permute-start = (bf16[128,2048]{1,0:T(8,128)(2,1)}, bf16[128,2048]{1,0:T(8,128)(2,1)}, u32[]{:S(2)}, u32[]{:S(2)}) collective-permute-start(bf16[128,2048]{1,0:T(8,128)(2,1)} %get-tuple-element.38.refs_0_), channel_id=1, source_target_pairs={{0,1},{1,2},{2,3},{3,0},{4,5},{5,6},{6,7},{7,4},{8,9},{9,10},{10,1... | collective-permute-start | bytes 1572872 | tf_op jit(solution)/shard_map/ppermute | solution.py:530
  5.3 18.4 %collective-permute-start.2 = (bf16[128,2048]{1,0:T(8,128)(2,1)}, bf16[128,2048]{1,0:T(8,128)(2,1)}, u32[]{:S(2)}, u32[]{:S(2)}) collective-permute-start(bf16[128,2048]{1,0:T(8,128)(2,1)} %get-tuple-element.39.refs_1_), channel_id=1, source_target_pairs={{0,3},{1,0},{2,1},{3,2},{4,7},{5,4},{6,5},{7,6},{8,11},{9,8},{10,9... | collective-permute-start | bytes 1572872 | tf_op jit(solution)/shard_map/ppermute | solution.py:530
  6.7 24.6 %collective-permute-start.4 = (bf16[128,2048]{1,0:T(8,128)(2,1)}, bf16[128,2048]{1,0:T(8,128)(2,1)}, u32[]{:S(2)}, u32[]{:S(2)}) collective-permute-start(bf16[128,2048]{1,0:T(8,128)(2,1)} %get-tuple-element.39.refs_1_), channel_id=1, source_target_pairs={{0,1},{1,2},{2,3},{3,0},{4,5},{5,6},{6,7},{7,4},{8,9},{9,10},{10,1... | collective-permute-start | bytes 1572872 | tf_op jit(solution)/shard_map/ppermute | solution.py:530
  6.8 24.4 %collective-permute-start.5 = (bf16[128,2048]{1,0:T(8,128)(2,1)}, bf16[128,2048]{1,0:T(8,128)(2,1)}, u32[]{:S(2)}, u32[]{:S(2)}) collective-permute-start(bf16[128,2048]{1,0:T(8,128)(2,1)} %get-tuple-element.38.refs_0_), channel_id=1, source_target_pairs={{0,3},{1,0},{2,1},{3,2},{4,7},{5,4},{6,5},{7,6},{8,11},{9,8},{10,9... | collective-permute-start | bytes 1572872 | tf_op jit(solution)/shard_map/ppermute | solution.py:530
  9.4 1.6 %copy-start = (bf16[2048,512]{1,0:T(8,128)(2,1)S(1)}, bf16[2048,512]{1,0:T(8,128)(2,1)}, u32[]{:S(2)}) copy-start(bf16[2048,512]{1,0:T(8,128)(2,1)} %refs_5_.7) | copy-start | bytes 6291460
  11.0 1.6 %copy-start.2 = (bf16[2048,512]{1,0:T(8,128)(2,1)S(1)}, bf16[2048,512]{1,0:T(8,128)(2,1)}, u32[]{:S(2)}) copy-start(bf16[2048,512]{1,0:T(8,128)(2,1)} %refs_6_.7) | copy-start | bytes 6291460
  12.6 1.6 %copy-start.4 = (bf16[2048,512]{1,0:T(8,128)(2,1)S(1)}, bf16[2048,512]{1,0:T(8,128)(2,1)}, u32[]{:S(2)}) copy-start(bf16[2048,512]{1,0:T(8,128)(2,1)} %refs_7_.7) | copy-start | bytes 6291460
  14.2 1.6 %copy-start.6 = (bf16[2048,512]{1,0:T(8,128)(2,1)S(1)}, bf16[2048,512]{1,0:T(8,128)(2,1)}, u32[]{:S(2)}) copy-start(bf16[2048,512]{1,0:T(8,128)(2,1)} %refs_8_.7) | copy-start | bytes 6291460
  15.7 0.7 copy-start.10
  16.5 0.7 copy-start.15
  17.1 0.7 copy-start.17
  17.8 1.0 copy-start.20
  18.8 1.0 copy-start.21
  19.9 6.5 %copy-start.1 = (bf16[2048,512]{1,0:T(8,128)(2,1)S(1)}, bf16[2048,512]{1,0:T(8,128)(2,1)}, u32[]{:S(2)}) copy-start(bf16[2048,512]{1,0:T(8,128)(2,1)} %refs_5_.7) | copy-start | bytes 6291460
  19.9 6.5 %copy-start.3 = (bf16[2048,512]{1,0:T(8,128)(2,1)S(1)}, bf16[2048,512]{1,0:T(8,128)(2,1)}, u32[]{:S(2)}) copy-start(bf16[2048,512]{1,0:T(8,128)(2,1)} %refs_6_.7) | copy-start | bytes 6291460
  19.9 6.5 %copy-start.5 = (bf16[2048,512]{1,0:T(8,128)(2,1)S(1)}, bf16[2048,512]{1,0:T(8,128)(2,1)}, u32[]{:S(2)}) copy-start(bf16[2048,512]{1,0:T(8,128)(2,1)} %refs_7_.7) | copy-start | bytes 6291460
  19.9 6.5 %copy-start.7 = (bf16[2048,512]{1,0:T(8,128)(2,1)S(1)}, bf16[2048,512]{1,0:T(8,128)(2,1)}, u32[]{:S(2)}) copy-start(bf16[2048,512]{1,0:T(8,128)(2,1)} %refs_8_.7) | copy-start | bytes 6291460
  19.9 6.5 %copy-start.16 = (f32[512]{0:T(512)S(1)}, f32[512]{0:T(512)}, u32[]{:S(2)}) copy-start(f32[512]{0:T(512)} %param.24) | copy-start | bytes 6148
  19.9 6.5 %copy-start.18 = (s32[64]{0:T(128)S(1)}, s32[64]{0:T(128)}, u32[]{:S(2)}) copy-start(s32[64]{0:T(128)} %constant.6.clone.places) | copy-start | bytes 772
  23.6 16.9 %collective-permute-start.1 = (bf16[128,2048]{1,0:T(8,128)(2,1)}, bf16[128,2048]{1,0:T(8,128)(2,1)S(1)}, u32[]{:S(2)}, u32[]{:S(2)}) collective-permute-start(bf16[128,2048]{1,0:T(8,128)(2,1)} %collective-permute-done.refs_0_), channel_id=1, source_target_pairs={{0,1},{1,2},{2,3},{3,0},{4,5},{5,6},{6,7},{7,4},{8,9},{9,10},{10,1... | collective-permute-start | bytes 1572872 | tf_op jit(solution)/shard_map/ppermute | solution.py:530
  23.7 16.8 %collective-permute-start.3 = (bf16[128,2048]{1,0:T(8,128)(2,1)}, bf16[128,2048]{1,0:T(8,128)(2,1)S(1)}, u32[]{:S(2)}, u32[]{:S(2)}) collective-permute-start(bf16[128,2048]{1,0:T(8,128)(2,1)} %collective-permute-done.2.refs_1_), channel_id=1, source_target_pairs={{0,3},{1,0},{2,1},{3,2},{4,7},{5,4},{6,5},{7,6},{8,11},{9,8},{10,9... | collective-permute-start | bytes 1572872 | tf_op jit(solution)/shard_map/ppermute | solution.py:530
  40.6 4.8 %copy-start.11 = (bf16[128,2048]{1,0:T(8,128)(2,1)}, bf16[128,2048]{1,0:T(8,128)(2,1)S(1)}, u32[]{:S(2)}) copy-start(bf16[128,2048]{1,0:T(8,128)(2,1)S(1)} %collective-permute-done.1.refs_0_) | copy-start | bytes 1572868
  40.6 4.9 %copy-start.12 = (bf16[128,2048]{1,0:T(8,128)(2,1)}, bf16[128,2048]{1,0:T(8,128)(2,1)S(1)}, u32[]{:S(2)}) copy-start(bf16[128,2048]{1,0:T(8,128)(2,1)S(1)} %collective-permute-done.3.refs_1_) | copy-start | bytes 1572868
  45.4 1.0 copy-start.9
  46.4 1.0 copy-start.19
  47.4 0.7 copy-start.22
  48.0 23.2 %copy-start.8 = (bf16[1024,1024]{1,0:T(8,128)(2,1)}, bf16[1024,1024]{1,0:T(8,128)(2,1)S(1)}, u32[]{:S(2)}) copy-start(bf16[1024,1024]{1,0:T(8,128)(2,1)S(1)} %get-tuple-element.52.refs_2_) | copy-start | bytes 6291460
  48.0 12.8 %collective-permute-start.6 = (bf16[32,512]{1,0:T(8,128)(2,1)S(1)}, bf16[32,512]{1,0:T(8,128)(2,1)S(1)}, u32[]{:S(2)}, u32[]{:S(2)}) collective-permute-start(bf16[32,512]{1,0:T(8,128)(2,1)S(1)} %get-tuple-element.57), channel_id=1, source_target_pairs={{0,4},{4,8},{8,12},{12,16},{16,20},{20,24},{24,28},{28,32},{32,36}... | collective-permute-start | bytes 98312 | tf_op jit(solution)/shard_map/ppermute | solution.py:569
  52.9 22.9 %all-to-all-start = ((bf16[32,24,128]{2,1,0:T(8,128)(2,1)}), bf16[32,24,128]{2,1,0:T(8,128)(2,1)S(1)}, u32[]{:S(2)}, u32[]{:S(2)}) async-start(bf16[32,24,128]{2,1,0:T(8,128)(2,1)} %get-tuple-element.55), calls=%async_computation | async-start | bytes 393216 | tf_op jit(solution)/shard_map/all_to_all | solution.py:267
  60.9 0.6 copy-start.27
  71.3 20.7 %collective-permute-start.7 = (f32[8,1024]{1,0:T(8,128)}, f32[8,1024]{1,0:T(8,128)S(1)}, u32[]{:S(2)}, u32[]{:S(2)}) collective-permute-start(f32[8,1024]{1,0:T(8,128)} %get-tuple-element.59.refs_12_.refs_7_), channel_id=1, source_target_pairs={{0,1},{1,2},{2,3},{3,0},{4,5},{5,6},{6,7},{7,4},{8,9},{9,10},{10,1... | collective-permute-start | bytes 98312 | tf_op jit(solution)/shard_map/ppermute | solution.py:530
  72.5 19.5 %collective-permute-start.8 = (f32[8,1024]{1,0:T(8,128)}, f32[8,1024]{1,0:T(8,128)S(1)}, u32[]{:S(2)}, u32[]{:S(2)}) collective-permute-start(f32[8,1024]{1,0:T(8,128)} %get-tuple-element.59.refs_12_.refs_7_), channel_id=1, source_target_pairs={{0,2},{1,3},{2,0},{3,1},{4,6},{5,7},{6,4},{7,5},{8,10},{9,11},{10,... | collective-permute-start | bytes 98312 | tf_op jit(solution)/shard_map/ppermute | solution.py:530
  75.1 16.9 %collective-permute-start.9 = (f32[8,1024]{1,0:T(8,128)}, f32[8,1024]{1,0:T(8,128)S(1)}, u32[]{:S(2)}, u32[]{:S(2)}) collective-permute-start(f32[8,1024]{1,0:T(8,128)} %get-tuple-element.59.refs_12_.refs_7_), channel_id=1, source_target_pairs={{0,3},{1,0},{2,1},{3,2},{4,7},{5,4},{6,5},{7,6},{8,11},{9,8},{10,9... | collective-permute-start | bytes 98312 | tf_op jit(solution)/shard_map/ppermute | solution.py:530
  76.5 15.8 %all-to-all-start.1 = ((bf16[32,16,128]{2,1,0:T(8,128)(2,1)}), bf16[32,16,128]{2,1,0:T(8,128)(2,1)S(1)}, u32[]{:S(2)}, u32[]{:S(2)}) async-start(bf16[32,16,128]{2,1,0:T(8,128)(2,1)} %prefix.1), calls=%async_computation.1 | async-start | bytes 262144 | tf_op jit(solution)/shard_map/all_to_all | solution.py:275
  92.0 0.6 copy-start.24
  92.0 0.6 copy-start.25
  92.0 0.6 copy-start.26
  92.3 0.6 copy-start.23
  100.1 21.9 %collective-permute-start.14 = (bf16[128,2048]{1,0:T(8,128)(2,1)}, bf16[128,2048]{1,0:T(8,128)(2,1)S(1)}, u32[]{:S(2)}, u32[]{:S(2)}) collective-permute-start(bf16[128,2048]{1,0:T(8,128)(2,1)} %get-tuple-element.70), channel_id=1, source_target_pairs={{0,3},{1,0},{2,1},{3,2},{4,7},{5,4},{6,5},{7,6},{8,11},{9,8},{10,9... | collective-permute-start | bytes 1572872 | tf_op jit(solution)/shard_map/ppermute | solution.py:530
  100.2 25.9 %collective-permute-start.11 = (bf16[128,2048]{1,0:T(8,128)(2,1)}, bf16[128,2048]{1,0:T(8,128)(2,1)S(1)}, u32[]{:S(2)}, u32[]{:S(2)}) collective-permute-start(bf16[128,2048]{1,0:T(8,128)(2,1)} %get-tuple-element.66), channel_id=1, source_target_pairs={{0,1},{1,2},{2,3},{3,0},{4,5},{5,6},{6,7},{7,4},{8,9},{9,10},{10,1... | collective-permute-start | bytes 1572872 | tf_op jit(solution)/shard_map/ppermute | solution.py:530
  111.1 25.7 %collective-permute-start.10 = (bf16[128,2048]{1,0:T(8,128)(2,1)}, bf16[128,2048]{1,0:T(8,128)(2,1)S(1)}, u32[]{:S(2)}, u32[]{:S(2)}) collective-permute-start(bf16[128,2048]{1,0:T(8,128)(2,1)} %get-tuple-element.61), channel_id=1, source_target_pairs={{0,3},{1,0},{2,1},{3,2},{4,7},{5,4},{6,5},{7,6},{8,11},{9,8},{10,9... | collective-permute-start | bytes 1572872 | tf_op jit(solution)/shard_map/ppermute | solution.py:530
  112.4 24.3 %collective-permute-start.13 = (bf16[128,2048]{1,0:T(8,128)(2,1)}, bf16[128,2048]{1,0:T(8,128)(2,1)S(1)}, u32[]{:S(2)}, u32[]{:S(2)}) collective-permute-start(bf16[128,2048]{1,0:T(8,128)(2,1)} %get-tuple-element.68), channel_id=1, source_target_pairs={{0,1},{1,2},{2,3},{3,0},{4,5},{5,6},{6,7},{7,4},{8,9},{9,10},{10,1... | collective-permute-start | bytes 1572872 | tf_op jit(solution)/shard_map/ppermute | solution.py:530
  123.2 13.5 %collective-permute-start.15 = (bf16[128,2048]{1,0:T(8,128)(2,1)S(1)}, bf16[128,2048]{1,0:T(8,128)(2,1)S(1)}, u32[]{:S(2)}, u32[]{:S(2)}) collective-permute-start(bf16[128,2048]{1,0:T(8,128)(2,1)S(1)} %add_convert_fusion), channel_id=1, source_target_pairs={{0,3},{1,0},{2,1},{3,2},{4,7},{5,4},{6,5},{7,6},{8,11},{9,8},{10,9... | collective-permute-start | bytes 1572872 | tf_op jit(solution)/shard_map/ppermute | solution.py:530
  127.2 13.1 %collective-permute-start.12 = (bf16[128,2048]{1,0:T(8,128)(2,1)S(1)}, bf16[128,2048]{1,0:T(8,128)(2,1)S(1)}, u32[]{:S(2)}, u32[]{:S(2)}) collective-permute-start(bf16[128,2048]{1,0:T(8,128)(2,1)S(1)} %add_convert_fusion.1), channel_id=1, source_target_pairs={{0,1},{1,2},{2,3},{3,0},{4,5},{5,6},{6,7},{7,4},{8,9},{9,10},{10,1... | collective-permute-start | bytes 1572872 | tf_op jit(solution)/shard_map/ppermute | solution.py:530
  140.3 1.0 copy-start.13
  141.4 1.0 copy-start.14

commit v4 on v3

--- a/solution.py
+++ b/solution.py
@@ -33,8 +33,11 @@
     return places[16 * t[0] + 8 + block]
 
 
-def params(mib=8, **kw):
-    return pltpu.CompilerParams(vmem_limit_bytes=mib * 1024 * 1024, **kw)
+LIMITS = {"norm": 8, "keys": 28, "last": 28, "filter": 58, "prefix": 50, "query": 58, "merge_3": 16, "merge": 24, "merge_0": 24}
+
+
+def params(kind):
+    return pltpu.CompilerParams(vmem_limit_bytes=LIMITS[kind] * 1024 * 1024)
 
 
 def dot(a, b, dims=((1,), (0,))):
@@ -114,7 +117,7 @@
         in_specs=[hbm_spec(), pl.BlockSpec(gain.shape, lambda: (0, 0))],
         out_shape=[half, half],
         scratch_shapes=[pltpu.VMEM(tokens.shape, BF16), pltpu.SemaphoreType.DMA((2,))],
-        compiler_params=params(58),
+        compiler_params=params("norm"),
         name="norm_rows",
     )(tokens, gain)
 
@@ -247,7 +250,7 @@
         ),
         out_shape=out_shape,
         input_output_aliases={11 + k: k for k in range(aliased)},
-        compiler_params=params(28),
+        compiler_params=params("last" if last else "keys"),
         cost_estimate=pl.CostEstimate(
             flops=2 * rows * depth * WIDE * 6, bytes_accessed=12 * 2**20, transcendentals=0
         ),
@@ -268,7 +271,7 @@
     arriving = pl.pallas_call(
         prefix_kernel,
         out_shape=jax.ShapeDtypeStruct((32, 16, HEAD), BF16),
-        compiler_params=params(),
+        compiler_params=params("prefix"),
         cost_estimate=pl.CostEstimate(flops=10**8, bytes_accessed=2**20, transcendentals=0),
         name="prefix",
     )(packs)
@@ -339,7 +342,7 @@
             jax.ShapeDtypeStruct((8 * BLK, WIDE), F32),
             jax.ShapeDtypeStruct((8, 8 * BLK), F32),
         ],
-        compiler_params=params(58),
+        compiler_params=params("filter"),
         cost_estimate=pl.CostEstimate(flops=7 * 10**9, bytes_accessed=5 * 2**20, transcendentals=0),
         name="filter_rows",
     )(t, jnp.asarray(PLACES), mixed, halo, taps)
@@ -405,7 +408,7 @@
             scratch_shapes=[pltpu.VMEM(*v) for v in QUERY_SCRATCH] + [pltpu.SemaphoreType.DMA((5,))],
         ),
         out_shape=[jax.ShapeDtypeStruct((2 * BLK, WIDE), kind) for kind in (F32, BF16, BF16)],
-        compiler_params=params(58),
+        compiler_params=params("query"),
         cost_estimate=pl.CostEstimate(
             flops=2 * 2 * BLK * 2048 * WIDE * 4, bytes_accessed=6 * 2**20, transcendentals=0
         ),
@@ -500,30 +503,11 @@
             scratch_shapes=scratch,
         ),
         out_shape=[jax.ShapeDtypeStruct((BLK, width), BF16)] * 2,
-        compiler_params=params(58),
+        compiler_params=params({3: "merge_3", 0: "merge_0"}.get(group, "merge")),
         cost_estimate=pl.CostEstimate(
             flops=2 * 2 * BLK * 1024 * 2048 * 6, bytes_accessed=10 * 2**20, transcendentals=0
         ),
     )(t, jnp.asarray(PLACES), *lead, starts, offsets, arrived, filtered, *stats, out_rec, out_conv, head_gain, conv_gain)
-
-
-def finish_kernel(own_a, got_a, sum_a, own_b, got_b, sum_b, out):
-    for k, parts in enumerate(((own_a, got_a, sum_a), (own_b, got_b, sum_b))):
-        total = sum(p[...].astype(F32) for p in parts[1:]) + parts[0][...].astype(F32)
-        out[k * BLK : (k + 1) * BLK, :] = total.astype(BF16)
-
-
-def finish(*parts):
-    width = parts[0].shape[1]
-    return pl.pallas_call(
-        finish_kernel,
-        grid=(4,),
-        in_specs=[pl.BlockSpec((BLK, width // 4), lambda n: (0, n))] * 6,
-        out_specs=pl.BlockSpec((2 * BLK, width // 4), lambda n: (0, n)),
-        out_shape=jax.ShapeDtypeStruct((2 * BLK, width), BF16),
-        compiler_params=params(),
-        name="finish",
-    )(*parts)
 
 
 def permuted(value, perm):
@@ -588,7 +572,10 @@
     sum_a = permuted(add(front_a, via_back), ahead)
     sum_b = permuted(add(back_b, via_front), behind)
     own_a, own_b = part(0, slots[0])
-    return finish(own_a, got_a, sum_a, own_b, got_b, sum_b)
+    wide = lambda x: x.astype(F32)
+    ready = jnp.concatenate([wide(own_a) + wide(got_a), wide(own_b) + wide(got_b)], axis=0)
+    ready = lax.optimization_barrier(ready)
+    return (ready + wide(jnp.concatenate([sum_a, sum_b], axis=0))).astype(BF16)
 
 
 def solution(mesh):

time: 147 us -> 146 us (level)
  Pallas kernels: 76.4 us -> 65.1 us
  waiting for transfers between devices: 8.37 us -> 15 us
  local copies, waits for them, and re-layouts: 16.5 us -> 19.1 us
    pallas_call x4, Pallas kernels: 35.4 us -> 26 us  [merge(): pl.pallas_call(functools.partial(merge_kernel, group, split), grid_spec=p...]
    ppermute x15, waiting for transfers between devices: 8.06 us -> 15 us  [permuted(): return lax.ppermute(value, 'tp', perm)]
    unnamed x56 -> x78, local copies, waits for them, and re-layouts: 16.5 us -> 19.1 us
    convert_element_type x2, other arithmetic: 2.33 us -> 0.26 us  [on_device(): add = lambda x, y: (x.astype(F32) + y.astype(F32)).astype(BF16)]
    pallas_call x1 -> x0, Pallas kernels: 1.91 us -> none  [finish(): pl.pallas_call(finish_kernel, grid=(4,), in_specs=[pl.BlockSpec((BLK, wid...]
    pallas_call x1, Pallas kernels: 3.24 us -> 1.57 us  [norm_rows(): pl.pallas_call(norm_kernel, in_specs=[hbm_spec(), pl.BlockSpec(gain.shape...]
  transfers between devices with their start and end apart: 18 -> 18, of which waited for: 3 -> 2; matrix products, arithmetic and copies ran while one was open for 2% -> 0% of each run, Pallas kernels for 41% -> 39%
where the time goes in v4:
time: 146 us; the launch traced here: 143 us
  Pallas kernels  65.1 us (45%)
  starting transfers between devices  41.5 us (28%)
  local copies, waits for them, and re-layouts  19.1 us (13%)
  waiting for transfers between devices  15 us (10%)
  other arithmetic  2.01 us (1%)
    pallas_call x4, Pallas kernels, merge(): pl.pallas_call(functools.partial(merge_kernel, group, split), grid_spec=p...  26 us
    ppermute x15, starting transfers between devices, permuted(): return lax.ppermute(value, 'tp', perm)  20.5 us
    pallas_call x4, Pallas kernels, keys(): pl.pallas_call(functools.partial(keys_kernel, first, last), grid_spec=plt...  19.6 us
    unnamed x78, local copies, waits for them, and re-layouts  19.1 us
    ppermute x15, waiting for transfers between devices, permuted(): return lax.ppermute(value, 'tp', perm)  15 us
    pallas_call x1, Pallas kernels, filter_rows(): pl.pallas_call(filter_kernel, grid_spec=pltpu.PrefetchScalarGridSpec(num_...  9.78 us
    all_to_all x1, starting transfers between devices, arriving_states(): lax.all_to_all(arriving, 'sp', split_axis=0, concat_axis=0, tiled=True)  8.23 us
    all_to_all x1, starting transfers between devices, arriving_states(): packs = lax.all_to_all(pack, 'sp', split_axis=0, concat_axis=0, tiled=True)  7.93 us
  transfers between devices with their start and end apart: 18, of which 2 were waited for; matrix products, arithmetic and copies ran while one was open for 0% of the time, Pallas kernels for 39%

profile of v4, /device:TPU:1, one launch (start us, length us, event | category | flops | bytes accessed | tf_op | source)
XLA Modules:
  0.0 143.2 jit_solution(7315296701758914787)
XLA Ops:
  0.0 1.2 copy-done.11
  1.2 0.7 copy-done.19
  1.9 1.6 %norm_rows.1 = (bf16[128,2048]{1,0:T(8,128)(2,1)}, bf16[128,2048]{1,0:T(8,128)(2,1)}) custom-call(bf16[256,2048]{1,0:T(8,128)(2,1)S(1)} %copy-done.11, f32[1,2048]{1,0:T(1,128)S(1)} %bitcast.35), custom_call_target="tpu_custom_call" | custom-call | tf_op jit(solution)/shard_map/norm_rows/pallas_call | solution.py:115
  3.5 2.1 %collective-permute-start = (bf16[128,2048]{1,0:T(8,128)(2,1)}, bf16[128,2048]{1,0:T(8,128)(2,1)}, u32[]{:S(2)}, u32[]{:S(2)}) collective-permute-start(bf16[128,2048]{1,0:T(8,128)(2,1)} %get-tuple-element.38.refs_0_), channel_id=1, source_target_pairs={{0,1},{1,2},{2,3},{3,0},{4,5},{5,6},{6,7},{7,4},{8,9},{9,10},{10,1... | collective-permute-start | bytes 1572872 | tf_op jit(solution)/shard_map/ppermute | solution.py:514
  5.6 1.4 collective-permute-start.2
  7.1 2.6 %collective-permute-start.5 = (bf16[128,2048]{1,0:T(8,128)(2,1)}, bf16[128,2048]{1,0:T(8,128)(2,1)}, u32[]{:S(2)}, u32[]{:S(2)}) collective-permute-start(bf16[128,2048]{1,0:T(8,128)(2,1)} %get-tuple-element.38.refs_0_), channel_id=1, source_target_pairs={{0,3},{1,0},{2,1},{3,2},{4,7},{5,4},{6,5},{7,6},{8,11},{9,8},{10,9... | collective-permute-start | bytes 1572872 | tf_op jit(solution)/shard_map/ppermute | solution.py:514
  9.6 1.6 %copy-done = bf16[2048,512]{1,0:T(8,128)(2,1)S(1)} copy-done((bf16[2048,512]{1,0:T(8,128)(2,1)S(1)}, bf16[2048,512]{1,0:T(8,128)(2,1)}, u32[]{:S(2)}) %copy-start) | copy-done | bytes 2097176
  11.2 1.6 %copy-done.2 = bf16[2048,512]{1,0:T(8,128)(2,1)S(1)} copy-done((bf16[2048,512]{1,0:T(8,128)(2,1)S(1)}, bf16[2048,512]{1,0:T(8,128)(2,1)}, u32[]{:S(2)}) %copy-start.2) | copy-done | bytes 2097176
  12.8 1.6 %copy-done.4 = bf16[2048,512]{1,0:T(8,128)(2,1)S(1)} copy-done((bf16[2048,512]{1,0:T(8,128)(2,1)S(1)}, bf16[2048,512]{1,0:T(8,128)(2,1)}, u32[]{:S(2)}) %copy-start.4) | copy-done | bytes 2097176
  14.4 1.6 %copy-done.6 = bf16[2048,512]{1,0:T(8,128)(2,1)S(1)} copy-done((bf16[2048,512]{1,0:T(8,128)(2,1)S(1)}, bf16[2048,512]{1,0:T(8,128)(2,1)}, u32[]{:S(2)}) %copy-start.6) | copy-done | bytes 2097176
  16.0 0.7 copy-done.12
  16.7 0.7 copy-done.16
  17.4 0.7 copy-done.20
  18.1 5.1 %shard_map.154 = (bf16[1024,1024]{1,0:T(8,128)(2,1)S(1)}, bf16[1024,512]{1,0:T(8,128)(2,1)S(1)}, f32[8,4,128,128]{3,2,1,0:T(8,128)S(1)}, f32[8,8,512]{2,1,0:T(8,128)S(1)}) custom-call(s32[1]{0:T(128)} %bitcast.t, s32[64]{0:T(128)S(1)} %copy-done.20, bf16[128,2048]{1,0:T(8,128)(2,1)} %get-tuple-element.38.refs_0_, ...), custom_call_target="tpu_custom_call" | custom-call | flops 3221225472 | bytes 12582912 | tf_op jit(solution)/shard_map/pallas_call | solution.py:238
  23.3 2.7 %collective-permute-start.3 = (bf16[128,2048]{1,0:T(8,128)(2,1)}, bf16[128,2048]{1,0:T(8,128)(2,1)S(1)}, u32[]{:S(2)}, u32[]{:S(2)}) collective-permute-start(bf16[128,2048]{1,0:T(8,128)(2,1)} %collective-permute-done.2.refs_1_), channel_id=1, source_target_pairs={{0,3},{1,0},{2,1},{3,2},{4,7},{5,4},{6,5},{7,6},{8,11},{9,8},{10,9... | collective-permute-start | bytes 1572872 | tf_op jit(solution)/shard_map/ppermute | solution.py:514
  26.0 4.8 %shard_map.155 = (bf16[1024,1024]{1,0:T(8,128)(2,1)S(1)}, bf16[1024,512]{1,0:T(8,128)(2,1)S(1)}, f32[8,4,128,128]{3,2,1,0:T(8,128)S(1)}, f32[8,8,512]{2,1,0:T(8,128)S(1)}) custom-call(s32[1]{0:T(128)} %bitcast.t, s32[64]{0:T(128)S(1)} %copy-done.21, ...), custom_call_target="tpu_custom_call", output_to_operand_aliasing={{0}: (11, {}), {1}: (12, {}), {2}: (13, {}), {3}: (14, {})} | custom-call | flops 3221225472 | bytes 12582912 | tf_op jit(solution)/shard_map/pallas_call | solution.py:238
  30.8 4.8 %shard_map.156 = (bf16[1024,1024]{1,0:T(8,128)(2,1)S(1)}, bf16[1024,512]{1,0:T(8,128)(2,1)S(1)}, f32[8,4,128,128]{3,2,1,0:T(8,128)S(1)}, f32[8,8,512]{2,1,0:T(8,128)S(1)}) custom-call(s32[1]{0:T(128)} %bitcast.t, s32[64]{0:T(128)S(1)} %copy-done.21, ...), custom_call_target="tpu_custom_call", output_to_operand_aliasing={{0}: (11, {}), {1}: (12, {}), {2}: (13, {}), {3}: (14, {})} | custom-call | flops 3221225472 | bytes 12582912 | tf_op jit(solution)/shard_map/pallas_call | solution.py:238
  35.7 5.1 %collective-permute-done.1.refs_0_ = bf16[128,2048]{1,0:T(8,128)(2,1)S(1)} collective-permute-done((bf16[128,2048]{1,0:T(8,128)(2,1)}, bf16[128,2048]{1,0:T(8,128)(2,1)S(1)}, u32[]{:S(2)}, u32[]{:S(2)}) %collective-permute-start.1) | collective-permute-done | bytes 524320 | tf_op jit(solution)/shard_map/ppermute | solution.py:514
  40.8 4.8 %shard_map.157 = (bf16[1024,1024]{1,0:T(8,128)(2,1)S(1)}, bf16[1024,512]{1,0:T(8,128)(2,1)S(1)}, bf16[32,24,128]{2,1,0:T(8,128)(2,1)}, bf16[8,4,128,128]{3,2,1,0...) custom-call(s32[1]{0:T(128)} %bitcast.t, ...), custom_call_target="tpu_custom_call", output_to_operand_aliasing={{0}: (11, {}), {1}: (12, {})} | custom-call | flops 3221225472 | bytes 12582912 | tf_op jit(solution)/shard_map/pallas_call | solution.py:238
  45.7 1.0 copy-done.10
  46.7 1.0 copy-done.28
  47.7 4.9 %collective-permute-start.6 = (bf16[32,512]{1,0:T(8,128)(2,1)S(1)}, bf16[32,512]{1,0:T(8,128)(2,1)S(1)}, u32[]{:S(2)}, u32[]{:S(2)}) collective-permute-start(bf16[32,512]{1,0:T(8,128)(2,1)S(1)} %get-tuple-element.57), channel_id=1, source_target_pairs={{0,4},{4,8},{8,12},{12,16},{16,20},{20,24},{24,28},{28,32},{32,36}... | collective-permute-start | bytes 98312 | tf_op jit(solution)/shard_map/ppermute | solution.py:553
  52.5 7.9 %all-to-all-start = ((bf16[32,24,128]{2,1,0:T(8,128)(2,1)}), bf16[32,24,128]{2,1,0:T(8,128)(2,1)S(1)}, u32[]{:S(2)}, u32[]{:S(2)}) async-start(bf16[32,24,128]{2,1,0:T(8,128)(2,1)} %get-tuple-element.55), calls=%async_computation | async-start | bytes 393216 | tf_op jit(solution)/shard_map/all_to_all | solution.py:270
  60.5 0.6 copy-done.38
  61.1 9.8 %filter_rows.1 = (f32[1024,512]{1,0:T(8,128)}, f32[8,1024]{1,0:T(8,128)}) custom-call(s32[1]{0:T(128)} %bitcast.t, s32[64]{0:T(128)} %constant.6.clone.places, bf16[1024,512]{1,0:T(8,128)(2,1)} %copy-done.10, bf16[32,512]{1,0:T(8,128)(2,1)} %copy-done.38, f32[31,512]{1,0:T(8,128)} %taps.1), custom_call_target="tpu_custom_call" | custom-call | flops 7000000000 | bytes 5242880 | tf_op jit(solution)/shard_map/filter_rows/pallas_call | solution.py:325
  70.9 1.2 collective-permute-start.7
  72.1 2.6 %collective-permute-start.8 = (f32[8,1024]{1,0:T(8,128)}, f32[8,1024]{1,0:T(8,128)S(1)}, u32[]{:S(2)}, u32[]{:S(2)}) collective-permute-start(f32[8,1024]{1,0:T(8,128)} %get-tuple-element.59.refs_12_.refs_7_), channel_id=1, source_target_pairs={{0,2},{1,3},{2,0},{3,1},{4,6},{5,7},{6,4},{7,5},{8,10},{9,11},{10,... | collective-permute-start | bytes 98312 | tf_op jit(solution)/shard_map/ppermute | solution.py:514
  74.7 0.7 collective-permute-start.9
  75.4 0.7 prefix.1
  76.1 8.2 %all-to-all-start.1 = ((bf16[32,16,128]{2,1,0:T(8,128)(2,1)}), bf16[32,16,128]{2,1,0:T(8,128)(2,1)S(1)}, u32[]{:S(2)}, u32[]{:S(2)}) async-start(bf16[32,16,128]{2,1,0:T(8,128)(2,1)} %prefix.1), calls=%async_computation.1 | async-start | bytes 262144 | tf_op jit(solution)/shard_map/all_to_all | solution.py:278
  84.4 7.5 %shard_map.161 = (f32[256,512]{1,0:T(8,128)}, bf16[256,512]{1,0:T(8,128)(2,1)}, bf16[256,512]{1,0:T(8,128)(2,1)}) custom-call(s32[1]{0:T(128)} %bitcast.t, s32[64]{0:T(128)} %constant.6.clone.places, bf16[128,2048]{1,0:T(8,128)(2,1)} %copy-done.14, bf16[128,2048]{1,0:T(8,128)(2,1)} %copy-done.15, bf16[1024,1024]{1,0:T(8,128)(2,1)} %copy-done.8, ...), custom_call_target="tpu_custom_call" | custom-call | flops 2147483648 | bytes 6291456 | tf_op jit(solution)/shard_map/pallas_call | solution.py:401
  92.0 1.6 %copy-done.26 = bf16[512,2048]{1,0:T(8,128)(2,1)S(1)} copy-done((bf16[512,2048]{1,0:T(8,128)(2,1)S(1)}, bf16[512,2048]{1,0:T(8,128)(2,1)}, u32[]{:S(2)}) %copy-start.26) | copy-done | bytes 2097176
  93.6 1.0 copy-done.33
  94.6 0.9 copy-done.34
  95.6 0.9 copy-done.35
  96.5 1.6 %copy-done.36 = f32[1024,512]{1,0:T(8,128)S(1)} copy-done((f32[1024,512]{1,0:T(8,128)S(1)}, f32[1024,512]{1,0:T(8,128)}, u32[]{:S(2)}) %copy-start.36) | copy-done | bytes 2097176
  98.2 3.4 %shard_map.162 = (bf16[128,2048]{1,0:T(8,128)(2,1)S(1)}, bf16[128,2048]{1,0:T(8,128)(2,1)S(1)}) custom-call(s32[1]{0:T(128)} %bitcast.t, s32[64]{0:T(128)S(1)} %copy-done.22, f32[256,512]{1,0:T(8,128)S(1)} %copy-done.33, bf16[256,512]{1,0:T(8,128)(2,1)S(1)} %copy-done.34, bf16[256,512]{1,0:T(8,128)(2,1)S(1)} %copy-done.35, ...), custom_call_target="tpu_custom_call" | custom-call | flops 6442450944 | bytes 10485760 | tf_op jit(solution)/shard_map/pallas_call | solution.py:496
  101.5 0.9 collective-permute-start.12
  102.4 1.9 %collective-permute-start.14 = (bf16[128,2048]{1,0:T(8,128)(2,1)S(1)}, bf16[128,2048]{1,0:T(8,128)(2,1)S(1)}, u32[]{:S(2)}, u32[]{:S(2)}) collective-permute-start(bf16[128,2048]{1,0:T(8,128)(2,1)S(1)} %get-tuple-element.70), channel_id=1, source_target_pairs={{0,3},{1,0},{2,1},{3,2},{4,7},{5,4},{6,5},{7,6},{8,11},{9,8},{10,9... | collective-permute-start | bytes 1572872 | tf_op jit(solution)/shard_map/ppermute | solution.py:514
  104.3 7.6 %shard_map.159 = (bf16[128,2048]{1,0:T(8,128)(2,1)S(1)}, bf16[128,2048]{1,0:T(8,128)(2,1)S(1)}) custom-call(s32[1]{0:T(128)} %bitcast.t, s32[64]{0:T(128)S(1)} %copy-done.22, bf16[128,2048]{1,0:T(8,128)(2,1)} %collective-permute-done.refs_0_, bf16[128,2048]{1,0:T(8,128)(2,1)} %collective-permute-done.2.refs_1_, bf16[1024,1024]{1,0:T(8,128)(2,1)S(1)} %copy-done.9, ...), custom_call_target="tpu_custom_call" | custom-call | flops 6442450944 | bytes 10485760 | tf_op jit(solution)/shard_map/pallas_call | solution.py:496
  112.0 1.4 %collective-permute-start.11 = (bf16[128,2048]{1,0:T(8,128)(2,1)S(1)}, bf16[128,2048]{1,0:T(8,128)(2,1)S(1)}, u32[]{:S(2)}, u32[]{:S(2)}) collective-permute-start(bf16[128,2048]{1,0:T(8,128)(2,1)S(1)} %get-tuple-element.63), channel_id=1, source_target_pairs={{0,1},{1,2},{2,3},{3,0},{4,5},{5,6},{6,7},{7,4},{8,9},{9,10},{10,1... | collective-permute-start | bytes 1572872 | tf_op jit(solution)/shard_map/ppermute | solution.py:514
  113.4 7.5 %shard_map.160 = (bf16[128,2048]{1,0:T(8,128)(2,1)S(1)}, bf16[128,2048]{1,0:T(8,128)(2,1)S(1)}) custom-call(s32[1]{0:T(128)} %bitcast.t, s32[64]{0:T(128)S(1)} %copy-done.22, bf16[128,2048]{1,0:T(8,128)(2,1)} %collective-permute-done.4.refs_0_, bf16[128,2048]{1,0:T(8,128)(2,1)} %collective-permute-done.5.refs_1_, bf16[1024,1024]{1,0:T(8,128)(2,1)S(1)} %copy-done.9, ...), custom_call_target="tpu_custom_call" | custom-call | flops 6442450944 | bytes 10485760 | tf_op jit(solution)/shard_map/pallas_call | solution.py:496
  121.0 7.6 %shard_map.158 = (bf16[128,2048]{1,0:T(8,128)(2,1)S(1)}, bf16[128,2048]{1,0:T(8,128)(2,1)S(1)}) custom-call(s32[1]{0:T(128)} %bitcast.t, s32[64]{0:T(128)S(1)} %copy-done.22, bf16[128,2048]{1,0:T(8,128)(2,1)} %get-tuple-element.38.refs_0_, bf16[128,2048]{1,0:T(8,128)(2,1)} %get-tuple-element.39.refs_1_, bf16[1024,1024]{1,0:T(8,128)(2,1)S(1)} %copy-done.9, ...), custom_call_target="tpu_custom_call" | custom-call | flops 6442450944 | bytes 10485760 | tf_op jit(solution)/shard_map/pallas_call | solution.py:496
  128.7 0.2 collective-permute-start.13
  129.0 2.7 %collective-permute-start.15 = (bf16[128,2048]{1,0:T(8,128)(2,1)S(1)}, bf16[128,2048]{1,0:T(8,128)(2,1)S(1)}, u32[]{:S(2)}, u32[]{:S(2)}) collective-permute-start(bf16[128,2048]{1,0:T(8,128)(2,1)S(1)} %add_convert_fusion.1), channel_id=1, source_target_pairs={{0,3},{1,0},{2,1},{3,2},{4,7},{5,4},{6,5},{7,6},{8,11},{9,8},{10,9... | collective-permute-start | bytes 1572872 | tf_op jit(solution)/shard_map/ppermute | solution.py:514
  131.9 0.2 pad_maximum_fusion
  132.1 9.8 %collective-permute-done.13 = bf16[128,2048]{1,0:T(8,128)(2,1)S(1)} collective-permute-done((bf16[128,2048]{1,0:T(8,128)(2,1)S(1)}, bf16[128,2048]{1,0:T(8,128)(2,1)S(1)}, u32[]{:S(2)}, u32[]{:S(2)}) %collective-permute-start.13) | collective-permute-done | bytes 524320 | tf_op jit(solution)/shard_map/ppermute | solution.py:514
  141.9 1.3 add_convert_fusion
  (84 shorter events, 1.0 us)
Async XLA Ops:
  0.0 1.2 copy-start.11
  3.5 19.7 %collective-permute-start = (bf16[128,2048]{1,0:T(8,128)(2,1)}, bf16[128,2048]{1,0:T(8,128)(2,1)}, u32[]{:S(2)}, u32[]{:S(2)}) collective-permute-start(bf16[128,2048]{1,0:T(8,128)(2,1)} %get-tuple-element.38.refs_0_), channel_id=1, source_target_pairs={{0,1},{1,2},{2,3},{3,0},{4,5},{5,6},{6,7},{7,4},{8,9},{9,10},{10,1... | collective-permute-start | bytes 1572872 | tf_op jit(solution)/shard_map/ppermute | solution.py:514
  5.6 17.7 %collective-permute-start.2 = (bf16[128,2048]{1,0:T(8,128)(2,1)}, bf16[128,2048]{1,0:T(8,128)(2,1)}, u32[]{:S(2)}, u32[]{:S(2)}) collective-permute-start(bf16[128,2048]{1,0:T(8,128)(2,1)} %get-tuple-element.39.refs_1_), channel_id=1, source_target_pairs={{0,3},{1,0},{2,1},{3,2},{4,7},{5,4},{6,5},{7,6},{8,11},{9,8},{10,9... | collective-permute-start | bytes 1572872 | tf_op jit(solution)/shard_map/ppermute | solution.py:514
  7.0 23.9 %collective-permute-start.4 = (bf16[128,2048]{1,0:T(8,128)(2,1)}, bf16[128,2048]{1,0:T(8,128)(2,1)}, u32[]{:S(2)}, u32[]{:S(2)}) collective-permute-start(bf16[128,2048]{1,0:T(8,128)(2,1)} %get-tuple-element.39.refs_1_), channel_id=1, source_target_pairs={{0,1},{1,2},{2,3},{3,0},{4,5},{5,6},{6,7},{7,4},{8,9},{9,10},{10,1... | collective-permute-start | bytes 1572872 | tf_op jit(solution)/shard_map/ppermute | solution.py:514
  7.1 23.8 %collective-permute-start.5 = (bf16[128,2048]{1,0:T(8,128)(2,1)}, bf16[128,2048]{1,0:T(8,128)(2,1)}, u32[]{:S(2)}, u32[]{:S(2)}) collective-permute-start(bf16[128,2048]{1,0:T(8,128)(2,1)} %get-tuple-element.38.refs_0_), channel_id=1, source_target_pairs={{0,3},{1,0},{2,1},{3,2},{4,7},{5,4},{6,5},{7,6},{8,11},{9,8},{10,9... | collective-permute-start | bytes 1572872 | tf_op jit(solution)/shard_map/ppermute | solution.py:514
  9.6 1.6 %copy-start = (bf16[2048,512]{1,0:T(8,128)(2,1)S(1)}, bf16[2048,512]{1,0:T(8,128)(2,1)}, u32[]{:S(2)}) copy-start(bf16[2048,512]{1,0:T(8,128)(2,1)} %refs_5_.7) | copy-start | bytes 6291460
  11.2 1.6 %copy-start.2 = (bf16[2048,512]{1,0:T(8,128)(2,1)S(1)}, bf16[2048,512]{1,0:T(8,128)(2,1)}, u32[]{:S(2)}) copy-start(bf16[2048,512]{1,0:T(8,128)(2,1)} %refs_6_.7) | copy-start | bytes 6291460
  12.8 1.6 %copy-start.4 = (bf16[2048,512]{1,0:T(8,128)(2,1)S(1)}, bf16[2048,512]{1,0:T(8,128)(2,1)}, u32[]{:S(2)}) copy-start(bf16[2048,512]{1,0:T(8,128)(2,1)} %refs_7_.7) | copy-start | bytes 6291460
  14.4 1.6 %copy-start.6 = (bf16[2048,512]{1,0:T(8,128)(2,1)S(1)}, bf16[2048,512]{1,0:T(8,128)(2,1)}, u32[]{:S(2)}) copy-start(bf16[2048,512]{1,0:T(8,128)(2,1)} %refs_8_.7) | copy-start | bytes 6291460
  18.1 7.9 %copy-start.1 = (bf16[2048,512]{1,0:T(8,128)(2,1)S(1)}, bf16[2048,512]{1,0:T(8,128)(2,1)}, u32[]{:S(2)}) copy-start(bf16[2048,512]{1,0:T(8,128)(2,1)} %refs_5_.7) | copy-start | bytes 6291460
  18.1 7.9 %copy-start.3 = (bf16[2048,512]{1,0:T(8,128)(2,1)S(1)}, bf16[2048,512]{1,0:T(8,128)(2,1)}, u32[]{:S(2)}) copy-start(bf16[2048,512]{1,0:T(8,128)(2,1)} %refs_6_.7) | copy-start | bytes 6291460
  18.1 7.9 %copy-start.5 = (bf16[2048,512]{1,0:T(8,128)(2,1)S(1)}, bf16[2048,512]{1,0:T(8,128)(2,1)}, u32[]{:S(2)}) copy-start(bf16[2048,512]{1,0:T(8,128)(2,1)} %refs_7_.7) | copy-start | bytes 6291460
  18.1 7.9 %copy-start.7 = (bf16[2048,512]{1,0:T(8,128)(2,1)S(1)}, bf16[2048,512]{1,0:T(8,128)(2,1)}, u32[]{:S(2)}) copy-start(bf16[2048,512]{1,0:T(8,128)(2,1)} %refs_8_.7) | copy-start | bytes 6291460
  18.1 7.9 %copy-start.17 = (f32[512]{0:T(512)S(1)}, f32[512]{0:T(512)}, u32[]{:S(2)}) copy-start(f32[512]{0:T(512)} %param.24) | copy-start | bytes 6148
  18.1 7.9 %copy-start.21 = (s32[64]{0:T(128)S(1)}, s32[64]{0:T(128)}, u32[]{:S(2)}) copy-start(s32[64]{0:T(128)} %constant.6.clone.places) | copy-start | bytes 772
  23.2 17.6 %collective-permute-start.1 = (bf16[128,2048]{1,0:T(8,128)(2,1)}, bf16[128,2048]{1,0:T(8,128)(2,1)S(1)}, u32[]{:S(2)}, u32[]{:S(2)}) collective-permute-start(bf16[128,2048]{1,0:T(8,128)(2,1)} %collective-permute-done.refs_0_), channel_id=1, source_target_pairs={{0,1},{1,2},{2,3},{3,0},{4,5},{5,6},{6,7},{7,4},{8,9},{9,10},{10,1... | collective-permute-start | bytes 1572872 | tf_op jit(solution)/shard_map/ppermute | solution.py:514
  23.3 17.5 %collective-permute-start.3 = (bf16[128,2048]{1,0:T(8,128)(2,1)}, bf16[128,2048]{1,0:T(8,128)(2,1)S(1)}, u32[]{:S(2)}, u32[]{:S(2)}) collective-permute-start(bf16[128,2048]{1,0:T(8,128)(2,1)} %collective-permute-done.2.refs_1_), channel_id=1, source_target_pairs={{0,3},{1,0},{2,1},{3,2},{4,7},{5,4},{6,5},{7,6},{8,11},{9,8},{10,9... | collective-permute-start | bytes 1572872 | tf_op jit(solution)/shard_map/ppermute | solution.py:514
  40.8 4.8 %copy-start.14 = (bf16[128,2048]{1,0:T(8,128)(2,1)}, bf16[128,2048]{1,0:T(8,128)(2,1)S(1)}, u32[]{:S(2)}) copy-start(bf16[128,2048]{1,0:T(8,128)(2,1)S(1)} %collective-permute-done.1.refs_0_) | copy-start | bytes 1572868
  40.8 4.8 %copy-start.15 = (bf16[128,2048]{1,0:T(8,128)(2,1)}, bf16[128,2048]{1,0:T(8,128)(2,1)S(1)}, u32[]{:S(2)}) copy-start(bf16[128,2048]{1,0:T(8,128)(2,1)S(1)} %collective-permute-done.3.refs_1_) | copy-start | bytes 1572868
  47.6 23.2 %copy-start.8 = (bf16[1024,1024]{1,0:T(8,128)(2,1)}, bf16[1024,1024]{1,0:T(8,128)(2,1)S(1)}, u32[]{:S(2)}) copy-start(bf16[1024,1024]{1,0:T(8,128)(2,1)S(1)} %get-tuple-element.52.refs_2_) | copy-start | bytes 6291460
  47.7 12.8 %collective-permute-start.6 = (bf16[32,512]{1,0:T(8,128)(2,1)S(1)}, bf16[32,512]{1,0:T(8,128)(2,1)S(1)}, u32[]{:S(2)}, u32[]{:S(2)}) collective-permute-start(bf16[32,512]{1,0:T(8,128)(2,1)S(1)} %get-tuple-element.57), channel_id=1, source_target_pairs={{0,4},{4,8},{8,12},{12,16},{16,20},{20,24},{24,28},{28,32},{32,36}... | collective-permute-start | bytes 98312 | tf_op jit(solution)/shard_map/ppermute | solution.py:553
  52.5 22.8 %all-to-all-start = ((bf16[32,24,128]{2,1,0:T(8,128)(2,1)}), bf16[32,24,128]{2,1,0:T(8,128)(2,1)S(1)}, u32[]{:S(2)}, u32[]{:S(2)}) async-start(bf16[32,24,128]{2,1,0:T(8,128)(2,1)} %get-tuple-element.55), calls=%async_computation | async-start | bytes 393216 | tf_op jit(solution)/shard_map/all_to_all | solution.py:270
  70.9 21.0 %collective-permute-start.7 = (f32[8,1024]{1,0:T(8,128)}, f32[8,1024]{1,0:T(8,128)S(1)}, u32[]{:S(2)}, u32[]{:S(2)}) collective-permute-start(f32[8,1024]{1,0:T(8,128)} %get-tuple-element.59.refs_12_.refs_7_), channel_id=1, source_target_pairs={{0,1},{1,2},{2,3},{3,0},{4,5},{5,6},{6,7},{7,4},{8,9},{9,10},{10,1... | collective-permute-start | bytes 98312 | tf_op jit(solution)/shard_map/ppermute | solution.py:514
  72.1 19.8 %collective-permute-start.8 = (f32[8,1024]{1,0:T(8,128)}, f32[8,1024]{1,0:T(8,128)S(1)}, u32[]{:S(2)}, u32[]{:S(2)}) collective-permute-start(f32[8,1024]{1,0:T(8,128)} %get-tuple-element.59.refs_12_.refs_7_), channel_id=1, source_target_pairs={{0,2},{1,3},{2,0},{3,1},{4,6},{5,7},{6,4},{7,5},{8,10},{9,11},{10,... | collective-permute-start | bytes 98312 | tf_op jit(solution)/shard_map/ppermute | solution.py:514
  74.7 17.2 %collective-permute-start.9 = (f32[8,1024]{1,0:T(8,128)}, f32[8,1024]{1,0:T(8,128)S(1)}, u32[]{:S(2)}, u32[]{:S(2)}) collective-permute-start(f32[8,1024]{1,0:T(8,128)} %get-tuple-element.59.refs_12_.refs_7_), channel_id=1, source_target_pairs={{0,3},{1,0},{2,1},{3,2},{4,7},{5,4},{6,5},{7,6},{8,11},{9,8},{10,9... | collective-permute-start | bytes 98312 | tf_op jit(solution)/shard_map/ppermute | solution.py:514
  76.1 15.8 %all-to-all-start.1 = ((bf16[32,16,128]{2,1,0:T(8,128)(2,1)}), bf16[32,16,128]{2,1,0:T(8,128)(2,1)S(1)}, u32[]{:S(2)}, u32[]{:S(2)}) async-start(bf16[32,16,128]{2,1,0:T(8,128)(2,1)} %prefix.1), calls=%async_computation.1 | async-start | bytes 262144 | tf_op jit(solution)/shard_map/all_to_all | solution.py:278
  84.4 7.6 %copy-start.22 = (s32[64]{0:T(128)S(1)}, s32[64]{0:T(128)}, u32[]{:S(2)}) copy-start(s32[64]{0:T(128)} %constant.6.clone.places) | copy-start | bytes 772
  84.4 7.6 %copy-start.25 = (bf16[512,2048]{1,0:T(8,128)(2,1)S(1)}, bf16[512,2048]{1,0:T(8,128)(2,1)}, u32[]{:S(2)}) copy-start(bf16[512,2048]{1,0:T(8,128)(2,1)} %refs_11_.1) | copy-start | bytes 6291460
  84.4 7.6 %copy-start.29 = (bf16[8,4,128,128]{3,2,1,0:T(8,128)(2,1)S(1)}, bf16[8,4,128,128]{3,2,1,0:T(8,128)(2,1)}, u32[]{:S(2)}) copy-start(bf16[8,4,128,128]{3,2,1,0:T(8,128)(2,1)} %copy-done.28) | copy-start | bytes 3145732
  84.4 7.6 %copy-start.30 = (f32[8,1024]{1,0:T(8,128)S(1)}, f32[8,1024]{1,0:T(8,128)}, u32[]{:S(2)}) copy-start(f32[8,1024]{1,0:T(8,128)} %get-tuple-element.59.refs_12_.refs_7_) | copy-start | bytes 98308
  84.4 7.6 %copy-start.31 = (f32[512]{0:T(512)S(1)}, f32[512]{0:T(512)}, u32[]{:S(2)}) copy-start(f32[512]{0:T(512)} %param.28) | copy-start | bytes 6148
  84.4 7.6 %copy-start.32 = (f32[128]{0:T(128)S(1)}, f32[128]{0:T(128)}, u32[]{:S(2)}) copy-start(f32[128]{0:T(128)} %param.26) | copy-start | bytes 1540
  92.0 1.6 %copy-start.26 = (bf16[512,2048]{1,0:T(8,128)(2,1)S(1)}, bf16[512,2048]{1,0:T(8,128)(2,1)}, u32[]{:S(2)}) copy-start(bf16[512,2048]{1,0:T(8,128)(2,1)} %refs_12_.1) | copy-start | bytes 6291460
  93.6 1.0 copy-start.33
  96.5 1.6 %copy-start.36 = (f32[1024,512]{1,0:T(8,128)S(1)}, f32[1024,512]{1,0:T(8,128)}, u32[]{:S(2)}) copy-start(f32[1024,512]{1,0:T(8,128)} %get-tuple-element.58.refs_11_.refs_6_) | copy-start | bytes 6291460
  98.1 6.2 %copy-start.9 = (bf16[1024,1024]{1,0:T(8,128)(2,1)S(1)}, bf16[1024,1024]{1,0:T(8,128)(2,1)}, u32[]{:S(2)}) copy-start(bf16[1024,1024]{1,0:T(8,128)(2,1)} %copy-done.8) | copy-start | bytes 6291460
  98.1 6.2 %copy-start.13 = (f32[1024,4]{0,1:T(4,128)S(1)}, f32[1024,4]{0,1:T(4,128)}, u32[]{:S(2)}) copy-start(f32[1024,4]{0,1:T(4,128)} %param.25) | copy-start | bytes 49156
  98.1 6.2 %copy-start.18 = (f32[512]{0:T(512)S(1)}, f32[512]{0:T(512)}, u32[]{:S(2)}) copy-start(f32[512]{0:T(512)} %param.24) | copy-start | bytes 6148
  98.1 6.2 %copy-start.23 = (bf16[2048,512]{1,0:T(8,128)(2,1)S(1)}, bf16[2048,512]{1,0:T(8,128)(2,1)}, u32[]{:S(2)}) copy-start(bf16[2048,512]{1,0:T(8,128)(2,1)} %refs_3_.7) | copy-start | bytes 6291460
  98.1 6.2 %copy-start.24 = (bf16[2048,512]{1,0:T(8,128)(2,1)S(1)}, bf16[2048,512]{1,0:T(8,128)(2,1)}, u32[]{:S(2)}) copy-start(bf16[2048,512]{1,0:T(8,128)(2,1)} %refs_4_.7) | copy-start | bytes 6291460
  98.2 6.2 %copy-start.27 = (bf16[512,2048]{1,0:T(8,128)(2,1)S(1)}, bf16[512,2048]{1,0:T(8,128)(2,1)}, u32[]{:S(2)}) copy-start(bf16[512,2048]{1,0:T(8,128)(2,1)} %refs_12_.1) | copy-start | bytes 6291460
  101.5 27.0 %collective-permute-start.12 = (bf16[128,2048]{1,0:T(8,128)(2,1)S(1)}, bf16[128,2048]{1,0:T(8,128)(2,1)S(1)}, u32[]{:S(2)}, u32[]{:S(2)}) collective-permute-start(bf16[128,2048]{1,0:T(8,128)(2,1)S(1)} %get-tuple-element.68), channel_id=1, source_target_pairs={{0,1},{1,2},{2,3},{3,0},{4,5},{5,6},{6,7},{7,4},{8,9},{9,10},{10,1... | collective-permute-start | bytes 1572872 | tf_op jit(solution)/shard_map/ppermute | solution.py:514
  102.4 26.5 %collective-permute-start.14 = (bf16[128,2048]{1,0:T(8,128)(2,1)S(1)}, bf16[128,2048]{1,0:T(8,128)(2,1)S(1)}, u32[]{:S(2)}, u32[]{:S(2)}) collective-permute-start(bf16[128,2048]{1,0:T(8,128)(2,1)S(1)} %get-tuple-element.70), channel_id=1, source_target_pairs={{0,3},{1,0},{2,1},{3,2},{4,7},{5,4},{6,5},{7,6},{8,11},{9,8},{10,9... | collective-permute-start | bytes 1572872 | tf_op jit(solution)/shard_map/ppermute | solution.py:514
  111.9 19.8 %collective-permute-start.10 = (bf16[128,2048]{1,0:T(8,128)(2,1)S(1)}, bf16[128,2048]{1,0:T(8,128)(2,1)S(1)}, u32[]{:S(2)}, u32[]{:S(2)}) collective-permute-start(bf16[128,2048]{1,0:T(8,128)(2,1)S(1)} %get-tuple-element.61), channel_id=1, source_target_pairs={{0,3},{1,0},{2,1},{3,2},{4,7},{5,4},{6,5},{7,6},{8,11},{9,8},{10,9... | collective-permute-start | bytes 1572872 | tf_op jit(solution)/shard_map/ppermute | solution.py:514
  112.0 9.0 %copy-start.37 = (f32[1024,512]{1,0:T(8,128)S(1)}, f32[1024,512]{1,0:T(8,128)}, u32[]{:S(2)}) copy-start(f32[1024,512]{1,0:T(8,128)} %get-tuple-element.58.refs_11_.refs_6_) | copy-start | bytes 6291460
  112.0 19.8 %collective-permute-start.11 = (bf16[128,2048]{1,0:T(8,128)(2,1)S(1)}, bf16[128,2048]{1,0:T(8,128)(2,1)S(1)}, u32[]{:S(2)}, u32[]{:S(2)}) collective-permute-start(bf16[128,2048]{1,0:T(8,128)(2,1)S(1)} %get-tuple-element.63), channel_id=1, source_target_pairs={{0,1},{1,2},{2,3},{3,0},{4,5},{5,6},{6,7},{7,4},{8,9},{9,10},{10,1... | collective-permute-start | bytes 1572872 | tf_op jit(solution)/shard_map/ppermute | solution.py:514
  128.7 13.2 %collective-permute-start.13 = (bf16[128,2048]{1,0:T(8,128)(2,1)S(1)}, bf16[128,2048]{1,0:T(8,128)(2,1)S(1)}, u32[]{:S(2)}, u32[]{:S(2)}) collective-permute-start(bf16[128,2048]{1,0:T(8,128)(2,1)S(1)} %add_convert_fusion.2), channel_id=1, source_target_pairs={{0,1},{1,2},{2,3},{3,0},{4,5},{5,6},{6,7},{7,4},{8,9},{9,10},{10,1... | collective-permute-start | bytes 1572872 | tf_op jit(solution)/shard_map/ppermute | solution.py:514
  129.0 12.9 %collective-permute-start.15 = (bf16[128,2048]{1,0:T(8,128)(2,1)S(1)}, bf16[128,2048]{1,0:T(8,128)(2,1)S(1)}, u32[]{:S(2)}, u32[]{:S(2)}) collective-permute-start(bf16[128,2048]{1,0:T(8,128)(2,1)S(1)} %add_convert_fusion.1), channel_id=1, source_target_pairs={{0,3},{1,0},{2,1},{3,2},{4,7},{5,4},{6,5},{7,6},{8,11},{9,8},{10,9... | collective-permute-start | bytes 1572872 | tf_op jit(solution)/shard_map/ppermute | solution.py:514
  (9 other events, 7.2 us)
